TPU v7x, 256 devices: a whole 4x4x8 slice. The times are simulated.
256 devices in a mesh: tp: 32 (over z, y), dp: 8 (over x, core).
Axes of the slice: x: 4, y: 4, z: 8, core: 2. Of those that a mesh axis runs over, the one named last changes fastest.
Arguments:
- stream: bfloat16 [256, 2048], P('tp', 'dp'), may hold values from -12 to 12
- norm_gain: float32 [2, 2048], P(None, 'dp'), may hold values from 0.1 to 1.9
- w_input: bfloat16 [2, 2048, 2048], P(None, 'dp', 'tp'), may hold values from -0.125 to 0.125
- lam_re: float32 [2, 128, 64], P(None, 'tp'), may hold values from -1 to -0.05
- lam_im: float32 [2, 128, 64], P(None, 'tp'), may hold values from 0 to 6
- log_dt: float32 [2, 128], P(None, 'tp'), may hold values from -3 to 0
- b_re: float32 [2, 128, 64, 16], P(None, 'tp'), may hold values from -1 to 1
- b_im: float32 [2, 128, 64, 16], P(None, 'tp'), may hold values from -1 to 1
- readout_real: float32 [2, 128, 16, 64], P(None, 'tp'), may hold values from -0.5 to 0.5
- readout_imaginary: float32 [2, 128, 16, 64], P(None, 'tp'), may hold values from -0.5 to 0.5
- d_skip: float32 [2, 2048], P(None, 'tp'), may hold values from -4 to 4
- w_val: bfloat16 [2, 2048, 2048], P(None, 'tp', 'dp'), may hold values from -0.375 to 0.375
- w_gate: bfloat16 [2, 2048, 2048], P(None, 'tp', 'dp'), may hold values from -0.375 to 0.375
- state: float32 [2, 256, 128, 128], P(None, 'dp', 'tp'), may hold values from -6 to 6
Outputs:
- stream_out: bfloat16 [256, 2048], P('tp', 'dp')
- states_out: float32 [2, 256, 128, 128], P(None, 'dp', 'tp')
All inputs are finite; a program needn't handle non-finite values.
Results may differ from a plain program's by a relative error of at most 0.0064.
Values may be sent and summed in bfloat16 or wider, within the bound.
No kernel may reach another device: no remote copies, remote signals or barrier semaphores. Data moves between devices by JAX's collectives and lax.ppermute only.
A program may use at most 64 MiB of HBM per device.

v0:
```python
import jax
import jax.numpy as jnp
from jax import lax
from jax.experimental import pallas as pl
from jax.experimental.pallas import tpu as pltpu
from jax.sharding import Mesh
from jax.sharding import PartitionSpec as P

D = 2048
LAYERS = 2
NZ, NY, NX, NC = 8, 4, 4, 2
ND = NX * NC
TP = ("z", "y")
DP = ("x", "c")
ALL = ("z", "y", "x", "c")
ROWS = 8
SEQS = NY * ROWS
COLS = 256
BLOCK = 64
WIDTH = NZ * BLOCK
PAY = 1024

eps = 1e-06
HIGHEST = lax.Precision.HIGHEST
f32 = jnp.float32
bf16 = jnp.bfloat16


def turn(value):
    pairs = []
    for z in range(NZ):
        for y in range(NY):
            for d in range(ND):
                pairs.append(((z * NY + y) * ND + d, (d * NY + y) * ND + z))
    return lax.ppermute(value, ALL, pairs)


def shift_y(value, k):
    return lax.ppermute(value, "y", [(i, (i + k) % NY) for i in range(NY)])


def shift_z(value, k):
    return lax.ppermute(value, "z", [(i, (i + k) % NZ) for i in range(NZ)])


def ring_z(own):
    up1 = shift_z(own, 1)
    down1 = shift_z(own, -1)
    up2 = shift_z(up1, 1)
    down2 = shift_z(down1, -1)
    up3 = shift_z(up2, 1)
    down3 = shift_z(down2, -1)
    up4 = shift_z(up3, 1)
    return [own, up1, up2, up3, up4, down3, down2, down1]


def two_halves(value):
    high = value.astype(bf16)
    low = (value - high.astype(f32)).astype(bf16)
    return high, low


def prep_kernel(lam_re, lam_im, log_dt, b_re, b_im, r_re, r_im, d_skip, state, base, drive, carried):
    groups, chans, half = b_re.shape[1:]
    size = groups * chans
    row = lax.broadcasted_iota(jnp.int32, (size, size), 0)
    col = lax.broadcasted_iota(jnp.int32, (size, size), 1)
    for n in range(LAYERS):
        steps = jnp.concatenate([jnp.full((1, half), log_dt[n, g], f32) for g in range(groups)])
        step = jnp.exp(steps)
        re, im = lam_re[n], lam_im[n]
        decay = jnp.exp(re * step)
        angle = im * step
        keep_re = decay * jnp.cos(angle)
        keep_im = decay * jnp.sin(angle)
        denom = re * re + im * im
        ratio_re = ((keep_re - 1.0) * re + keep_im * im) / denom
        ratio_im = (keep_im * re - (keep_re - 1.0) * im) / denom
        drives, reads, offsets = [], [], []
        for g in range(groups):
            q_re, q_im = ratio_re[g : g + 1], ratio_im[g : g + 1]
            d_re = q_re * b_re[n, g] - q_im * b_im[n, g]
            d_im = q_re * b_im[n, g] + q_im * b_re[n, g]
            drives.append(jnp.concatenate([d_re, d_im], axis=1))
            reads.append(jnp.concatenate([r_re[n, g], -r_im[n, g]], axis=1))
            k_re, k_im = keep_re[g : g + 1], keep_im[g : g + 1]
            old = state[n, :, g, :]
            swapped = jnp.concatenate([old[:, half:], old[:, :half]], axis=1)
            new = (
                jnp.concatenate([k_re, k_re], axis=1) * old
                + jnp.concatenate([-k_im, k_im], axis=1) * swapped
            )
            base[n, :, g, :] = new
            offsets.append(times_turned(new, reads[g], HIGHEST))
        dcat = jnp.concatenate(drives)
        drive[n] = dcat
        full = times_turned(dcat, jnp.concatenate(reads), HIGHEST)
        mix = jnp.where(row // chans == col // chans, full, 0.0)
        mix = mix + jnp.where(row == col, d_skip[n : n + 1, :], 0.0)
        carried[n, :SEQS, :] = jnp.concatenate(offsets, axis=1)
        carried[n, SEQS:, :] = mix


def write_payload(pay_ref, x, carried, blocks):
    squares = jnp.sum(x * x, axis=1, keepdims=True)
    s_high, s_low = two_halves(squares)
    lane = lax.broadcasted_iota(jnp.int32, (SEQS, 128), 1)
    s_part = jnp.where(lane == 0, s_high.astype(f32), jnp.where(lane == 1, s_low.astype(f32), 0.0))
    o_high, o_low = two_halves(carried[:SEQS])
    m_high, m_low = two_halves(carried[SEQS:])
    half = BLOCK // 2
    row = jnp.concatenate(
        [blocks[j].astype(bf16) for j in range(NZ)]
        + [o_high, o_low, s_part.astype(bf16), m_high[:half], m_high[half:], m_low[:half], m_low[half:]],
        axis=1,
    )
    for i in range(ND):
        pay_ref[i] = row


def times_turned(left, right, precision=None):
    return lax.dot_general(
        left, right, (((1,), (1,)), ((), ())), precision=precision, preferred_element_type=f32
    )


def first_kernel(p0, p1, p2, p3, gain, carried, w, pay_ref, x_ref, rows):
    y = lax.axis_index("y")
    for k, piece in enumerate((p0, p1, p2, p3)):
        rows[lax.rem(y + NY - k, NY)] = piece[...].astype(f32)
    x = rows[...].reshape(SEQS, COLS)
    x_ref[...] = x
    normed = (x * gain[0:1]).astype(bf16)
    blocks = [times_turned(normed, w[j]) for j in range(NZ)]
    write_payload(pay_ref, x, carried[0], blocks)


def next_kernel(out, r1, r2, r3, x_old, gain, carried, *refs):
    w = refs[:NZ]
    pay_ref, x_ref, blocks = refs[NZ:]
    z = lax.axis_index("z")
    total = out[...] + r1[...] + r2[...] + r3[...]
    x = x_old[...] + total[:, :COLS] * jax.nn.sigmoid(total[:, COLS:])
    x = x.astype(bf16).astype(f32)
    x_ref[...] = x
    normed = (x * gain[1:2]).astype(bf16)
    for k in range(NZ):
        blocks[lax.rem(z + NZ - k, NZ)] = times_turned(normed, w[k][:, 4 * COLS :])
    write_payload(pay_ref, x, carried[1], blocks)


def inputs_of(got):
    total = got[0, :, :WIDTH].astype(f32)
    squares = got[0, :, WIDTH + 128 : WIDTH + 256].astype(f32)
    for i in range(1, ND):
        total = total + got[i, :, :WIDTH].astype(f32)
        squares = squares + got[i, :, WIDTH + 128 : WIDTH + 256].astype(f32)
    return total * lax.rsqrt(jnp.sum(squares, axis=1, keepdims=True) / D + eps)


def gated(got, u, w, first_col, mixed, ordered, weights):
    z = lax.axis_index("z")
    for j in range(NZ):
        offset = got[j, :, WIDTH : WIDTH + BLOCK].astype(f32) + got[
            j, :, WIDTH + BLOCK : WIDTH + 2 * BLOCK
        ].astype(f32)
        high, low = two_halves(u[:, j * BLOCK : (j + 1) * BLOCK])
        m = got[j, :, WIDTH + 256 :]
        m_high = jnp.concatenate([m[:, :BLOCK], m[:, BLOCK : 2 * BLOCK]], axis=0)
        m_low = jnp.concatenate([m[:, 2 * BLOCK : 3 * BLOCK], m[:, 3 * BLOCK :]], axis=0)
        pre = (
            offset
            + jnp.dot(high, m_low, preferred_element_type=f32)
            + jnp.dot(low, m_high, preferred_element_type=f32)
            + jnp.dot(high, m_high, preferred_element_type=f32)
        )
        mixed[j] = jax.nn.gelu(pre)
    for k in range(NZ):
        ordered[:, k * BLOCK : (k + 1) * BLOCK] = mixed[lax.rem(z + NZ - k, NZ)].astype(bf16)
        weights[k * BLOCK : (k + 1) * BLOCK, :] = w[k][:, first_col : first_col + 2 * COLS]
    return jnp.dot(ordered[...], weights[...], preferred_element_type=f32)


def own_block(u, u_blocks):
    d = lax.axis_index("x") * NC + lax.axis_index("c")
    for j in range(NZ):
        u_blocks[j] = u[:, j * BLOCK : (j + 1) * BLOCK]
    return u_blocks[d]


def mid_kernel(got, *refs):
    w = refs[:NZ]
    out, own_u, u_blocks, mixed, ordered, weights = refs[NZ:]
    u = inputs_of(got)
    own_u[...] = own_block(u, u_blocks)
    out[...] = gated(got, u, w, 0, mixed, ordered, weights)


def inputs_kernel(got, u_ref, own_u, u_blocks):
    u = inputs_of(got)
    u_ref[...] = u
    own_u[...] = own_block(u, u_blocks)


def last_kernel(got, u, *refs):
    w = refs[:NZ]
    own_out, s1, s2, s3, mixed, ordered, weights, by_y = refs[NZ:]
    out = gated(got, u[...], w, 2 * COLS, mixed, ordered, weights)
    y = lax.axis_index("y")
    by_y[...] = out.reshape(NY, ROWS, 2 * COLS)
    own_out[...] = by_y[y]
    for k, ref in enumerate((s1, s2, s3), 1):
        ref[...] = by_y[lax.rem(y + k, NY)]


def stream_kernel(own, r1, r2, r3, x, out):
    y = lax.axis_index("y")
    total = own[...] + r1[...] + r2[...] + r3[...]
    mine = x[pl.ds(pl.multiple_of(y * ROWS, ROWS), ROWS), :]
    out[...] = (mine + total[:, :COLS] * jax.nn.sigmoid(total[:, COLS:])).astype(bf16)


def states_kernel(base, drive, u0, u1, out):
    groups = base.shape[2]
    chans = BLOCK // groups
    for n, u in enumerate((u0, u1)):
        for g in range(groups):
            cut = slice(g * chans, (g + 1) * chans)
            push = jnp.dot(u[:, cut], drive[n, cut, :], precision=HIGHEST, preferred_element_type=f32)
            out[n, :, g, :] = base[n, :, g, :] + push


def call(body, args, outs, scratch=(), scalar=None):
    spaces = [pltpu.SMEM if i == scalar else pltpu.VMEM for i in range(len(args))]
    return pl.pallas_call(
        body,
        in_specs=[pl.BlockSpec(memory_space=s) for s in spaces],
        out_specs=[pl.BlockSpec(memory_space=pltpu.VMEM) for _ in outs],
        out_shape=outs,
        scratch_shapes=list(scratch),
        compiler_params=pltpu.CompilerParams(vmem_limit_bytes=12 << 20),
        cost_estimate=pl.CostEstimate(flops=1 << 24, bytes_accessed=1 << 20, transcendentals=0),
    )(*args)


def shape(dims, dtype=f32):
    return jax.ShapeDtypeStruct(dims, dtype)


PAY_OUTS = [shape((ND, SEQS, PAY), bf16), shape((SEQS, COLS))]
BLOCKS = pltpu.VMEM((NZ, SEQS, BLOCK), f32)
GATED = [BLOCKS, pltpu.VMEM((SEQS, WIDTH), bf16), pltpu.VMEM((WIDTH, 2 * COLS), bf16)]


def both_layers(
    stream,
    norm_gain,
    w_input,
    lam_re,
    lam_im,
    log_dt,
    b_re,
    b_im,
    readout_real,
    readout_imaginary,
    d_skip,
    w_val,
    w_gate,
    state,
):
    w_turned = jnp.swapaxes(w_input, 1, 2)
    first_w = lax.all_to_all(
        jnp.broadcast_to(w_turned[0][None], (NZ, BLOCK, COLS)), "z", 0, 0, tiled=True
    )
    pieces = [stream] + [shift_y(stream, k) for k in range(1, NY)]
    late = jnp.concatenate([w_val[0], w_gate[0], w_val[1], w_gate[1], w_turned[1]], axis=1)
    ring = ring_z(late)

    base, drive, own = call(
        prep_kernel,
        [
            lam_re,
            lam_im,
            log_dt,
            jnp.swapaxes(b_re, 2, 3),
            jnp.swapaxes(b_im, 2, 3),
            readout_real,
            readout_imaginary,
            d_skip,
            state,
        ],
        [
            shape(state.shape),
            shape((LAYERS, BLOCK, state.shape[-1])),
            shape((LAYERS, SEQS + BLOCK, BLOCK)),
        ],
        scalar=2,
    )
    carried = turn(own)

    payload, x = call(
        first_kernel,
        [*pieces, norm_gain, carried, first_w],
        PAY_OUTS,
        [pltpu.VMEM((NY, ROWS, COLS), f32)],
    )
    got = lax.all_to_all(payload, DP, 0, 0, tiled=True)
    out, u0 = call(
        mid_kernel,
        [got, *ring],
        [shape((SEQS, 2 * COLS)), shape((SEQS, BLOCK))],
        [BLOCKS, *GATED],
    )
    others = [shift_y(out, k) for k in range(1, NY)]
    u0 = turn(u0)
    payload, x = call(next_kernel, [out, *others, x, norm_gain, carried, *ring], PAY_OUTS, [BLOCKS])
    got = lax.all_to_all(payload, DP, 0, 0, tiled=True)
    u, u1 = call(
        inputs_kernel, [got], [shape((SEQS, WIDTH)), shape((SEQS, BLOCK))], [BLOCKS]
    )
    u1 = turn(u1)
    own, s1, s2, s3 = call(
        last_kernel,
        [got, u, *ring],
        [shape((ROWS, 2 * COLS))] * NY,
        [*GATED, pltpu.VMEM((NY, ROWS, 2 * COLS), f32)],
    )
    others = [shift_y(sent, k) for k, sent in enumerate((s1, s2, s3), 1)]
    (stream,) = call(stream_kernel, [own, *others, x], [shape((ROWS, COLS), bf16)])
    (states,) = call(states_kernel, [base, drive, u0, u1], [shape(state.shape)])
    return (stream, states)


def solution(mesh):
    grid = Mesh(mesh.devices.reshape(NZ, NY, NX, NC), ALL)
    return jax.shard_map(
        both_layers,
        mesh=grid,
        in_specs=(
            P(TP, DP),
            P(None, DP),
            P(None, DP, TP),
            P(None, TP, None),
            P(None, TP, None),
            P(None, TP),
            P(None, TP, None, None),
            P(None, TP, None, None),
            P(None, TP, None, None),
            P(None, TP, None, None),
            P(None, TP),
            P(None, TP, DP),
            P(None, TP, DP),
            P(None, DP, TP, None),
        ),
        out_specs=(P(TP, DP), P(None, DP, TP, None)),
        check_vma=False,
    )
```

profile of v0, /device:TPU:4, one launch (start us, length us, event | category | flops | bytes accessed | tf_op | source)
XLA Modules:
  0.0 107.4 jit_solution(17095999884996612423)
XLA Ops:
  2.1 8.6 %all-to-all-start = ((bf16[8,64,256]{2,1,0:T(8,128)(2,1)}), bf16[8,64,256]{2,1,0:T(8,128)(2,1)S(1)}, u32[]{:S(2)}, u32[]{:S(2)}) async-start(bf16[8,64,256]{2,1,0:T(8,128)(2,1)} %broadcast_in_dim.8), calls=%async_computation | async-start | bytes 524288 | tf_op jit(solution)/shard_map/all_to_all | solution.py:272
  10.9 2.1 %collective-permute-start.4 = (bf16[64,1280]{1,0:T(8,128)(2,1)S(1)}, bf16[64,1280]{1,0:T(8,128)(2,1)S(1)}, u32[]{:S(2)}, u32[]{:S(2)}) collective-permute-start(bf16[64,1280]{1,0:T(8,128)(2,1)S(1)} %fusion.refs_0_), channel_id=1, source_target_pairs={{0,32},{32,64},{64,96},{96,128},{128,160},{160,192},{192,224},{224... | collective-permute-start | bytes 491528 | tf_op jit(solution)/shard_map/ppermute | solution.py:43
  13.7 1.2 %shard_map.149 = (f32[2,32,4,128]{3,2,1,0:T(4,128)S(1)}, f32[2,64,128]{2,1,0:T(8,128)S(1)}, f32[2,96,64]{2,1,0:T(8,128)S(1)}) custom-call(f32[2,4,64]{2,1,0:T(4,128)S(1)} %copy-done.6, f32[2,4,64]{2,1,0:T(4,128)S(1)} %copy-done.7, f32[2,4]{1,0:T(2,128)S(1)} %copy-done.9, f32[2,4,16,64]{3,2,1,0:T(8,128)S(1)} %bitcast.17, f32[2,4,16,64]{3,2,1,0:T(8,128)S(1)} %bitcast.18, ...), custom_call_target="tpu_custom_call" | custom-call | flops 16777216 | bytes 1048576 | tf_op jit(solution)/shard_map/pallas_call | solution.py:235
  14.9 6.4 %collective-permute-start.3 = (f32[2,96,64]{2,1,0:T(8,128)S(1)}, f32[2,96,64]{2,1,0:T(8,128)S(1)}, u32[]{:S(2)}, u32[]{:S(2)}) collective-permute-start(f32[2,96,64]{2,1,0:T(8,128)S(1)} %get-tuple-element.17), channel_id=1, source_target_pairs={{0,0},{1,32},{2,64},{3,96},{4,128},{5,160},{6,192},{7,224},{8,8},{... | collective-permute-start | bytes 147464 | tf_op jit(solution)/shard_map/ppermute | solution.py:35
  21.3 2.1 %collective-permute-done.4.refs_1_ = bf16[64,1280]{1,0:T(8,128)(2,1)S(1)} collective-permute-done((bf16[64,1280]{1,0:T(8,128)(2,1)S(1)}, bf16[64,1280]{1,0:T(8,128)(2,1)S(1)}, u32[]{:S(2)}, u32[]{:S(2)}) %collective-permute-start.4) | collective-permute-done | bytes 163872 | tf_op jit(solution)/shard_map/ppermute | solution.py:43
  23.4 1.6 %collective-permute-start = (bf16[8,256]{1,0:T(8,128)(2,1)S(1)}, bf16[8,256]{1,0:T(8,128)(2,1)S(1)}, u32[]{:S(2)}, u32[]{:S(2)}) collective-permute-start(bf16[8,256]{1,0:T(8,128)(2,1)S(1)} %copy-done.8), channel_id=1, source_target_pairs={{0,8},{8,16},{16,24},{24,0},{1,9},{9,17},{17,25},{25,1},{2,10},{10... | collective-permute-start | bytes 12296 | tf_op jit(solution)/shard_map/ppermute | solution.py:39
  25.0 2.9 %collective-permute-start.1 = (bf16[8,256]{1,0:T(8,128)(2,1)S(1)}, bf16[8,256]{1,0:T(8,128)(2,1)S(1)}, u32[]{:S(2)}, u32[]{:S(2)}) collective-permute-start(bf16[8,256]{1,0:T(8,128)(2,1)S(1)} %copy-done.8), channel_id=1, source_target_pairs={{0,16},{8,24},{16,0},{24,8},{1,17},{9,25},{17,1},{25,9},{2,18},{10... | collective-permute-start | bytes 12296 | tf_op jit(solution)/shard_map/ppermute | solution.py:39
  28.3 1.8 %collective-permute-start.2 = (bf16[8,256]{1,0:T(8,128)(2,1)S(1)}, bf16[8,256]{1,0:T(8,128)(2,1)S(1)}, u32[]{:S(2)}, u32[]{:S(2)}) collective-permute-start(bf16[8,256]{1,0:T(8,128)(2,1)S(1)} %copy-done.8), channel_id=1, source_target_pairs={{0,24},{8,0},{16,8},{24,16},{1,25},{9,1},{17,9},{25,17},{2,26},{10... | collective-permute-start | bytes 12296 | tf_op jit(solution)/shard_map/ppermute | solution.py:39
  30.1 1.7 %collective-permute-done.2.p3 = bf16[8,256]{1,0:T(8,128)(2,1)S(1)} collective-permute-done((bf16[8,256]{1,0:T(8,128)(2,1)S(1)}, bf16[8,256]{1,0:T(8,128)(2,1)S(1)}, u32[]{:S(2)}, u32[]{:S(2)}) %collective-permute-start.2) | collective-permute-done | bytes 4128 | tf_op jit(solution)/shard_map/ppermute | solution.py:39
  33.0 4.8 %all-to-all-start.1 = ((bf16[8,32,1024]{2,1,0:T(8,128)(2,1)}), bf16[8,32,1024]{2,1,0:T(8,128)(2,1)S(1)}, u32[]{:S(2)}, u32[]{:S(2)}) async-start(bf16[8,32,1024]{2,1,0:T(8,128)(2,1)} %get-tuple-element.18), calls=%async_computation.1 | async-start | bytes 1048576 | tf_op jit(solution)/shard_map/all_to_all | solution.py:307
  37.8 3.5 %collective-permute-start.9 = (bf16[64,1280]{1,0:T(8,128)(2,1)S(1)}, bf16[64,1280]{1,0:T(8,128)(2,1)S(1)}, u32[]{:S(2)}, u32[]{:S(2)}) collective-permute-start(bf16[64,1280]{1,0:T(8,128)(2,1)S(1)} %collective-permute-done.8.refs_7_), channel_id=1, source_target_pairs={{0,224},{32,0},{64,32},{96,64},{128,96},{160,128},{192,160},{224,1... | collective-permute-start | bytes 491528 | tf_op jit(solution)/shard_map/ppermute | solution.py:43
  41.3 3.7 %collective-permute-done.9.refs_6_ = bf16[64,1280]{1,0:T(8,128)(2,1)S(1)} collective-permute-done((bf16[64,1280]{1,0:T(8,128)(2,1)S(1)}, bf16[64,1280]{1,0:T(8,128)(2,1)S(1)}, u32[]{:S(2)}, u32[]{:S(2)}) %collective-permute-start.9) | collective-permute-done | bytes 163872 | tf_op jit(solution)/shard_map/ppermute | solution.py:43
  45.0 4.1 %collective-permute-start.10 = (bf16[64,1280]{1,0:T(8,128)(2,1)S(1)}, bf16[64,1280]{1,0:T(8,128)(2,1)S(1)}, u32[]{:S(2)}, u32[]{:S(2)}) collective-permute-start(bf16[64,1280]{1,0:T(8,128)(2,1)S(1)} %collective-permute-done.9.refs_6_), channel_id=1, source_target_pairs={{0,224},{32,0},{64,32},{96,64},{128,96},{160,128},{192,160},{224,1... | collective-permute-start | bytes 491528 | tf_op jit(solution)/shard_map/ppermute | solution.py:43
  49.6 2.4 %collective-permute-done.10.refs_5_ = bf16[64,1280]{1,0:T(8,128)(2,1)S(1)} collective-permute-done((bf16[64,1280]{1,0:T(8,128)(2,1)S(1)}, bf16[64,1280]{1,0:T(8,128)(2,1)S(1)}, u32[]{:S(2)}, u32[]{:S(2)}) %collective-permute-start.10) | collective-permute-done | bytes 163872 | tf_op jit(solution)/shard_map/ppermute | solution.py:43
  52.1 4.2 %collective-permute-done.7.refs_4_ = bf16[64,1280]{1,0:T(8,128)(2,1)S(1)} collective-permute-done((bf16[64,1280]{1,0:T(8,128)(2,1)S(1)}, bf16[64,1280]{1,0:T(8,128)(2,1)S(1)}, u32[]{:S(2)}, u32[]{:S(2)}) %collective-permute-start.7) | collective-permute-done | bytes 163872 | tf_op jit(solution)/shard_map/ppermute | solution.py:43
  57.2 4.1 %collective-permute-start.12 = (f32[32,512]{1,0:T(8,128)S(1)}, f32[32,512]{1,0:T(8,128)S(1)}, u32[]{:S(2)}, u32[]{:S(2)}) collective-permute-start(f32[32,512]{1,0:T(8,128)S(1)} %get-tuple-element.19.out), channel_id=1, source_target_pairs={{0,16},{8,24},{16,0},{24,8},{1,17},{9,25},{17,1},{25,9},{2,18},{10... | collective-permute-start | bytes 196616 | tf_op jit(solution)/shard_map/ppermute | solution.py:39
  62.4 1.9 %collective-permute-done.12.r2 = f32[32,512]{1,0:T(8,128)S(1)} collective-permute-done((f32[32,512]{1,0:T(8,128)S(1)}, f32[32,512]{1,0:T(8,128)S(1)}, u32[]{:S(2)}, u32[]{:S(2)}) %collective-permute-start.12) | collective-permute-done | bytes 65568 | tf_op jit(solution)/shard_map/ppermute | solution.py:39
  64.3 1.3 %collective-permute-done.13.r3 = f32[32,512]{1,0:T(8,128)S(1)} collective-permute-done((f32[32,512]{1,0:T(8,128)S(1)}, f32[32,512]{1,0:T(8,128)S(1)}, u32[]{:S(2)}, u32[]{:S(2)}) %collective-permute-start.13) | collective-permute-done | bytes 65568 | tf_op jit(solution)/shard_map/ppermute | solution.py:39
  66.0 11.8 %all_to_all.15.got = bf16[8,32,1024]{2,1,0:T(8,128)(2,1)S(1)} all-to-all(bf16[8,32,1024]{2,1,0:T(8,128)(2,1)S(1)} %get-tuple-element.21), channel_id=1, replica_groups=mesh['z'=8,'y'=4,'x'=4,'c'=2] {'x','c'}, dimensions={0} | all-to-all | bytes 1048576 | tf_op jit(solution)/shard_map/all_to_all | solution.py:317
  78.6 2.8 %collective-permute-start.15 = (f32[8,512]{1,0:T(8,128)S(1)}, f32[8,512]{1,0:T(8,128)S(1)}, u32[]{:S(2)}, u32[]{:S(2)}) collective-permute-start(f32[8,512]{1,0:T(8,128)S(1)} %get-tuple-element.25), channel_id=1, source_target_pairs={{0,16},{8,24},{16,0},{24,8},{1,17},{9,25},{17,1},{25,9},{2,18},{10... | collective-permute-start | bytes 49160 | tf_op jit(solution)/shard_map/ppermute | solution.py:39
  81.4 1.3 %collective-permute-start.16 = (f32[8,512]{1,0:T(8,128)S(1)}, f32[8,512]{1,0:T(8,128)S(1)}, u32[]{:S(2)}, u32[]{:S(2)}) collective-permute-start(f32[8,512]{1,0:T(8,128)S(1)} %get-tuple-element.26), channel_id=1, source_target_pairs={{0,24},{8,0},{16,8},{24,16},{1,25},{9,1},{17,9},{25,17},{2,26},{10... | collective-permute-start | bytes 49160 | tf_op jit(solution)/shard_map/ppermute | solution.py:39
  82.7 11.1 %collective-permute-start.17 = (f32[32,64]{1,0:T(8,128)S(1)}, f32[32,64]{1,0:T(8,128)S(1)}, u32[]{:S(2)}, u32[]{:S(2)}) collective-permute-start(f32[32,64]{1,0:T(8,128)S(1)} %get-tuple-element.30), channel_id=1, source_target_pairs={{0,0},{1,32},{2,64},{3,96},{4,128},{5,160},{6,192},{7,224},{8,8},{... | collective-permute-start | bytes 24584 | tf_op jit(solution)/shard_map/ppermute | solution.py:35
  93.8 1.9 %collective-permute-start.18 = (f32[32,64]{1,0:T(8,128)S(1)}, f32[32,64]{1,0:T(8,128)S(1)}, u32[]{:S(2)}, u32[]{:S(2)}) collective-permute-start(f32[32,64]{1,0:T(8,128)S(1)} %get-tuple-element.31), channel_id=1, source_target_pairs={{0,0},{1,32},{2,64},{3,96},{4,128},{5,160},{6,192},{7,224},{8,8},{... | collective-permute-start | bytes 24584 | tf_op jit(solution)/shard_map/ppermute | solution.py:35
  95.7 10.0 %collective-permute-done.18.u1 = f32[32,64]{1,0:T(8,128)S(1)} collective-permute-done((f32[32,64]{1,0:T(8,128)S(1)}, f32[32,64]{1,0:T(8,128)S(1)}, u32[]{:S(2)}, u32[]{:S(2)}) %collective-permute-start.18) | collective-permute-done | bytes 8224 | tf_op jit(solution)/shard_map/ppermute | solution.py:35
  (62 shorter events, 9.1 us)
Async XLA Ops:
  2.1 10.9 %copy-start.4 = (f32[2,4,16,64]{3,2,1,0:T(8,128)S(1)}, f32[2,4,16,64]{3,2,1,0:T(8,128)}, u32[]{:S(2)}) copy-start(f32[2,4,16,64]{3,2,1,0:T(8,128)} %r_im.1) | copy-start | bytes 98308
  2.1 10.9 %copy-start.6 = (f32[2,4,64]{2,1,0:T(4,128)S(1)}, f32[2,4,64]{2,1,0:T(4,128)}, u32[]{:S(2)}) copy-start(f32[2,4,64]{2,1,0:T(4,128)} %lam_re.1) | copy-start | bytes 6148
  2.1 29.7 %all-to-all-start = ((bf16[8,64,256]{2,1,0:T(8,128)(2,1)}), bf16[8,64,256]{2,1,0:T(8,128)(2,1)S(1)}, u32[]{:S(2)}, u32[]{:S(2)}) async-start(bf16[8,64,256]{2,1,0:T(8,128)(2,1)} %broadcast_in_dim.8), calls=%async_computation | async-start | bytes 524288 | tf_op jit(solution)/shard_map/all_to_all | solution.py:272
  10.9 12.5 %collective-permute-start.4 = (bf16[64,1280]{1,0:T(8,128)(2,1)S(1)}, bf16[64,1280]{1,0:T(8,128)(2,1)S(1)}, u32[]{:S(2)}, u32[]{:S(2)}) collective-permute-start(bf16[64,1280]{1,0:T(8,128)(2,1)S(1)} %fusion.refs_0_), channel_id=1, source_target_pairs={{0,32},{32,64},{64,96},{96,128},{128,160},{160,192},{192,224},{224... | collective-permute-start | bytes 491528 | tf_op jit(solution)/shard_map/ppermute | solution.py:43
  13.7 18.2 %copy-start.5 = (f32[2,256]{1,0:T(2,128)S(1)}, f32[2,256]{1,0:T(2,128)}, u32[]{:S(2)}) copy-start(f32[2,256]{1,0:T(2,128)} %gain.3) | copy-start | bytes 6148
  14.9 17.0 %collective-permute-start.3 = (f32[2,96,64]{2,1,0:T(8,128)S(1)}, f32[2,96,64]{2,1,0:T(8,128)S(1)}, u32[]{:S(2)}, u32[]{:S(2)}) collective-permute-start(f32[2,96,64]{2,1,0:T(8,128)S(1)} %get-tuple-element.17), channel_id=1, source_target_pairs={{0,0},{1,32},{2,64},{3,96},{4,128},{5,160},{6,192},{7,224},{8,8},{... | collective-permute-start | bytes 147464 | tf_op jit(solution)/shard_map/ppermute | solution.py:35
  21.2 16.6 %collective-permute-start.8 = (bf16[64,1280]{1,0:T(8,128)(2,1)S(1)}, bf16[64,1280]{1,0:T(8,128)(2,1)S(1)}, u32[]{:S(2)}, u32[]{:S(2)}) collective-permute-start(bf16[64,1280]{1,0:T(8,128)(2,1)S(1)} %fusion.refs_0_), channel_id=1, source_target_pairs={{0,224},{32,0},{64,32},{96,64},{128,96},{160,128},{192,160},{224,1... | collective-permute-start | bytes 491528 | tf_op jit(solution)/shard_map/ppermute | solution.py:43
  23.4 17.9 %collective-permute-start.5 = (bf16[64,1280]{1,0:T(8,128)(2,1)S(1)}, bf16[64,1280]{1,0:T(8,128)(2,1)S(1)}, u32[]{:S(2)}, u32[]{:S(2)}) collective-permute-start(bf16[64,1280]{1,0:T(8,128)(2,1)S(1)} %collective-permute-done.4.refs_1_), channel_id=1, source_target_pairs={{0,32},{32,64},{64,96},{96,128},{128,160},{160,192},{192,224},{224... | collective-permute-start | bytes 491528 | tf_op jit(solution)/shard_map/ppermute | solution.py:43
  23.4 4.8 %collective-permute-start = (bf16[8,256]{1,0:T(8,128)(2,1)S(1)}, bf16[8,256]{1,0:T(8,128)(2,1)S(1)}, u32[]{:S(2)}, u32[]{:S(2)}) collective-permute-start(bf16[8,256]{1,0:T(8,128)(2,1)S(1)} %copy-done.8), channel_id=1, source_target_pairs={{0,8},{8,16},{16,24},{24,0},{1,9},{9,17},{17,25},{25,1},{2,10},{10... | collective-permute-start | bytes 12296 | tf_op jit(solution)/shard_map/ppermute | solution.py:39
  25.0 5.1 %collective-permute-start.1 = (bf16[8,256]{1,0:T(8,128)(2,1)S(1)}, bf16[8,256]{1,0:T(8,128)(2,1)S(1)}, u32[]{:S(2)}, u32[]{:S(2)}) collective-permute-start(bf16[8,256]{1,0:T(8,128)(2,1)S(1)} %copy-done.8), channel_id=1, source_target_pairs={{0,16},{8,24},{16,0},{24,8},{1,17},{9,25},{17,1},{25,9},{2,18},{10... | collective-permute-start | bytes 12296 | tf_op jit(solution)/shard_map/ppermute | solution.py:39
  28.3 3.6 %collective-permute-start.2 = (bf16[8,256]{1,0:T(8,128)(2,1)S(1)}, bf16[8,256]{1,0:T(8,128)(2,1)S(1)}, u32[]{:S(2)}, u32[]{:S(2)}) collective-permute-start(bf16[8,256]{1,0:T(8,128)(2,1)S(1)} %copy-done.8), channel_id=1, source_target_pairs={{0,24},{8,0},{16,8},{24,16},{1,25},{9,1},{17,9},{25,17},{2,26},{10... | collective-permute-start | bytes 12296 | tf_op jit(solution)/shard_map/ppermute | solution.py:39
  33.0 23.2 %all-to-all-start.1 = ((bf16[8,32,1024]{2,1,0:T(8,128)(2,1)}), bf16[8,32,1024]{2,1,0:T(8,128)(2,1)S(1)}, u32[]{:S(2)}, u32[]{:S(2)}) async-start(bf16[8,32,1024]{2,1,0:T(8,128)(2,1)} %get-tuple-element.18), calls=%async_computation.1 | async-start | bytes 1048576 | tf_op jit(solution)/shard_map/all_to_all | solution.py:307
  37.8 7.3 %collective-permute-start.9 = (bf16[64,1280]{1,0:T(8,128)(2,1)S(1)}, bf16[64,1280]{1,0:T(8,128)(2,1)S(1)}, u32[]{:S(2)}, u32[]{:S(2)}) collective-permute-start(bf16[64,1280]{1,0:T(8,128)(2,1)S(1)} %collective-permute-done.8.refs_7_), channel_id=1, source_target_pairs={{0,224},{32,0},{64,32},{96,64},{128,96},{160,128},{192,160},{224,1... | collective-permute-start | bytes 491528 | tf_op jit(solution)/shard_map/ppermute | solution.py:43
  41.3 8.3 %collective-permute-start.6 = (bf16[64,1280]{1,0:T(8,128)(2,1)S(1)}, bf16[64,1280]{1,0:T(8,128)(2,1)S(1)}, u32[]{:S(2)}, u32[]{:S(2)}) collective-permute-start(bf16[64,1280]{1,0:T(8,128)(2,1)S(1)} %collective-permute-done.5.refs_2_), channel_id=1, source_target_pairs={{0,32},{32,64},{64,96},{96,128},{128,160},{160,192},{192,224},{224... | collective-permute-start | bytes 491528 | tf_op jit(solution)/shard_map/ppermute | solution.py:43
  45.0 7.0 %collective-permute-start.10 = (bf16[64,1280]{1,0:T(8,128)(2,1)S(1)}, bf16[64,1280]{1,0:T(8,128)(2,1)S(1)}, u32[]{:S(2)}, u32[]{:S(2)}) collective-permute-start(bf16[64,1280]{1,0:T(8,128)(2,1)S(1)} %collective-permute-done.9.refs_6_), channel_id=1, source_target_pairs={{0,224},{32,0},{64,32},{96,64},{128,96},{160,128},{192,160},{224,1... | collective-permute-start | bytes 491528 | tf_op jit(solution)/shard_map/ppermute | solution.py:43
  49.6 6.6 %collective-permute-start.7 = (bf16[64,1280]{1,0:T(8,128)(2,1)S(1)}, bf16[64,1280]{1,0:T(8,128)(2,1)S(1)}, u32[]{:S(2)}, u32[]{:S(2)}) collective-permute-start(bf16[64,1280]{1,0:T(8,128)(2,1)S(1)} %collective-permute-done.6.refs_3_), channel_id=1, source_target_pairs={{0,32},{32,64},{64,96},{96,128},{128,160},{160,192},{192,224},{224... | collective-permute-start | bytes 491528 | tf_op jit(solution)/shard_map/ppermute | solution.py:43
  56.9 5.6 %collective-permute-start.11 = (f32[32,512]{1,0:T(8,128)S(1)}, f32[32,512]{1,0:T(8,128)S(1)}, u32[]{:S(2)}, u32[]{:S(2)}) collective-permute-start(f32[32,512]{1,0:T(8,128)S(1)} %get-tuple-element.19.out), channel_id=1, source_target_pairs={{0,8},{8,16},{16,24},{24,0},{1,9},{9,17},{17,25},{25,1},{2,10},{10... | collective-permute-start | bytes 196616 | tf_op jit(solution)/shard_map/ppermute | solution.py:39
  57.2 7.1 %collective-permute-start.12 = (f32[32,512]{1,0:T(8,128)S(1)}, f32[32,512]{1,0:T(8,128)S(1)}, u32[]{:S(2)}, u32[]{:S(2)}) collective-permute-start(f32[32,512]{1,0:T(8,128)S(1)} %get-tuple-element.19.out), channel_id=1, source_target_pairs={{0,16},{8,24},{16,0},{24,8},{1,17},{9,25},{17,1},{25,9},{2,18},{10... | collective-permute-start | bytes 196616 | tf_op jit(solution)/shard_map/ppermute | solution.py:39
  61.4 4.3 %collective-permute-start.13 = (f32[32,512]{1,0:T(8,128)S(1)}, f32[32,512]{1,0:T(8,128)S(1)}, u32[]{:S(2)}, u32[]{:S(2)}) collective-permute-start(f32[32,512]{1,0:T(8,128)S(1)} %get-tuple-element.19.out), channel_id=1, source_target_pairs={{0,24},{8,0},{16,8},{24,16},{1,25},{9,1},{17,9},{25,17},{2,26},{10... | collective-permute-start | bytes 196616 | tf_op jit(solution)/shard_map/ppermute | solution.py:39
  78.5 28.2 %collective-permute-start.14 = (f32[8,512]{1,0:T(8,128)S(1)}, f32[8,512]{1,0:T(8,128)S(1)}, u32[]{:S(2)}, u32[]{:S(2)}) collective-permute-start(f32[8,512]{1,0:T(8,128)S(1)} %get-tuple-element.24), channel_id=1, source_target_pairs={{0,8},{8,16},{16,24},{24,0},{1,9},{9,17},{17,25},{25,1},{2,10},{10... | collective-permute-start | bytes 49160 | tf_op jit(solution)/shard_map/ppermute | solution.py:39
  78.6 28.2 %collective-permute-start.15 = (f32[8,512]{1,0:T(8,128)S(1)}, f32[8,512]{1,0:T(8,128)S(1)}, u32[]{:S(2)}, u32[]{:S(2)}) collective-permute-start(f32[8,512]{1,0:T(8,128)S(1)} %get-tuple-element.25), channel_id=1, source_target_pairs={{0,16},{8,24},{16,0},{24,8},{1,17},{9,25},{17,1},{25,9},{2,18},{10... | collective-permute-start | bytes 49160 | tf_op jit(solution)/shard_map/ppermute | solution.py:39
  81.4 25.4 %collective-permute-start.16 = (f32[8,512]{1,0:T(8,128)S(1)}, f32[8,512]{1,0:T(8,128)S(1)}, u32[]{:S(2)}, u32[]{:S(2)}) collective-permute-start(f32[8,512]{1,0:T(8,128)S(1)} %get-tuple-element.26), channel_id=1, source_target_pairs={{0,24},{8,0},{16,8},{24,16},{1,25},{9,1},{17,9},{25,17},{2,26},{10... | collective-permute-start | bytes 49160 | tf_op jit(solution)/shard_map/ppermute | solution.py:39
  82.7 13.0 %collective-permute-start.17 = (f32[32,64]{1,0:T(8,128)S(1)}, f32[32,64]{1,0:T(8,128)S(1)}, u32[]{:S(2)}, u32[]{:S(2)}) collective-permute-start(f32[32,64]{1,0:T(8,128)S(1)} %get-tuple-element.30), channel_id=1, source_target_pairs={{0,0},{1,32},{2,64},{3,96},{4,128},{5,160},{6,192},{7,224},{8,8},{... | collective-permute-start | bytes 24584 | tf_op jit(solution)/shard_map/ppermute | solution.py:35
  93.8 11.9 %collective-permute-start.18 = (f32[32,64]{1,0:T(8,128)S(1)}, f32[32,64]{1,0:T(8,128)S(1)}, u32[]{:S(2)}, u32[]{:S(2)}) collective-permute-start(f32[32,64]{1,0:T(8,128)S(1)} %get-tuple-element.31), channel_id=1, source_target_pairs={{0,0},{1,32},{2,64},{3,96},{4,128},{5,160},{6,192},{7,224},{8,8},{... | collective-permute-start | bytes 24584 | tf_op jit(solution)/shard_map/ppermute | solution.py:35
  (11 other events, 58.4 us)
where the time goes:
time: 108 us; the launch traced here: 107 us
  starting transfers between devices  57.7 us (53%)
  waiting for transfers between devices  29.2 us (27%)
  blocking collectives  11.8 us (11%)
  Pallas kernels  5.62 us (5%)
  local copies, waits for them, and re-layouts  2.18 us (2%)
    ppermute x3, starting transfers between devices, turn(): return lax.ppermute(value, ALL, pairs)  19.3 us
    ppermute x9, starting transfers between devices, shift_y(): return lax.ppermute(value, 'y', [(i, (i + k) % NY) for i in range(NY)])  15.1 us
    ppermute x7, waiting for transfers between devices, shift_z(): return lax.ppermute(value, 'z', [(i, (i + k) % NZ) for i in range(NZ)])  12.9 us
    all_to_all x1, blocking collectives, both_layers(): got = lax.all_to_all(payload, DP, 0, 0, tiled=True)  11.8 us
    ppermute x3, waiting for transfers between devices, turn(): return lax.ppermute(value, ALL, pairs)  10 us
    ppermute x7, starting transfers between devices, shift_z(): return lax.ppermute(value, 'z', [(i, (i + k) % NZ) for i in range(NZ)])  9.83 us
    all_to_all x1, starting transfers between devices, both_layers(): lax.all_to_all(jnp.broadcast_to(w_turned[0][None], (NZ, BLOCK, COLS)), 'z...  8.61 us
    ppermute x9, waiting for transfers between devices, shift_y(): return lax.ppermute(value, 'y', [(i, (i + k) % NY) for i in range(NY)])  6.28 us
  transfers between devices with their start and end apart: 21, of which 12 were waited for; matrix products, arithmetic and copies ran while one was open for 0% of the time, Pallas kernels for 3%

commit v1 on v0

--- a/solution.py
+++ b/solution.py
@@ -18,7 +18,6 @@
 COLS = 256
 BLOCK = 64
 WIDTH = NZ * BLOCK
-PAY = 1024
 
 eps = 1e-06
 HIGHEST = lax.Precision.HIGHEST
@@ -26,12 +25,23 @@
 bf16 = jnp.bfloat16
 
 
-def turn(value):
+STEP_X = (2, 3, 1, 0, 0, 1, 3, 2)
+STEP_C = (1, 1, 1, 1, 0, 0, 0, 0)
+
+
+def place(z, delta):
+    return lax.rem(lax.div(z, 2) + STEP_X[delta], NX) * NC + STEP_C[delta]
+
+
+def turn(value, back=False):
     pairs = []
     for z in range(NZ):
         for y in range(NY):
-            for d in range(ND):
-                pairs.append(((z * NY + y) * ND + d, (d * NY + y) * ND + z))
+            for delta in range(NZ):
+                owner = ((z + delta) % NZ * NY + y) * ND + z
+                d = (z // 2 + STEP_X[delta]) % NX * NC + STEP_C[delta]
+                user = (z * NY + y) * ND + d
+                pairs.append((user, owner) if back else (owner, user))
     return lax.ppermute(value, ALL, pairs)
 
 
@@ -60,7 +70,30 @@
     return high, low
 
 
-def prep_kernel(lam_re, lam_im, log_dt, b_re, b_im, r_re, r_im, d_skip, state, base, drive, carried):
+def pack_kernel(w_in, w_val, w_gate, out):
+    row = jnp.concatenate([w_in[0], w_val[0], w_gate[0]], axis=1)
+    for i in range(NZ):
+        out[i] = row
+
+
+def prep_kernel(
+    lam_re,
+    lam_im,
+    log_dt,
+    b_re,
+    b_im,
+    r_re,
+    r_im,
+    d_skip,
+    state,
+    w_in,
+    w_val,
+    w_gate,
+    base,
+    drive,
+    carried,
+    late,
+):
     groups, chans, half = b_re.shape[1:]
     size = groups * chans
     row = lax.broadcasted_iota(jnp.int32, (size, size), 0)
@@ -97,23 +130,25 @@
         full = times_turned(dcat, jnp.concatenate(reads), HIGHEST)
         mix = jnp.where(row // chans == col // chans, full, 0.0)
         mix = mix + jnp.where(row == col, d_skip[n : n + 1, :], 0.0)
-        carried[n, :SEQS, :] = jnp.concatenate(offsets, axis=1)
-        carried[n, SEQS:, :] = mix
-
-
-def write_payload(pay_ref, x, carried, blocks):
+        carried[n * SEQS : (n + 1) * SEQS, :] = jnp.concatenate(offsets, axis=1)
+        if n == 0:
+            carried[LAYERS * SEQS :, :] = mix
+        else:
+            late[...] = jnp.concatenate([w_val[n], w_gate[n], w_in[n], *two_halves(mix)], axis=1)
+
+
+def write_payload(pay_ref, x, blocks, offset, mix=None):
     squares = jnp.sum(x * x, axis=1, keepdims=True)
     s_high, s_low = two_halves(squares)
     lane = lax.broadcasted_iota(jnp.int32, (SEQS, 128), 1)
     s_part = jnp.where(lane == 0, s_high.astype(f32), jnp.where(lane == 1, s_low.astype(f32), 0.0))
-    o_high, o_low = two_halves(carried[:SEQS])
-    m_high, m_low = two_halves(carried[SEQS:])
-    half = BLOCK // 2
-    row = jnp.concatenate(
-        [blocks[j].astype(bf16) for j in range(NZ)]
-        + [o_high, o_low, s_part.astype(bf16), m_high[:half], m_high[half:], m_low[:half], m_low[half:]],
-        axis=1,
-    )
+    parts = [blocks[j].astype(bf16) for j in range(NZ)]
+    parts += [*two_halves(offset), s_part.astype(bf16)]
+    if mix is not None:
+        half = BLOCK // 2
+        for m in two_halves(mix):
+            parts += [m[:half], m[half:]]
+    row = jnp.concatenate(parts, axis=1)
     for i in range(ND):
         pay_ref[i] = row
 
@@ -124,15 +159,15 @@
     )
 
 
-def first_kernel(p0, p1, p2, p3, gain, carried, w, pay_ref, x_ref, rows):
+def first_kernel(p0, p1, p2, p3, gain, carried, w, up, down, pay_ref, x_ref, rows):
     y = lax.axis_index("y")
     for k, piece in enumerate((p0, p1, p2, p3)):
         rows[lax.rem(y + NY - k, NY)] = piece[...].astype(f32)
     x = rows[...].reshape(SEQS, COLS)
     x_ref[...] = x
     normed = (x * gain[0:1]).astype(bf16)
-    blocks = [times_turned(normed, w[j]) for j in range(NZ)]
-    write_payload(pay_ref, x, carried[0], blocks)
+    blocks = [times_turned(normed, w[j, :, :COLS]) for j in range(NZ)]
+    write_payload(pay_ref, x, blocks, carried[:SEQS], carried[LAYERS * SEQS :])
 
 
 def next_kernel(out, r1, r2, r3, x_old, gain, carried, *refs):
@@ -145,8 +180,8 @@
     x_ref[...] = x
     normed = (x * gain[1:2]).astype(bf16)
     for k in range(NZ):
-        blocks[lax.rem(z + NZ - k, NZ)] = times_turned(normed, w[k][:, 4 * COLS :])
-    write_payload(pay_ref, x, carried[1], blocks)
+        blocks[lax.rem(z + NZ - k, NZ)] = times_turned(normed, w[k][:, 2 * COLS : 3 * COLS])
+    write_payload(pay_ref, x, blocks, carried[SEQS : LAYERS * SEQS])
 
 
 def inputs_of(got):
@@ -158,54 +193,63 @@
     return total * lax.rsqrt(jnp.sum(squares, axis=1, keepdims=True) / D + eps)
 
 
-def gated(got, u, w, first_col, mixed, ordered, weights):
+def gated(got, u_blocks, w, ordered, weights):
     z = lax.axis_index("z")
-    for j in range(NZ):
-        offset = got[j, :, WIDTH : WIDTH + BLOCK].astype(f32) + got[
-            j, :, WIDTH + BLOCK : WIDTH + 2 * BLOCK
-        ].astype(f32)
-        high, low = two_halves(u[:, j * BLOCK : (j + 1) * BLOCK])
-        m = got[j, :, WIDTH + 256 :]
-        m_high = jnp.concatenate([m[:, :BLOCK], m[:, BLOCK : 2 * BLOCK]], axis=0)
-        m_low = jnp.concatenate([m[:, 2 * BLOCK : 3 * BLOCK], m[:, 3 * BLOCK :]], axis=0)
+    for delta in range(NZ):
+        block, slot, source = lax.rem(z + delta, NZ), (NZ - delta) % NZ, place(z, delta)
+        sent = got[source]
+        offset = sent[:, WIDTH : WIDTH + BLOCK].astype(f32)
+        offset = offset + sent[:, WIDTH + BLOCK : WIDTH + 2 * BLOCK].astype(f32)
+        cut = slice(slot * BLOCK, (slot + 1) * BLOCK)
+        if isinstance(w, list):
+            m_high = w[slot][:, 3 * COLS : 3 * COLS + BLOCK]
+            m_low = w[slot][:, 3 * COLS + BLOCK :]
+            weights[cut, :] = w[slot][:, : 2 * COLS]
+        else:
+            m = sent[:, WIDTH + 256 :]
+            m_high = jnp.concatenate([m[:, :BLOCK], m[:, BLOCK : 2 * BLOCK]], axis=0)
+            m_low = jnp.concatenate([m[:, 2 * BLOCK : 3 * BLOCK], m[:, 3 * BLOCK :]], axis=0)
+            weights[cut, :] = w[block][:, COLS:]
+        high, low = two_halves(u_blocks[block])
         pre = (
             offset
             + jnp.dot(high, m_low, preferred_element_type=f32)
             + jnp.dot(low, m_high, preferred_element_type=f32)
             + jnp.dot(high, m_high, preferred_element_type=f32)
         )
-        mixed[j] = jax.nn.gelu(pre)
-    for k in range(NZ):
-        ordered[:, k * BLOCK : (k + 1) * BLOCK] = mixed[lax.rem(z + NZ - k, NZ)].astype(bf16)
-        weights[k * BLOCK : (k + 1) * BLOCK, :] = w[k][:, first_col : first_col + 2 * COLS]
+        ordered[:, cut] = jax.nn.gelu(pre).astype(bf16)
     return jnp.dot(ordered[...], weights[...], preferred_element_type=f32)
 
 
-def own_block(u, u_blocks):
+def own_block(u_blocks):
+    z = lax.axis_index("z")
     d = lax.axis_index("x") * NC + lax.axis_index("c")
+    delta = jnp.int32(0)
+    for other in range(1, NZ):
+        delta = jnp.where(place(z, other) == d, other, delta)
+    return u_blocks[lax.rem(z + delta, NZ)]
+
+
+def split_blocks(u, u_blocks):
     for j in range(NZ):
         u_blocks[j] = u[:, j * BLOCK : (j + 1) * BLOCK]
-    return u_blocks[d]
-
-
-def mid_kernel(got, *refs):
-    w = refs[:NZ]
-    out, own_u, u_blocks, mixed, ordered, weights = refs[NZ:]
-    u = inputs_of(got)
-    own_u[...] = own_block(u, u_blocks)
-    out[...] = gated(got, u, w, 0, mixed, ordered, weights)
-
-
-def inputs_kernel(got, u_ref, own_u, u_blocks):
-    u = inputs_of(got)
-    u_ref[...] = u
-    own_u[...] = own_block(u, u_blocks)
-
-
-def last_kernel(got, u, *refs):
-    w = refs[:NZ]
-    own_out, s1, s2, s3, mixed, ordered, weights, by_y = refs[NZ:]
-    out = gated(got, u[...], w, 2 * COLS, mixed, ordered, weights)
+
+
+def mid_kernel(got, w, out, own_u, u_blocks, ordered, weights):
+    split_blocks(inputs_of(got), u_blocks)
+    own_u[...] = own_block(u_blocks)
+    out[...] = gated(got, u_blocks, w, ordered, weights)
+
+
+def inputs_kernel(got, earlier, u_blocks, own_u):
+    split_blocks(inputs_of(got), u_blocks)
+    own_u[...] = own_block(u_blocks)
+
+
+def last_kernel(got, u_blocks, *refs):
+    w = list(refs[:NZ])
+    own_out, s1, s2, s3, ordered, weights, by_y = refs[NZ:]
+    out = gated(got, u_blocks, w, ordered, weights)
     y = lax.axis_index("y")
     by_y[...] = out.reshape(NY, ROWS, 2 * COLS)
     own_out[...] = by_y[y]
@@ -247,9 +291,10 @@
     return jax.ShapeDtypeStruct(dims, dtype)
 
 
-PAY_OUTS = [shape((ND, SEQS, PAY), bf16), shape((SEQS, COLS))]
+FIRST_PAY = WIDTH + 512
+NEXT_PAY = WIDTH + 256
 BLOCKS = pltpu.VMEM((NZ, SEQS, BLOCK), f32)
-GATED = [BLOCKS, pltpu.VMEM((SEQS, WIDTH), bf16), pltpu.VMEM((WIDTH, 2 * COLS), bf16)]
+GATED = [pltpu.VMEM((SEQS, WIDTH), bf16), pltpu.VMEM((WIDTH, 2 * COLS), bf16)]
 
 
 def both_layers(
@@ -269,14 +314,10 @@
     state,
 ):
     w_turned = jnp.swapaxes(w_input, 1, 2)
-    first_w = lax.all_to_all(
-        jnp.broadcast_to(w_turned[0][None], (NZ, BLOCK, COLS)), "z", 0, 0, tiled=True
-    )
+    (packed,) = call(pack_kernel, [w_turned, w_val, w_gate], [shape((NZ, BLOCK, 3 * COLS), bf16)])
+    first_w = lax.all_to_all(packed, "z", 0, 0, tiled=True)
     pieces = [stream] + [shift_y(stream, k) for k in range(1, NY)]
-    late = jnp.concatenate([w_val[0], w_gate[0], w_val[1], w_gate[1], w_turned[1]], axis=1)
-    ring = ring_z(late)
-
-    base, drive, own = call(
+    base, drive, own, late = call(
         prep_kernel,
         [
             lam_re,
@@ -288,37 +329,47 @@
             readout_imaginary,
             d_skip,
             state,
+            w_turned,
+            w_val,
+            w_gate,
         ],
         [
             shape(state.shape),
             shape((LAYERS, BLOCK, state.shape[-1])),
-            shape((LAYERS, SEQS + BLOCK, BLOCK)),
+            shape((LAYERS * SEQS + BLOCK, BLOCK)),
+            shape((BLOCK, 3 * COLS + 2 * BLOCK), bf16),
         ],
         scalar=2,
     )
     carried = turn(own)
+    ring = ring_z(late)
 
     payload, x = call(
         first_kernel,
-        [*pieces, norm_gain, carried, first_w],
-        PAY_OUTS,
+        [*pieces, norm_gain, carried, first_w, ring[1], ring[-1]],
+        [shape((ND, SEQS, FIRST_PAY), bf16), shape((SEQS, COLS))],
         [pltpu.VMEM((NY, ROWS, COLS), f32)],
     )
     got = lax.all_to_all(payload, DP, 0, 0, tiled=True)
     out, u0 = call(
         mid_kernel,
-        [got, *ring],
+        [got, first_w],
         [shape((SEQS, 2 * COLS)), shape((SEQS, BLOCK))],
         [BLOCKS, *GATED],
     )
     others = [shift_y(out, k) for k in range(1, NY)]
-    u0 = turn(u0)
-    payload, x = call(next_kernel, [out, *others, x, norm_gain, carried, *ring], PAY_OUTS, [BLOCKS])
+    u0 = turn(u0, back=True)
+    payload, x = call(
+        next_kernel,
+        [out, *others, x, norm_gain, carried, *ring],
+        [shape((ND, SEQS, NEXT_PAY), bf16), shape((SEQS, COLS))],
+        [BLOCKS],
+    )
     got = lax.all_to_all(payload, DP, 0, 0, tiled=True)
     u, u1 = call(
-        inputs_kernel, [got], [shape((SEQS, WIDTH)), shape((SEQS, BLOCK))], [BLOCKS]
-    )
-    u1 = turn(u1)
+        inputs_kernel, [got, u0], [shape((NZ, SEQS, BLOCK)), shape((SEQS, BLOCK))]
+    )
+    u1 = turn(u1, back=True)
     own, s1, s2, s3 = call(
         last_kernel,
         [got, u, *ring],

time: 108 us -> 100 us (0.926)
  the two profiles are of different devices: /device:TPU:4 before, /device:TPU:110 now
where the time goes in v1:
time: 100 us; the launch traced here: 99.8 us
  starting transfers between devices  51.6 us (52%)
  waiting for transfers between devices  36.9 us (37%)
  Pallas kernels  7.3 us (7%)
  local copies, waits for them, and re-layouts  3.16 us (3%)
    ppermute x3, waiting for transfers between devices, turn(): return lax.ppermute(value, ALL, pairs)  26.1 us
    ppermute x7, starting transfers between devices, shift_z(): return lax.ppermute(value, 'z', [(i, (i + k) % NZ) for i in range(NZ)])  15.2 us
    ppermute x9, starting transfers between devices, shift_y(): return lax.ppermute(value, 'y', [(i, (i + k) % NY) for i in range(NY)])  14.9 us
    all_to_all x2, starting transfers between devices, both_layers(): got = lax.all_to_all(payload, DP, 0, 0, tiled=True)  11.7 us
    all_to_all x1, starting transfers between devices, both_layers(): first_w = lax.all_to_all(packed, 'z', 0, 0, tiled=True)  7.8 us
    pallas_call x9, Pallas kernels, call(): pl.pallas_call(body, in_specs=[pl.BlockSpec(memory_space=s) for s in spac...  7.3 us
    ppermute x9, waiting for transfers between devices, shift_y(): return lax.ppermute(value, 'y', [(i, (i + k) % NY) for i in range(NY)])  5.59 us
    ppermute x7, waiting for transfers between devices, shift_z(): return lax.ppermute(value, 'z', [(i, (i + k) % NZ) for i in range(NZ)])  5.14 us
  transfers between devices with their start and end apart: 22, of which 10 were waited for; matrix products, arithmetic and copies ran while one was open for 0% of the time, Pallas kernels for 3%

profile of v1, /device:TPU:110, one launch (start us, length us, event | category | flops | bytes accessed | tf_op | source)
XLA Modules:
  0.0 99.8 jit_solution(6773558259301775521)
XLA Ops:
  4.2 7.8 %all-to-all-start = ((bf16[8,64,768]{2,1,0:T(8,128)(2,1)}), bf16[8,64,768]{2,1,0:T(8,128)(2,1)S(1)}, u32[]{:S(2)}, u32[]{:S(2)}) async-start(bf16[8,64,768]{2,1,0:T(8,128)(2,1)} %shard_map.150), calls=%async_computation | async-start | bytes 1572864 | tf_op jit(solution)/shard_map/all_to_all | solution.py:318
  12.7 1.2 %shard_map.149 = (f32[2,32,4,128]{3,2,1,0:T(4,128)S(1)}, f32[2,64,128]{2,1,0:T(8,128)S(1)}, f32[128,64]{1,0:T(8,128)S(1)}, bf16[64,896]{1,0:T(8,128)(2,1)S(1)}) custom-call(f32[2,4,64]{2,1,0:T(4,128)S(1)} %copy-done.12, f32[2,4,64]{2,1,0:T(4,128)S(1)} %copy-done.13, f32[2,4]{1,0:T(2,128)S(1)} %copy-done.15, f32[2,4,16,64]{3,2,1,0:T(8,128)S(1)} %bitcast.5, ...), custom_call_target="tpu_custom_call" | custom-call | flops 16777216 | bytes 1048576 | tf_op jit(solution)/shard_map/pallas_call | solution.py:279
  13.9 2.8 %collective-permute-start.4 = (bf16[64,896]{1,0:T(8,128)(2,1)S(1)}, bf16[64,896]{1,0:T(8,128)(2,1)S(1)}, u32[]{:S(2)}, u32[]{:S(2)}) collective-permute-start(bf16[64,896]{1,0:T(8,128)(2,1)S(1)} %get-tuple-element.19.refs_0_), channel_id=1, source_target_pairs={{0,32},{32,64},{64,96},{96,128},{128,160},{160,192},{192,224},{224... | collective-permute-start | bytes 344072 | tf_op jit(solution)/shard_map/ppermute | solution.py:53
  16.7 1.9 %collective-permute-start.3 = (f32[128,64]{1,0:T(8,128)S(1)}, f32[128,64]{1,0:T(8,128)S(1)}, u32[]{:S(2)}, u32[]{:S(2)}) collective-permute-start(f32[128,64]{1,0:T(8,128)S(1)} %get-tuple-element.18), channel_id=1, source_target_pairs={{0,5},{32,7},{64,3},{96,1},{128,0},{160,2},{192,6},{224,4},{8,13},... | collective-permute-start | bytes 98312 | tf_op jit(solution)/shard_map/ppermute | solution.py:45
  18.6 1.6 %collective-permute-start = (bf16[8,256]{1,0:T(8,128)(2,1)S(1)}, bf16[8,256]{1,0:T(8,128)(2,1)S(1)}, u32[]{:S(2)}, u32[]{:S(2)}) collective-permute-start(bf16[8,256]{1,0:T(8,128)(2,1)S(1)} %copy-done.14), channel_id=1, source_target_pairs={{0,8},{8,16},{16,24},{24,0},{1,9},{9,17},{17,25},{25,1},{2,10},{10... | collective-permute-start | bytes 12296 | tf_op jit(solution)/shard_map/ppermute | solution.py:49
  22.2 1.7 %collective-permute-start.2 = (bf16[8,256]{1,0:T(8,128)(2,1)S(1)}, bf16[8,256]{1,0:T(8,128)(2,1)S(1)}, u32[]{:S(2)}, u32[]{:S(2)}) collective-permute-start(bf16[8,256]{1,0:T(8,128)(2,1)S(1)} %copy-done.14), channel_id=1, source_target_pairs={{0,24},{8,0},{16,8},{24,16},{1,25},{9,1},{17,9},{25,17},{2,26},{10... | collective-permute-start | bytes 12296 | tf_op jit(solution)/shard_map/ppermute | solution.py:49
  23.9 1.4 %collective-permute-done.1.p2 = bf16[8,256]{1,0:T(8,128)(2,1)S(1)} collective-permute-done((bf16[8,256]{1,0:T(8,128)(2,1)S(1)}, bf16[8,256]{1,0:T(8,128)(2,1)S(1)}, u32[]{:S(2)}, u32[]{:S(2)}) %collective-permute-start.1) | collective-permute-done | bytes 4128 | tf_op jit(solution)/shard_map/ppermute | solution.py:49
  25.8 8.4 %collective-permute-done.3.carried = f32[128,64]{1,0:T(8,128)S(1)} collective-permute-done((f32[128,64]{1,0:T(8,128)S(1)}, f32[128,64]{1,0:T(8,128)S(1)}, u32[]{:S(2)}, u32[]{:S(2)}) %collective-permute-start.3) | collective-permute-done | bytes 32800 | tf_op jit(solution)/shard_map/ppermute | solution.py:45
  34.3 1.1 %shard_map.151 = (bf16[8,32,1024]{2,1,0:T(8,128)(2,1)}, f32[32,256]{1,0:T(8,128)S(1)}) custom-call(bf16[8,256]{1,0:T(8,128)(2,1)S(1)} %copy-done.14, bf16[8,256]{1,0:T(8,128)(2,1)S(1)} %collective-permute-done.p1, bf16[8,256]{1,0:T(8,128)(2,1)S(1)} %collective-permute-done.1.p2, bf16[8,256]{1,0:T(8,128)(2,1)S(1)} %collective-permute-done.2.p3, ...), custom_call_target="tpu_custom_call" | custom-call | flops 16777216 | bytes 1048576 | tf_op jit(solution)/shard_map/pallas_call | solution.py:279
  35.4 6.8 %all-to-all-start.1 = ((bf16[8,32,1024]{2,1,0:T(8,128)(2,1)}), bf16[8,32,1024]{2,1,0:T(8,128)(2,1)S(1)}, u32[]{:S(2)}, u32[]{:S(2)}) async-start(bf16[8,32,1024]{2,1,0:T(8,128)(2,1)} %get-tuple-element.20), calls=%async_computation.1 | async-start | bytes 1048576 | tf_op jit(solution)/shard_map/all_to_all | solution.py:353
  42.2 5.1 %collective-permute-start.9 = (bf16[64,896]{1,0:T(8,128)(2,1)S(1)}, bf16[64,896]{1,0:T(8,128)(2,1)S(1)}, u32[]{:S(2)}, u32[]{:S(2)}) collective-permute-start(bf16[64,896]{1,0:T(8,128)(2,1)S(1)} %collective-permute-done.4.up.refs_1_), channel_id=1, source_target_pairs={{0,32},{32,64},{64,96},{96,128},{128,160},{160,192},{192,224},{224... | collective-permute-start | bytes 344072 | tf_op jit(solution)/shard_map/ppermute | solution.py:53
  47.3 2.7 %collective-permute-done.9.refs_2_ = bf16[64,896]{1,0:T(8,128)(2,1)S(1)} collective-permute-done((bf16[64,896]{1,0:T(8,128)(2,1)S(1)}, bf16[64,896]{1,0:T(8,128)(2,1)S(1)}, u32[]{:S(2)}, u32[]{:S(2)}) %collective-permute-start.9) | collective-permute-done | bytes 114720 | tf_op jit(solution)/shard_map/ppermute | solution.py:53
  50.0 3.7 %collective-permute-start.10 = (bf16[64,896]{1,0:T(8,128)(2,1)S(1)}, bf16[64,896]{1,0:T(8,128)(2,1)S(1)}, u32[]{:S(2)}, u32[]{:S(2)}) collective-permute-start(bf16[64,896]{1,0:T(8,128)(2,1)S(1)} %collective-permute-done.9.refs_2_), channel_id=1, source_target_pairs={{0,32},{32,64},{64,96},{96,128},{128,160},{160,192},{192,224},{224... | collective-permute-start | bytes 344072 | tf_op jit(solution)/shard_map/ppermute | solution.py:53
  53.7 2.4 %collective-permute-done.10.refs_3_ = bf16[64,896]{1,0:T(8,128)(2,1)S(1)} collective-permute-done((bf16[64,896]{1,0:T(8,128)(2,1)S(1)}, bf16[64,896]{1,0:T(8,128)(2,1)S(1)}, u32[]{:S(2)}, u32[]{:S(2)}) %collective-permute-start.10) | collective-permute-done | bytes 114720 | tf_op jit(solution)/shard_map/ppermute | solution.py:53
  56.0 3.6 %collective-permute-start.11 = (bf16[64,896]{1,0:T(8,128)(2,1)S(1)}, bf16[64,896]{1,0:T(8,128)(2,1)S(1)}, u32[]{:S(2)}, u32[]{:S(2)}) collective-permute-start(bf16[64,896]{1,0:T(8,128)(2,1)S(1)} %collective-permute-done.10.refs_3_), channel_id=1, source_target_pairs={{0,32},{32,64},{64,96},{96,128},{128,160},{160,192},{192,224},{224... | collective-permute-start | bytes 344072 | tf_op jit(solution)/shard_map/ppermute | solution.py:53
  60.3 1.6 %collective-permute-start.6 = (f32[32,512]{1,0:T(8,128)S(1)}, f32[32,512]{1,0:T(8,128)S(1)}, u32[]{:S(2)}, u32[]{:S(2)}) collective-permute-start(f32[32,512]{1,0:T(8,128)S(1)} %get-tuple-element.21.out), channel_id=1, source_target_pairs={{0,8},{8,16},{16,24},{24,0},{1,9},{9,17},{17,25},{25,1},{2,10},{10... | collective-permute-start | bytes 196616 | tf_op jit(solution)/shard_map/ppermute | solution.py:49
  62.9 2.4 %collective-permute-start.8 = (f32[32,512]{1,0:T(8,128)S(1)}, f32[32,512]{1,0:T(8,128)S(1)}, u32[]{:S(2)}, u32[]{:S(2)}) collective-permute-start(f32[32,512]{1,0:T(8,128)S(1)} %get-tuple-element.21.out), channel_id=1, source_target_pairs={{0,24},{8,0},{16,8},{24,16},{1,25},{9,1},{17,9},{25,17},{2,26},{10... | collective-permute-start | bytes 196616 | tf_op jit(solution)/shard_map/ppermute | solution.py:49
  65.3 2.5 %collective-permute-done.7.r2 = f32[32,512]{1,0:T(8,128)S(1)} collective-permute-done((f32[32,512]{1,0:T(8,128)S(1)}, f32[32,512]{1,0:T(8,128)S(1)}, u32[]{:S(2)}, u32[]{:S(2)}) %collective-permute-start.7) | collective-permute-done | bytes 65568 | tf_op jit(solution)/shard_map/ppermute | solution.py:49
  68.9 5.0 %all-to-all-start.2 = ((bf16[8,32,768]{2,1,0:T(8,128)(2,1)}), bf16[8,32,768]{2,1,0:T(8,128)(2,1)S(1)}, u32[]{:S(2)}, u32[]{:S(2)}) async-start(bf16[8,32,768]{2,1,0:T(8,128)(2,1)} %get-tuple-element.23), calls=%async_computation.2 | async-start | bytes 786432 | tf_op jit(solution)/shard_map/all_to_all | solution.py:368
  73.9 8.9 %collective-permute-done.14.earlier.u0 = f32[32,64]{1,0:T(8,128)S(1)} collective-permute-done((f32[32,64]{1,0:T(8,128)S(1)}, f32[32,64]{1,0:T(8,128)S(1)}, u32[]{:S(2)}, u32[]{:S(2)}) %collective-permute-start.14) | collective-permute-done | bytes 8224 | tf_op jit(solution)/shard_map/ppermute | solution.py:45
  83.4 1.2 %collective-permute-start.15 = (f32[8,512]{1,0:T(8,128)S(1)}, f32[8,512]{1,0:T(8,128)S(1)}, u32[]{:S(2)}, u32[]{:S(2)}) collective-permute-start(f32[8,512]{1,0:T(8,128)S(1)} %get-tuple-element.27), channel_id=1, source_target_pairs={{0,8},{8,16},{16,24},{24,0},{1,9},{9,17},{17,25},{25,1},{2,10},{10... | collective-permute-start | bytes 49160 | tf_op jit(solution)/shard_map/ppermute | solution.py:49
  84.7 2.6 %collective-permute-start.16 = (f32[8,512]{1,0:T(8,128)S(1)}, f32[8,512]{1,0:T(8,128)S(1)}, u32[]{:S(2)}, u32[]{:S(2)}) collective-permute-start(f32[8,512]{1,0:T(8,128)S(1)} %get-tuple-element.28), channel_id=1, source_target_pairs={{0,16},{8,24},{16,0},{24,8},{1,17},{9,25},{17,1},{25,9},{2,18},{10... | collective-permute-start | bytes 49160 | tf_op jit(solution)/shard_map/ppermute | solution.py:49
  87.3 2.0 %collective-permute-start.17 = (f32[8,512]{1,0:T(8,128)S(1)}, f32[8,512]{1,0:T(8,128)S(1)}, u32[]{:S(2)}, u32[]{:S(2)}) collective-permute-start(f32[8,512]{1,0:T(8,128)S(1)} %get-tuple-element.29), channel_id=1, source_target_pairs={{0,24},{8,0},{16,8},{24,16},{1,25},{9,1},{17,9},{25,17},{2,26},{10... | collective-permute-start | bytes 49160 | tf_op jit(solution)/shard_map/ppermute | solution.py:49
  89.3 8.9 %collective-permute-done.18.u1 = f32[32,64]{1,0:T(8,128)S(1)} collective-permute-done((f32[32,64]{1,0:T(8,128)S(1)}, f32[32,64]{1,0:T(8,128)S(1)}, u32[]{:S(2)}, u32[]{:S(2)}) %collective-permute-start.18) | collective-permute-done | bytes 8224 | tf_op jit(solution)/shard_map/ppermute | solution.py:45
  (63 shorter events, 11.8 us)
Async XLA Ops:
  4.1 7.9 %copy-start.7 = (f32[2,4,64,16]{2,3,1,0:T(8,128)S(1)}, f32[2,4,64,16]{2,3,1,0:T(8,128)}, u32[]{:S(2)}) copy-start(f32[2,4,64,16]{2,3,1,0:T(8,128)} %param.20) | copy-start | bytes 98308
  4.2 30.1 %all-to-all-start = ((bf16[8,64,768]{2,1,0:T(8,128)(2,1)}), bf16[8,64,768]{2,1,0:T(8,128)(2,1)S(1)}, u32[]{:S(2)}, u32[]{:S(2)}) async-start(bf16[8,64,768]{2,1,0:T(8,128)(2,1)} %shard_map.150), calls=%async_computation | async-start | bytes 1572864 | tf_op jit(solution)/shard_map/all_to_all | solution.py:318
  13.9 20.4 %copy-start.11 = (f32[2,256]{1,0:T(2,128)S(1)}, f32[2,256]{1,0:T(2,128)}, u32[]{:S(2)}) copy-start(f32[2,256]{1,0:T(2,128)} %gain.3) | copy-start | bytes 6148
  13.9 20.3 %collective-permute-start.4 = (bf16[64,896]{1,0:T(8,128)(2,1)S(1)}, bf16[64,896]{1,0:T(8,128)(2,1)S(1)}, u32[]{:S(2)}, u32[]{:S(2)}) collective-permute-start(bf16[64,896]{1,0:T(8,128)(2,1)S(1)} %get-tuple-element.19.refs_0_), channel_id=1, source_target_pairs={{0,32},{32,64},{64,96},{96,128},{128,160},{160,192},{192,224},{224... | collective-permute-start | bytes 344072 | tf_op jit(solution)/shard_map/ppermute | solution.py:53
  16.7 17.7 %collective-permute-start.5 = (bf16[64,896]{1,0:T(8,128)(2,1)S(1)}, bf16[64,896]{1,0:T(8,128)(2,1)S(1)}, u32[]{:S(2)}, u32[]{:S(2)}) collective-permute-start(bf16[64,896]{1,0:T(8,128)(2,1)S(1)} %get-tuple-element.19.refs_0_), channel_id=1, source_target_pairs={{0,224},{32,0},{64,32},{96,64},{128,96},{160,128},{192,160},{224,1... | collective-permute-start | bytes 344072 | tf_op jit(solution)/shard_map/ppermute | solution.py:53
  16.7 17.6 %collective-permute-start.3 = (f32[128,64]{1,0:T(8,128)S(1)}, f32[128,64]{1,0:T(8,128)S(1)}, u32[]{:S(2)}, u32[]{:S(2)}) collective-permute-start(f32[128,64]{1,0:T(8,128)S(1)} %get-tuple-element.18), channel_id=1, source_target_pairs={{0,5},{32,7},{64,3},{96,1},{128,0},{160,2},{192,6},{224,4},{8,13},... | collective-permute-start | bytes 98312 | tf_op jit(solution)/shard_map/ppermute | solution.py:45
  18.6 3.6 %collective-permute-start = (bf16[8,256]{1,0:T(8,128)(2,1)S(1)}, bf16[8,256]{1,0:T(8,128)(2,1)S(1)}, u32[]{:S(2)}, u32[]{:S(2)}) collective-permute-start(bf16[8,256]{1,0:T(8,128)(2,1)S(1)} %copy-done.14), channel_id=1, source_target_pairs={{0,8},{8,16},{16,24},{24,0},{1,9},{9,17},{17,25},{25,1},{2,10},{10... | collective-permute-start | bytes 12296 | tf_op jit(solution)/shard_map/ppermute | solution.py:49
  20.2 5.1 %collective-permute-start.1 = (bf16[8,256]{1,0:T(8,128)(2,1)S(1)}, bf16[8,256]{1,0:T(8,128)(2,1)S(1)}, u32[]{:S(2)}, u32[]{:S(2)}) collective-permute-start(bf16[8,256]{1,0:T(8,128)(2,1)S(1)} %copy-done.14), channel_id=1, source_target_pairs={{0,16},{8,24},{16,0},{24,8},{1,17},{9,25},{17,1},{25,9},{2,18},{10... | collective-permute-start | bytes 12296 | tf_op jit(solution)/shard_map/ppermute | solution.py:49
  22.2 3.6 %collective-permute-start.2 = (bf16[8,256]{1,0:T(8,128)(2,1)S(1)}, bf16[8,256]{1,0:T(8,128)(2,1)S(1)}, u32[]{:S(2)}, u32[]{:S(2)}) collective-permute-start(bf16[8,256]{1,0:T(8,128)(2,1)S(1)} %copy-done.14), channel_id=1, source_target_pairs={{0,24},{8,0},{16,8},{24,16},{1,25},{9,1},{17,9},{25,17},{2,26},{10... | collective-permute-start | bytes 12296 | tf_op jit(solution)/shard_map/ppermute | solution.py:49
  35.4 24.3 %all-to-all-start.1 = ((bf16[8,32,1024]{2,1,0:T(8,128)(2,1)}), bf16[8,32,1024]{2,1,0:T(8,128)(2,1)S(1)}, u32[]{:S(2)}, u32[]{:S(2)}) async-start(bf16[8,32,1024]{2,1,0:T(8,128)(2,1)} %get-tuple-element.20), calls=%async_computation.1 | async-start | bytes 1048576 | tf_op jit(solution)/shard_map/all_to_all | solution.py:353
  42.2 7.8 %collective-permute-start.9 = (bf16[64,896]{1,0:T(8,128)(2,1)S(1)}, bf16[64,896]{1,0:T(8,128)(2,1)S(1)}, u32[]{:S(2)}, u32[]{:S(2)}) collective-permute-start(bf16[64,896]{1,0:T(8,128)(2,1)S(1)} %collective-permute-done.4.up.refs_1_), channel_id=1, source_target_pairs={{0,32},{32,64},{64,96},{96,128},{128,160},{160,192},{192,224},{224... | collective-permute-start | bytes 344072 | tf_op jit(solution)/shard_map/ppermute | solution.py:53
  47.3 6.4 %collective-permute-start.12 = (bf16[64,896]{1,0:T(8,128)(2,1)S(1)}, bf16[64,896]{1,0:T(8,128)(2,1)S(1)}, u32[]{:S(2)}, u32[]{:S(2)}) collective-permute-start(bf16[64,896]{1,0:T(8,128)(2,1)S(1)} %collective-permute-done.5.down.refs_7_), channel_id=1, source_target_pairs={{0,224},{32,0},{64,32},{96,64},{128,96},{160,128},{192,160},{224,1... | collective-permute-start | bytes 344072 | tf_op jit(solution)/shard_map/ppermute | solution.py:53
  50.0 6.1 %collective-permute-start.10 = (bf16[64,896]{1,0:T(8,128)(2,1)S(1)}, bf16[64,896]{1,0:T(8,128)(2,1)S(1)}, u32[]{:S(2)}, u32[]{:S(2)}) collective-permute-start(bf16[64,896]{1,0:T(8,128)(2,1)S(1)} %collective-permute-done.9.refs_2_), channel_id=1, source_target_pairs={{0,32},{32,64},{64,96},{96,128},{128,160},{160,192},{192,224},{224... | collective-permute-start | bytes 344072 | tf_op jit(solution)/shard_map/ppermute | solution.py:53
  53.7 11.6 %collective-permute-start.13 = (bf16[64,896]{1,0:T(8,128)(2,1)S(1)}, bf16[64,896]{1,0:T(8,128)(2,1)S(1)}, u32[]{:S(2)}, u32[]{:S(2)}) collective-permute-start(bf16[64,896]{1,0:T(8,128)(2,1)S(1)} %collective-permute-done.12.refs_6_), channel_id=1, source_target_pairs={{0,224},{32,0},{64,32},{96,64},{128,96},{160,128},{192,160},{224,1... | collective-permute-start | bytes 344072 | tf_op jit(solution)/shard_map/ppermute | solution.py:53
  56.0 9.2 %collective-permute-start.11 = (bf16[64,896]{1,0:T(8,128)(2,1)S(1)}, bf16[64,896]{1,0:T(8,128)(2,1)S(1)}, u32[]{:S(2)}, u32[]{:S(2)}) collective-permute-start(bf16[64,896]{1,0:T(8,128)(2,1)S(1)} %collective-permute-done.10.refs_3_), channel_id=1, source_target_pairs={{0,32},{32,64},{64,96},{96,128},{128,160},{160,192},{192,224},{224... | collective-permute-start | bytes 344072 | tf_op jit(solution)/shard_map/ppermute | solution.py:53
  60.3 5.0 %collective-permute-start.6 = (f32[32,512]{1,0:T(8,128)S(1)}, f32[32,512]{1,0:T(8,128)S(1)}, u32[]{:S(2)}, u32[]{:S(2)}) collective-permute-start(f32[32,512]{1,0:T(8,128)S(1)} %get-tuple-element.21.out), channel_id=1, source_target_pairs={{0,8},{8,16},{16,24},{24,0},{1,9},{9,17},{17,25},{25,1},{2,10},{10... | collective-permute-start | bytes 196616 | tf_op jit(solution)/shard_map/ppermute | solution.py:49
  61.9 5.9 %collective-permute-start.7 = (f32[32,512]{1,0:T(8,128)S(1)}, f32[32,512]{1,0:T(8,128)S(1)}, u32[]{:S(2)}, u32[]{:S(2)}) collective-permute-start(f32[32,512]{1,0:T(8,128)S(1)} %get-tuple-element.21.out), channel_id=1, source_target_pairs={{0,16},{8,24},{16,0},{24,8},{1,17},{9,25},{17,1},{25,9},{2,18},{10... | collective-permute-start | bytes 196616 | tf_op jit(solution)/shard_map/ppermute | solution.py:49
  62.9 5.0 %collective-permute-start.8 = (f32[32,512]{1,0:T(8,128)S(1)}, f32[32,512]{1,0:T(8,128)S(1)}, u32[]{:S(2)}, u32[]{:S(2)}) collective-permute-start(f32[32,512]{1,0:T(8,128)S(1)} %get-tuple-element.21.out), channel_id=1, source_target_pairs={{0,24},{8,0},{16,8},{24,16},{1,25},{9,1},{17,9},{25,17},{2,26},{10... | collective-permute-start | bytes 196616 | tf_op jit(solution)/shard_map/ppermute | solution.py:49
  68.9 13.8 %all-to-all-start.2 = ((bf16[8,32,768]{2,1,0:T(8,128)(2,1)}), bf16[8,32,768]{2,1,0:T(8,128)(2,1)S(1)}, u32[]{:S(2)}, u32[]{:S(2)}) async-start(bf16[8,32,768]{2,1,0:T(8,128)(2,1)} %get-tuple-element.23), calls=%async_computation.2 | async-start | bytes 786432 | tf_op jit(solution)/shard_map/all_to_all | solution.py:368
  73.9 8.9 %collective-permute-start.14 = (f32[32,64]{1,0:T(8,128)S(1)}, f32[32,64]{1,0:T(8,128)S(1)}, u32[]{:S(2)}, u32[]{:S(2)}) collective-permute-start(f32[32,64]{1,0:T(8,128)S(1)} %get-tuple-element.24), channel_id=1, source_target_pairs={{5,0},{7,32},{3,64},{1,96},{0,128},{2,160},{6,192},{4,224},{13,8},... | collective-permute-start | bytes 24584 | tf_op jit(solution)/shard_map/ppermute | solution.py:45
  83.4 15.7 %collective-permute-start.15 = (f32[8,512]{1,0:T(8,128)S(1)}, f32[8,512]{1,0:T(8,128)S(1)}, u32[]{:S(2)}, u32[]{:S(2)}) collective-permute-start(f32[8,512]{1,0:T(8,128)S(1)} %get-tuple-element.27), channel_id=1, source_target_pairs={{0,8},{8,16},{16,24},{24,0},{1,9},{9,17},{17,25},{25,1},{2,10},{10... | collective-permute-start | bytes 49160 | tf_op jit(solution)/shard_map/ppermute | solution.py:49
  84.7 14.5 %collective-permute-start.16 = (f32[8,512]{1,0:T(8,128)S(1)}, f32[8,512]{1,0:T(8,128)S(1)}, u32[]{:S(2)}, u32[]{:S(2)}) collective-permute-start(f32[8,512]{1,0:T(8,128)S(1)} %get-tuple-element.28), channel_id=1, source_target_pairs={{0,16},{8,24},{16,0},{24,8},{1,17},{9,25},{17,1},{25,9},{2,18},{10... | collective-permute-start | bytes 49160 | tf_op jit(solution)/shard_map/ppermute | solution.py:49
  87.3 11.8 %collective-permute-start.17 = (f32[8,512]{1,0:T(8,128)S(1)}, f32[8,512]{1,0:T(8,128)S(1)}, u32[]{:S(2)}, u32[]{:S(2)}) collective-permute-start(f32[8,512]{1,0:T(8,128)S(1)} %get-tuple-element.29), channel_id=1, source_target_pairs={{0,24},{8,0},{16,8},{24,16},{1,25},{9,1},{17,9},{25,17},{2,26},{10... | collective-permute-start | bytes 49160 | tf_op jit(solution)/shard_map/ppermute | solution.py:49
  89.3 8.9 %collective-permute-start.18 = (f32[32,64]{1,0:T(8,128)S(1)}, f32[32,64]{1,0:T(8,128)S(1)}, u32[]{:S(2)}, u32[]{:S(2)}) collective-permute-start(f32[32,64]{1,0:T(8,128)S(1)} %get-tuple-element.33), channel_id=1, source_target_pairs={{5,0},{7,32},{3,64},{1,96},{0,128},{2,160},{6,192},{4,224},{13,8},... | collective-permute-start | bytes 24584 | tf_op jit(solution)/shard_map/ppermute | solution.py:45
  (15 other events, 88.2 us)

commit v2 on v1

--- a/solution.py
+++ b/solution.py
@@ -70,10 +70,17 @@
     return high, low
 
 
-def pack_kernel(w_in, w_val, w_gate, out):
-    row = jnp.concatenate([w_in[0], w_val[0], w_gate[0]], axis=1)
+def pack_kernel(w_in, w_val, w_gate, out, row, sems):
+    copies = [
+        pltpu.make_async_copy(ref.at[0], row.at[:, pl.ds(i * COLS, COLS)], sems.at[i])
+        for i, ref in enumerate((w_in, w_val, w_gate))
+    ]
+    for copy in copies:
+        copy.start()
+    for copy in copies:
+        copy.wait()
     for i in range(NZ):
-        out[i] = row
+        out[i] = row[...]
 
 
 def prep_kernel(
@@ -274,15 +281,15 @@
             out[n, :, g, :] = base[n, :, g, :] + push
 
 
-def call(body, args, outs, scratch=(), scalar=None):
-    spaces = [pltpu.SMEM if i == scalar else pltpu.VMEM for i in range(len(args))]
+def call(body, args, outs, scratch=(), scalar=None, space=pltpu.VMEM):
+    spaces = [pltpu.SMEM if i == scalar else space for i in range(len(args))]
     return pl.pallas_call(
         body,
         in_specs=[pl.BlockSpec(memory_space=s) for s in spaces],
         out_specs=[pl.BlockSpec(memory_space=pltpu.VMEM) for _ in outs],
         out_shape=outs,
         scratch_shapes=list(scratch),
-        compiler_params=pltpu.CompilerParams(vmem_limit_bytes=12 << 20),
+        compiler_params=pltpu.CompilerParams(vmem_limit_bytes=(60 if space is pl.ANY else 12) << 20),
         cost_estimate=pl.CostEstimate(flops=1 << 24, bytes_accessed=1 << 20, transcendentals=0),
     )(*args)
 
@@ -314,7 +321,13 @@
     state,
 ):
     w_turned = jnp.swapaxes(w_input, 1, 2)
-    (packed,) = call(pack_kernel, [w_turned, w_val, w_gate], [shape((NZ, BLOCK, 3 * COLS), bf16)])
+    (packed,) = call(
+        pack_kernel,
+        [w_turned, w_val, w_gate],
+        [shape((NZ, BLOCK, 3 * COLS), bf16)],
+        [pltpu.VMEM((BLOCK, 3 * COLS), bf16), pltpu.SemaphoreType.DMA((3,))],
+        space=pl.ANY,
+    )
     first_w = lax.all_to_all(packed, "z", 0, 0, tiled=True)
     pieces = [stream] + [shift_y(stream, k) for k in range(1, NY)]
     base, drive, own, late = call(

time: 100 us -> 98.3 us (0.983)
  local copies, waits for them, and re-layouts: 3.16 us -> 0.66 us
    unnamed x34 -> x28, local copies, waits for them, and re-layouts: 3.16 us -> 0.66 us
where the time goes in v2:
time: 98.3 us; the launch traced here: 97.9 us
  starting transfers between devices  51.4 us (52%)
  waiting for transfers between devices  36.9 us (38%)
  Pallas kernels  8.12 us (8%)
    ppermute x3, waiting for transfers between devices, turn(): return lax.ppermute(value, ALL, pairs)  26.1 us
    ppermute x7, starting transfers between devices, shift_z(): return lax.ppermute(value, 'z', [(i, (i + k) % NZ) for i in range(NZ)])  15.2 us
    ppermute x9, starting transfers between devices, shift_y(): return lax.ppermute(value, 'y', [(i, (i + k) % NY) for i in range(NY)])  14.9 us
    all_to_all x2, starting transfers between devices, both_layers(): got = lax.all_to_all(payload, DP, 0, 0, tiled=True)  11.5 us
    pallas_call x9, Pallas kernels, call(): pl.pallas_call(body, in_specs=[pl.BlockSpec(memory_space=s) for s in spac...  8.12 us
    all_to_all x1, starting transfers between devices, both_layers(): first_w = lax.all_to_all(packed, 'z', 0, 0, tiled=True)  7.8 us
    ppermute x9, waiting for transfers between devices, shift_y(): return lax.ppermute(value, 'y', [(i, (i + k) % NY) for i in range(NY)])  5.59 us
    ppermute x7, waiting for transfers between devices, shift_z(): return lax.ppermute(value, 'z', [(i, (i + k) % NZ) for i in range(NZ)])  5.14 us
  transfers between devices with their start and end apart: 22, of which 10 were waited for; matrix products, arithmetic and copies ran while one was open for 0% of the time, Pallas kernels for 3%

profile of v2, /device:TPU:110, one launch (start us, length us, event | category | flops | bytes accessed | tf_op | source)
XLA Modules:
  0.0 97.9 jit_solution(5110091779056677376)
XLA Ops:
  0.6 1.8 %shard_map.150 = bf16[8,64,768]{2,1,0:T(8,128)(2,1)} custom-call(bf16[2,64,256]{2,1,0:T(8,128)(2,1)} %bitcast.3, bf16[2,64,256]{2,1,0:T(8,128)(2,1)} %w_val.3, bf16[2,64,256]{2,1,0:T(8,128)(2,1)} %w_gate.3), custom_call_target="tpu_custom_call" | custom-call | flops 16777216 | bytes 1048576 | tf_op jit(solution)/shard_map/pallas_call | solution.py:286
  2.5 7.8 %all-to-all-start = ((bf16[8,64,768]{2,1,0:T(8,128)(2,1)}), bf16[8,64,768]{2,1,0:T(8,128)(2,1)S(1)}, u32[]{:S(2)}, u32[]{:S(2)}) async-start(bf16[8,64,768]{2,1,0:T(8,128)(2,1)} %shard_map.150), calls=%async_computation | async-start | bytes 1572864 | tf_op jit(solution)/shard_map/all_to_all | solution.py:331
  11.0 1.2 %shard_map.149 = (f32[2,32,4,128]{3,2,1,0:T(4,128)S(1)}, f32[2,64,128]{2,1,0:T(8,128)S(1)}, f32[128,64]{1,0:T(8,128)S(1)}, bf16[64,896]{1,0:T(8,128)(2,1)S(1)}) custom-call(f32[2,4,64]{2,1,0:T(4,128)S(1)} %copy-done.9, f32[2,4,64]{2,1,0:T(4,128)S(1)} %copy-done.10, f32[2,4]{1,0:T(2,128)S(1)} %copy-done.12, f32[2,4,16,64]{3,2,1,0:T(8,128)S(1)} %bitcast.5, ...), custom_call_target="tpu_custom_call" | custom-call | flops 16777216 | bytes 1048576 | tf_op jit(solution)/shard_map/pallas_call | solution.py:286
  12.3 2.8 %collective-permute-start.4 = (bf16[64,896]{1,0:T(8,128)(2,1)S(1)}, bf16[64,896]{1,0:T(8,128)(2,1)S(1)}, u32[]{:S(2)}, u32[]{:S(2)}) collective-permute-start(bf16[64,896]{1,0:T(8,128)(2,1)S(1)} %get-tuple-element.19.refs_0_), channel_id=1, source_target_pairs={{0,32},{32,64},{64,96},{96,128},{128,160},{160,192},{192,224},{224... | collective-permute-start | bytes 344072 | tf_op jit(solution)/shard_map/ppermute | solution.py:53
  15.0 1.9 %collective-permute-start.3 = (f32[128,64]{1,0:T(8,128)S(1)}, f32[128,64]{1,0:T(8,128)S(1)}, u32[]{:S(2)}, u32[]{:S(2)}) collective-permute-start(f32[128,64]{1,0:T(8,128)S(1)} %get-tuple-element.18), channel_id=1, source_target_pairs={{0,5},{32,7},{64,3},{96,1},{128,0},{160,2},{192,6},{224,4},{8,13},... | collective-permute-start | bytes 98312 | tf_op jit(solution)/shard_map/ppermute | solution.py:45
  17.0 1.6 %collective-permute-start = (bf16[8,256]{1,0:T(8,128)(2,1)S(1)}, bf16[8,256]{1,0:T(8,128)(2,1)S(1)}, u32[]{:S(2)}, u32[]{:S(2)}) collective-permute-start(bf16[8,256]{1,0:T(8,128)(2,1)S(1)} %copy-done.11), channel_id=1, source_target_pairs={{0,8},{8,16},{16,24},{24,0},{1,9},{9,17},{17,25},{25,1},{2,10},{10... | collective-permute-start | bytes 12296 | tf_op jit(solution)/shard_map/ppermute | solution.py:49
  20.6 1.7 %collective-permute-start.2 = (bf16[8,256]{1,0:T(8,128)(2,1)S(1)}, bf16[8,256]{1,0:T(8,128)(2,1)S(1)}, u32[]{:S(2)}, u32[]{:S(2)}) collective-permute-start(bf16[8,256]{1,0:T(8,128)(2,1)S(1)} %copy-done.11), channel_id=1, source_target_pairs={{0,24},{8,0},{16,8},{24,16},{1,25},{9,1},{17,9},{25,17},{2,26},{10... | collective-permute-start | bytes 12296 | tf_op jit(solution)/shard_map/ppermute | solution.py:49
  22.2 1.4 %collective-permute-done.1.p2 = bf16[8,256]{1,0:T(8,128)(2,1)S(1)} collective-permute-done((bf16[8,256]{1,0:T(8,128)(2,1)S(1)}, bf16[8,256]{1,0:T(8,128)(2,1)S(1)}, u32[]{:S(2)}, u32[]{:S(2)}) %collective-permute-start.1) | collective-permute-done | bytes 4128 | tf_op jit(solution)/shard_map/ppermute | solution.py:49
  24.2 8.4 %collective-permute-done.3.carried = f32[128,64]{1,0:T(8,128)S(1)} collective-permute-done((f32[128,64]{1,0:T(8,128)S(1)}, f32[128,64]{1,0:T(8,128)S(1)}, u32[]{:S(2)}, u32[]{:S(2)}) %collective-permute-start.3) | collective-permute-done | bytes 32800 | tf_op jit(solution)/shard_map/ppermute | solution.py:45
  33.8 6.8 %all-to-all-start.1 = ((bf16[8,32,1024]{2,1,0:T(8,128)(2,1)}), bf16[8,32,1024]{2,1,0:T(8,128)(2,1)S(1)}, u32[]{:S(2)}, u32[]{:S(2)}) async-start(bf16[8,32,1024]{2,1,0:T(8,128)(2,1)} %get-tuple-element.20), calls=%async_computation.1 | async-start | bytes 1048576 | tf_op jit(solution)/shard_map/all_to_all | solution.py:366
  40.5 5.1 %collective-permute-start.9 = (bf16[64,896]{1,0:T(8,128)(2,1)S(1)}, bf16[64,896]{1,0:T(8,128)(2,1)S(1)}, u32[]{:S(2)}, u32[]{:S(2)}) collective-permute-start(bf16[64,896]{1,0:T(8,128)(2,1)S(1)} %collective-permute-done.4.up.refs_1_), channel_id=1, source_target_pairs={{0,32},{32,64},{64,96},{96,128},{128,160},{160,192},{192,224},{224... | collective-permute-start | bytes 344072 | tf_op jit(solution)/shard_map/ppermute | solution.py:53
  45.6 2.7 %collective-permute-done.9.refs_2_ = bf16[64,896]{1,0:T(8,128)(2,1)S(1)} collective-permute-done((bf16[64,896]{1,0:T(8,128)(2,1)S(1)}, bf16[64,896]{1,0:T(8,128)(2,1)S(1)}, u32[]{:S(2)}, u32[]{:S(2)}) %collective-permute-start.9) | collective-permute-done | bytes 114720 | tf_op jit(solution)/shard_map/ppermute | solution.py:53
  48.3 3.7 %collective-permute-start.10 = (bf16[64,896]{1,0:T(8,128)(2,1)S(1)}, bf16[64,896]{1,0:T(8,128)(2,1)S(1)}, u32[]{:S(2)}, u32[]{:S(2)}) collective-permute-start(bf16[64,896]{1,0:T(8,128)(2,1)S(1)} %collective-permute-done.9.refs_2_), channel_id=1, source_target_pairs={{0,32},{32,64},{64,96},{96,128},{128,160},{160,192},{192,224},{224... | collective-permute-start | bytes 344072 | tf_op jit(solution)/shard_map/ppermute | solution.py:53
  52.0 2.4 %collective-permute-done.10.refs_3_ = bf16[64,896]{1,0:T(8,128)(2,1)S(1)} collective-permute-done((bf16[64,896]{1,0:T(8,128)(2,1)S(1)}, bf16[64,896]{1,0:T(8,128)(2,1)S(1)}, u32[]{:S(2)}, u32[]{:S(2)}) %collective-permute-start.10) | collective-permute-done | bytes 114720 | tf_op jit(solution)/shard_map/ppermute | solution.py:53
  54.4 3.6 %collective-permute-start.11 = (bf16[64,896]{1,0:T(8,128)(2,1)S(1)}, bf16[64,896]{1,0:T(8,128)(2,1)S(1)}, u32[]{:S(2)}, u32[]{:S(2)}) collective-permute-start(bf16[64,896]{1,0:T(8,128)(2,1)S(1)} %collective-permute-done.10.refs_3_), channel_id=1, source_target_pairs={{0,32},{32,64},{64,96},{96,128},{128,160},{160,192},{192,224},{224... | collective-permute-start | bytes 344072 | tf_op jit(solution)/shard_map/ppermute | solution.py:53
  58.7 1.6 %collective-permute-start.6 = (f32[32,512]{1,0:T(8,128)S(1)}, f32[32,512]{1,0:T(8,128)S(1)}, u32[]{:S(2)}, u32[]{:S(2)}) collective-permute-start(f32[32,512]{1,0:T(8,128)S(1)} %get-tuple-element.21.out), channel_id=1, source_target_pairs={{0,8},{8,16},{16,24},{24,0},{1,9},{9,17},{17,25},{25,1},{2,10},{10... | collective-permute-start | bytes 196616 | tf_op jit(solution)/shard_map/ppermute | solution.py:49
  61.2 2.4 %collective-permute-start.8 = (f32[32,512]{1,0:T(8,128)S(1)}, f32[32,512]{1,0:T(8,128)S(1)}, u32[]{:S(2)}, u32[]{:S(2)}) collective-permute-start(f32[32,512]{1,0:T(8,128)S(1)} %get-tuple-element.21.out), channel_id=1, source_target_pairs={{0,24},{8,0},{16,8},{24,16},{1,25},{9,1},{17,9},{25,17},{2,26},{10... | collective-permute-start | bytes 196616 | tf_op jit(solution)/shard_map/ppermute | solution.py:49
  63.6 2.5 %collective-permute-done.7.r2 = f32[32,512]{1,0:T(8,128)S(1)} collective-permute-done((f32[32,512]{1,0:T(8,128)S(1)}, f32[32,512]{1,0:T(8,128)S(1)}, u32[]{:S(2)}, u32[]{:S(2)}) %collective-permute-start.7) | collective-permute-done | bytes 65568 | tf_op jit(solution)/shard_map/ppermute | solution.py:49
  67.2 4.8 %all-to-all-start.2 = ((bf16[8,32,768]{2,1,0:T(8,128)(2,1)}), bf16[8,32,768]{2,1,0:T(8,128)(2,1)S(1)}, u32[]{:S(2)}, u32[]{:S(2)}) async-start(bf16[8,32,768]{2,1,0:T(8,128)(2,1)} %get-tuple-element.23), calls=%async_computation.2 | async-start | bytes 786432 | tf_op jit(solution)/shard_map/all_to_all | solution.py:381
  72.0 8.9 %collective-permute-done.14.earlier.u0 = f32[32,64]{1,0:T(8,128)S(1)} collective-permute-done((f32[32,64]{1,0:T(8,128)S(1)}, f32[32,64]{1,0:T(8,128)S(1)}, u32[]{:S(2)}, u32[]{:S(2)}) %collective-permute-start.14) | collective-permute-done | bytes 8224 | tf_op jit(solution)/shard_map/ppermute | solution.py:45
  81.6 1.2 %collective-permute-start.15 = (f32[8,512]{1,0:T(8,128)S(1)}, f32[8,512]{1,0:T(8,128)S(1)}, u32[]{:S(2)}, u32[]{:S(2)}) collective-permute-start(f32[8,512]{1,0:T(8,128)S(1)} %get-tuple-element.27), channel_id=1, source_target_pairs={{0,8},{8,16},{16,24},{24,0},{1,9},{9,17},{17,25},{25,1},{2,10},{10... | collective-permute-start | bytes 49160 | tf_op jit(solution)/shard_map/ppermute | solution.py:49
  82.8 2.6 %collective-permute-start.16 = (f32[8,512]{1,0:T(8,128)S(1)}, f32[8,512]{1,0:T(8,128)S(1)}, u32[]{:S(2)}, u32[]{:S(2)}) collective-permute-start(f32[8,512]{1,0:T(8,128)S(1)} %get-tuple-element.28), channel_id=1, source_target_pairs={{0,16},{8,24},{16,0},{24,8},{1,17},{9,25},{17,1},{25,9},{2,18},{10... | collective-permute-start | bytes 49160 | tf_op jit(solution)/shard_map/ppermute | solution.py:49
  85.5 2.0 %collective-permute-start.17 = (f32[8,512]{1,0:T(8,128)S(1)}, f32[8,512]{1,0:T(8,128)S(1)}, u32[]{:S(2)}, u32[]{:S(2)}) collective-permute-start(f32[8,512]{1,0:T(8,128)S(1)} %get-tuple-element.29), channel_id=1, source_target_pairs={{0,24},{8,0},{16,8},{24,16},{1,25},{9,1},{17,9},{25,17},{2,26},{10... | collective-permute-start | bytes 49160 | tf_op jit(solution)/shard_map/ppermute | solution.py:49
  87.4 8.9 %collective-permute-done.18.u1 = f32[32,64]{1,0:T(8,128)S(1)} collective-permute-done((f32[32,64]{1,0:T(8,128)S(1)}, f32[32,64]{1,0:T(8,128)S(1)}, u32[]{:S(2)}, u32[]{:S(2)}) %collective-permute-start.18) | collective-permute-done | bytes 8224 | tf_op jit(solution)/shard_map/ppermute | solution.py:45
  (57 shorter events, 9.5 us)
Async XLA Ops:
  2.4 7.9 %copy-start = (bf16[2,256,64]{1,2,0:T(8,128)(2,1)S(1)}, bf16[2,256,64]{1,2,0:T(8,128)(2,1)}, u32[]{:S(2)}) copy-start(bf16[2,256,64]{1,2,0:T(8,128)(2,1)} %param.16) | copy-start | bytes 196612
  2.5 30.1 %all-to-all-start = ((bf16[8,64,768]{2,1,0:T(8,128)(2,1)}), bf16[8,64,768]{2,1,0:T(8,128)(2,1)S(1)}, u32[]{:S(2)}, u32[]{:S(2)}) async-start(bf16[8,64,768]{2,1,0:T(8,128)(2,1)} %shard_map.150), calls=%async_computation | async-start | bytes 1572864 | tf_op jit(solution)/shard_map/all_to_all | solution.py:331
  12.2 20.4 %copy-start.8 = (f32[2,256]{1,0:T(2,128)S(1)}, f32[2,256]{1,0:T(2,128)}, u32[]{:S(2)}) copy-start(f32[2,256]{1,0:T(2,128)} %gain.3) | copy-start | bytes 6148
  12.3 20.3 %collective-permute-start.4 = (bf16[64,896]{1,0:T(8,128)(2,1)S(1)}, bf16[64,896]{1,0:T(8,128)(2,1)S(1)}, u32[]{:S(2)}, u32[]{:S(2)}) collective-permute-start(bf16[64,896]{1,0:T(8,128)(2,1)S(1)} %get-tuple-element.19.refs_0_), channel_id=1, source_target_pairs={{0,32},{32,64},{64,96},{96,128},{128,160},{160,192},{192,224},{224... | collective-permute-start | bytes 344072 | tf_op jit(solution)/shard_map/ppermute | solution.py:53
  15.0 17.6 %collective-permute-start.5 = (bf16[64,896]{1,0:T(8,128)(2,1)S(1)}, bf16[64,896]{1,0:T(8,128)(2,1)S(1)}, u32[]{:S(2)}, u32[]{:S(2)}) collective-permute-start(bf16[64,896]{1,0:T(8,128)(2,1)S(1)} %get-tuple-element.19.refs_0_), channel_id=1, source_target_pairs={{0,224},{32,0},{64,32},{96,64},{128,96},{160,128},{192,160},{224,1... | collective-permute-start | bytes 344072 | tf_op jit(solution)/shard_map/ppermute | solution.py:53
  15.0 17.6 %collective-permute-start.3 = (f32[128,64]{1,0:T(8,128)S(1)}, f32[128,64]{1,0:T(8,128)S(1)}, u32[]{:S(2)}, u32[]{:S(2)}) collective-permute-start(f32[128,64]{1,0:T(8,128)S(1)} %get-tuple-element.18), channel_id=1, source_target_pairs={{0,5},{32,7},{64,3},{96,1},{128,0},{160,2},{192,6},{224,4},{8,13},... | collective-permute-start | bytes 98312 | tf_op jit(solution)/shard_map/ppermute | solution.py:45
  17.0 3.6 %collective-permute-start = (bf16[8,256]{1,0:T(8,128)(2,1)S(1)}, bf16[8,256]{1,0:T(8,128)(2,1)S(1)}, u32[]{:S(2)}, u32[]{:S(2)}) collective-permute-start(bf16[8,256]{1,0:T(8,128)(2,1)S(1)} %copy-done.11), channel_id=1, source_target_pairs={{0,8},{8,16},{16,24},{24,0},{1,9},{9,17},{17,25},{25,1},{2,10},{10... | collective-permute-start | bytes 12296 | tf_op jit(solution)/shard_map/ppermute | solution.py:49
  18.5 5.1 %collective-permute-start.1 = (bf16[8,256]{1,0:T(8,128)(2,1)S(1)}, bf16[8,256]{1,0:T(8,128)(2,1)S(1)}, u32[]{:S(2)}, u32[]{:S(2)}) collective-permute-start(bf16[8,256]{1,0:T(8,128)(2,1)S(1)} %copy-done.11), channel_id=1, source_target_pairs={{0,16},{8,24},{16,0},{24,8},{1,17},{9,25},{17,1},{25,9},{2,18},{10... | collective-permute-start | bytes 12296 | tf_op jit(solution)/shard_map/ppermute | solution.py:49
  20.6 3.6 %collective-permute-start.2 = (bf16[8,256]{1,0:T(8,128)(2,1)S(1)}, bf16[8,256]{1,0:T(8,128)(2,1)S(1)}, u32[]{:S(2)}, u32[]{:S(2)}) collective-permute-start(bf16[8,256]{1,0:T(8,128)(2,1)S(1)} %copy-done.11), channel_id=1, source_target_pairs={{0,24},{8,0},{16,8},{24,16},{1,25},{9,1},{17,9},{25,17},{2,26},{10... | collective-permute-start | bytes 12296 | tf_op jit(solution)/shard_map/ppermute | solution.py:49
  33.8 24.2 %all-to-all-start.1 = ((bf16[8,32,1024]{2,1,0:T(8,128)(2,1)}), bf16[8,32,1024]{2,1,0:T(8,128)(2,1)S(1)}, u32[]{:S(2)}, u32[]{:S(2)}) async-start(bf16[8,32,1024]{2,1,0:T(8,128)(2,1)} %get-tuple-element.20), calls=%async_computation.1 | async-start | bytes 1048576 | tf_op jit(solution)/shard_map/all_to_all | solution.py:366
  40.5 7.8 %collective-permute-start.9 = (bf16[64,896]{1,0:T(8,128)(2,1)S(1)}, bf16[64,896]{1,0:T(8,128)(2,1)S(1)}, u32[]{:S(2)}, u32[]{:S(2)}) collective-permute-start(bf16[64,896]{1,0:T(8,128)(2,1)S(1)} %collective-permute-done.4.up.refs_1_), channel_id=1, source_target_pairs={{0,32},{32,64},{64,96},{96,128},{128,160},{160,192},{192,224},{224... | collective-permute-start | bytes 344072 | tf_op jit(solution)/shard_map/ppermute | solution.py:53
  45.6 6.4 %collective-permute-start.12 = (bf16[64,896]{1,0:T(8,128)(2,1)S(1)}, bf16[64,896]{1,0:T(8,128)(2,1)S(1)}, u32[]{:S(2)}, u32[]{:S(2)}) collective-permute-start(bf16[64,896]{1,0:T(8,128)(2,1)S(1)} %collective-permute-done.5.down.refs_7_), channel_id=1, source_target_pairs={{0,224},{32,0},{64,32},{96,64},{128,96},{160,128},{192,160},{224,1... | collective-permute-start | bytes 344072 | tf_op jit(solution)/shard_map/ppermute | solution.py:53
  48.3 6.1 %collective-permute-start.10 = (bf16[64,896]{1,0:T(8,128)(2,1)S(1)}, bf16[64,896]{1,0:T(8,128)(2,1)S(1)}, u32[]{:S(2)}, u32[]{:S(2)}) collective-permute-start(bf16[64,896]{1,0:T(8,128)(2,1)S(1)} %collective-permute-done.9.refs_2_), channel_id=1, source_target_pairs={{0,32},{32,64},{64,96},{96,128},{128,160},{160,192},{192,224},{224... | collective-permute-start | bytes 344072 | tf_op jit(solution)/shard_map/ppermute | solution.py:53
  52.0 11.6 %collective-permute-start.13 = (bf16[64,896]{1,0:T(8,128)(2,1)S(1)}, bf16[64,896]{1,0:T(8,128)(2,1)S(1)}, u32[]{:S(2)}, u32[]{:S(2)}) collective-permute-start(bf16[64,896]{1,0:T(8,128)(2,1)S(1)} %collective-permute-done.12.refs_6_), channel_id=1, source_target_pairs={{0,224},{32,0},{64,32},{96,64},{128,96},{160,128},{192,160},{224,1... | collective-permute-start | bytes 344072 | tf_op jit(solution)/shard_map/ppermute | solution.py:53
  54.4 9.2 %collective-permute-start.11 = (bf16[64,896]{1,0:T(8,128)(2,1)S(1)}, bf16[64,896]{1,0:T(8,128)(2,1)S(1)}, u32[]{:S(2)}, u32[]{:S(2)}) collective-permute-start(bf16[64,896]{1,0:T(8,128)(2,1)S(1)} %collective-permute-done.10.refs_3_), channel_id=1, source_target_pairs={{0,32},{32,64},{64,96},{96,128},{128,160},{160,192},{192,224},{224... | collective-permute-start | bytes 344072 | tf_op jit(solution)/shard_map/ppermute | solution.py:53
  58.7 5.0 %collective-permute-start.6 = (f32[32,512]{1,0:T(8,128)S(1)}, f32[32,512]{1,0:T(8,128)S(1)}, u32[]{:S(2)}, u32[]{:S(2)}) collective-permute-start(f32[32,512]{1,0:T(8,128)S(1)} %get-tuple-element.21.out), channel_id=1, source_target_pairs={{0,8},{8,16},{16,24},{24,0},{1,9},{9,17},{17,25},{25,1},{2,10},{10... | collective-permute-start | bytes 196616 | tf_op jit(solution)/shard_map/ppermute | solution.py:49
  60.3 5.9 %collective-permute-start.7 = (f32[32,512]{1,0:T(8,128)S(1)}, f32[32,512]{1,0:T(8,128)S(1)}, u32[]{:S(2)}, u32[]{:S(2)}) collective-permute-start(f32[32,512]{1,0:T(8,128)S(1)} %get-tuple-element.21.out), channel_id=1, source_target_pairs={{0,16},{8,24},{16,0},{24,8},{1,17},{9,25},{17,1},{25,9},{2,18},{10... | collective-permute-start | bytes 196616 | tf_op jit(solution)/shard_map/ppermute | solution.py:49
  61.2 5.0 %collective-permute-start.8 = (f32[32,512]{1,0:T(8,128)S(1)}, f32[32,512]{1,0:T(8,128)S(1)}, u32[]{:S(2)}, u32[]{:S(2)}) collective-permute-start(f32[32,512]{1,0:T(8,128)S(1)} %get-tuple-element.21.out), channel_id=1, source_target_pairs={{0,24},{8,0},{16,8},{24,16},{1,25},{9,1},{17,9},{25,17},{2,26},{10... | collective-permute-start | bytes 196616 | tf_op jit(solution)/shard_map/ppermute | solution.py:49
  67.2 13.7 %all-to-all-start.2 = ((bf16[8,32,768]{2,1,0:T(8,128)(2,1)}), bf16[8,32,768]{2,1,0:T(8,128)(2,1)S(1)}, u32[]{:S(2)}, u32[]{:S(2)}) async-start(bf16[8,32,768]{2,1,0:T(8,128)(2,1)} %get-tuple-element.23), calls=%async_computation.2 | async-start | bytes 786432 | tf_op jit(solution)/shard_map/all_to_all | solution.py:381
  72.0 8.9 %collective-permute-start.14 = (f32[32,64]{1,0:T(8,128)S(1)}, f32[32,64]{1,0:T(8,128)S(1)}, u32[]{:S(2)}, u32[]{:S(2)}) collective-permute-start(f32[32,64]{1,0:T(8,128)S(1)} %get-tuple-element.24), channel_id=1, source_target_pairs={{5,0},{7,32},{3,64},{1,96},{0,128},{2,160},{6,192},{4,224},{13,8},... | collective-permute-start | bytes 24584 | tf_op jit(solution)/shard_map/ppermute | solution.py:45
  81.6 15.7 %collective-permute-start.15 = (f32[8,512]{1,0:T(8,128)S(1)}, f32[8,512]{1,0:T(8,128)S(1)}, u32[]{:S(2)}, u32[]{:S(2)}) collective-permute-start(f32[8,512]{1,0:T(8,128)S(1)} %get-tuple-element.27), channel_id=1, source_target_pairs={{0,8},{8,16},{16,24},{24,0},{1,9},{9,17},{17,25},{25,1},{2,10},{10... | collective-permute-start | bytes 49160 | tf_op jit(solution)/shard_map/ppermute | solution.py:49
  82.8 14.5 %collective-permute-start.16 = (f32[8,512]{1,0:T(8,128)S(1)}, f32[8,512]{1,0:T(8,128)S(1)}, u32[]{:S(2)}, u32[]{:S(2)}) collective-permute-start(f32[8,512]{1,0:T(8,128)S(1)} %get-tuple-element.28), channel_id=1, source_target_pairs={{0,16},{8,24},{16,0},{24,8},{1,17},{9,25},{17,1},{25,9},{2,18},{10... | collective-permute-start | bytes 49160 | tf_op jit(solution)/shard_map/ppermute | solution.py:49
  85.5 11.8 %collective-permute-start.17 = (f32[8,512]{1,0:T(8,128)S(1)}, f32[8,512]{1,0:T(8,128)S(1)}, u32[]{:S(2)}, u32[]{:S(2)}) collective-permute-start(f32[8,512]{1,0:T(8,128)S(1)} %get-tuple-element.29), channel_id=1, source_target_pairs={{0,24},{8,0},{16,8},{24,16},{1,25},{9,1},{17,9},{25,17},{2,26},{10... | collective-permute-start | bytes 49160 | tf_op jit(solution)/shard_map/ppermute | solution.py:49
  87.4 8.9 %collective-permute-start.18 = (f32[32,64]{1,0:T(8,128)S(1)}, f32[32,64]{1,0:T(8,128)S(1)}, u32[]{:S(2)}, u32[]{:S(2)}) collective-permute-start(f32[32,64]{1,0:T(8,128)S(1)} %get-tuple-element.33), channel_id=1, source_target_pairs={{5,0},{7,32},{3,64},{1,96},{0,128},{2,160},{6,192},{4,224},{13,8},... | collective-permute-start | bytes 24584 | tf_op jit(solution)/shard_map/ppermute | solution.py:45
  (12 other events, 85.8 us)

commit v3 on v2

--- a/solution.py
+++ b/solution.py
@@ -54,14 +54,12 @@
 
 
 def ring_z(own):
-    up1 = shift_z(own, 1)
-    down1 = shift_z(own, -1)
-    up2 = shift_z(up1, 1)
-    down2 = shift_z(down1, -1)
-    up3 = shift_z(up2, 1)
-    down3 = shift_z(down2, -1)
-    up4 = shift_z(up3, 1)
-    return [own, up1, up2, up3, up4, down3, down2, down1]
+    ups, downs = [own], [own]
+    for step in range(1, NZ // 2 + 1):
+        ups.append(shift_z(ups[-1], 1))
+        if step < NZ // 2:
+            downs.append(shift_z(downs[-1], -1))
+    return ups + downs[:0:-1]
 
 
 def two_halves(value):
@@ -70,17 +68,18 @@
     return high, low
 
 
-def pack_kernel(w_in, w_val, w_gate, out, row, sems):
-    copies = [
-        pltpu.make_async_copy(ref.at[0], row.at[:, pl.ds(i * COLS, COLS)], sems.at[i])
-        for i, ref in enumerate((w_in, w_val, w_gate))
-    ]
+def pack_kernel(w_in, w_val, w_gate, out, soon, first, row, sems):
+    parts = [(w_in.at[0], first), (w_val.at[0], row.at[:, pl.ds(0, COLS)])]
+    parts += [(w_gate.at[0], row.at[:, pl.ds(COLS, COLS)])]
+    parts += [(w_in.at[1], row.at[:, pl.ds(2 * COLS, COLS)])]
+    copies = [pltpu.make_async_copy(a, b, sems.at[i]) for i, (a, b) in enumerate(parts)]
     for copy in copies:
         copy.start()
     for copy in copies:
         copy.wait()
     for i in range(NZ):
-        out[i] = row[...]
+        out[i] = first[...]
+    soon[...] = row[...]
 
 
 def prep_kernel(
@@ -93,7 +92,6 @@
     r_im,
     d_skip,
     state,
-    w_in,
     w_val,
     w_gate,
     base,
@@ -141,7 +139,7 @@
         if n == 0:
             carried[LAYERS * SEQS :, :] = mix
         else:
-            late[...] = jnp.concatenate([w_val[n], w_gate[n], w_in[n], *two_halves(mix)], axis=1)
+            late[...] = jnp.concatenate([w_val[n], w_gate[n], *two_halves(mix)], axis=1)
 
 
 def write_payload(pay_ref, x, blocks, offset, mix=None):
@@ -166,14 +164,14 @@
     )
 
 
-def first_kernel(p0, p1, p2, p3, gain, carried, w, up, down, pay_ref, x_ref, rows):
+def first_kernel(p0, p1, p2, p3, gain, carried, w, pay_ref, x_ref, rows):
     y = lax.axis_index("y")
     for k, piece in enumerate((p0, p1, p2, p3)):
         rows[lax.rem(y + NY - k, NY)] = piece[...].astype(f32)
     x = rows[...].reshape(SEQS, COLS)
     x_ref[...] = x
     normed = (x * gain[0:1]).astype(bf16)
-    blocks = [times_turned(normed, w[j, :, :COLS]) for j in range(NZ)]
+    blocks = [times_turned(normed, w[j]) for j in range(NZ)]
     write_payload(pay_ref, x, blocks, carried[:SEQS], carried[LAYERS * SEQS :])
 
 
@@ -208,15 +206,14 @@
         offset = sent[:, WIDTH : WIDTH + BLOCK].astype(f32)
         offset = offset + sent[:, WIDTH + BLOCK : WIDTH + 2 * BLOCK].astype(f32)
         cut = slice(slot * BLOCK, (slot + 1) * BLOCK)
-        if isinstance(w, list):
-            m_high = w[slot][:, 3 * COLS : 3 * COLS + BLOCK]
-            m_low = w[slot][:, 3 * COLS + BLOCK :]
-            weights[cut, :] = w[slot][:, : 2 * COLS]
+        weights[cut, :] = w[slot][:, : 2 * COLS]
+        if got.shape[2] == NEXT_PAY:
+            m_high = w[slot][:, 2 * COLS : 2 * COLS + BLOCK]
+            m_low = w[slot][:, 2 * COLS + BLOCK :]
         else:
             m = sent[:, WIDTH + 256 :]
             m_high = jnp.concatenate([m[:, :BLOCK], m[:, BLOCK : 2 * BLOCK]], axis=0)
             m_low = jnp.concatenate([m[:, 2 * BLOCK : 3 * BLOCK], m[:, 3 * BLOCK :]], axis=0)
-            weights[cut, :] = w[block][:, COLS:]
         high, low = two_halves(u_blocks[block])
         pre = (
             offset
@@ -242,7 +239,9 @@
         u_blocks[j] = u[:, j * BLOCK : (j + 1) * BLOCK]
 
 
-def mid_kernel(got, w, out, own_u, u_blocks, ordered, weights):
+def mid_kernel(got, *refs):
+    w = refs[:NZ]
+    out, own_u, u_blocks, ordered, weights = refs[NZ:]
     split_blocks(inputs_of(got), u_blocks)
     own_u[...] = own_block(u_blocks)
     out[...] = gated(got, u_blocks, w, ordered, weights)
@@ -254,7 +253,7 @@
 
 
 def last_kernel(got, u_blocks, *refs):
-    w = list(refs[:NZ])
+    w = refs[:NZ]
     own_out, s1, s2, s3, ordered, weights, by_y = refs[NZ:]
     out = gated(got, u_blocks, w, ordered, weights)
     y = lax.axis_index("y")
@@ -321,11 +320,15 @@
     state,
 ):
     w_turned = jnp.swapaxes(w_input, 1, 2)
-    (packed,) = call(
+    packed, soon = call(
         pack_kernel,
         [w_turned, w_val, w_gate],
-        [shape((NZ, BLOCK, 3 * COLS), bf16)],
-        [pltpu.VMEM((BLOCK, 3 * COLS), bf16), pltpu.SemaphoreType.DMA((3,))],
+        [shape((NZ, BLOCK, COLS), bf16), shape((BLOCK, 3 * COLS), bf16)],
+        [
+            pltpu.VMEM((BLOCK, COLS), bf16),
+            pltpu.VMEM((BLOCK, 3 * COLS), bf16),
+            pltpu.SemaphoreType.DMA((4,)),
+        ],
         space=pl.ANY,
     )
     first_w = lax.all_to_all(packed, "z", 0, 0, tiled=True)
@@ -342,7 +345,6 @@
             readout_imaginary,
             d_skip,
             state,
-            w_turned,
             w_val,
             w_gate,
         ],
@@ -350,23 +352,24 @@
             shape(state.shape),
             shape((LAYERS, BLOCK, state.shape[-1])),
             shape((LAYERS * SEQS + BLOCK, BLOCK)),
-            shape((BLOCK, 3 * COLS + 2 * BLOCK), bf16),
+            shape((BLOCK, 2 * COLS + 2 * BLOCK), bf16),
         ],
         scalar=2,
     )
     carried = turn(own)
-    ring = ring_z(late)
+    ring_soon = ring_z(soon)
+    ring_late = ring_z(late)
 
     payload, x = call(
         first_kernel,
-        [*pieces, norm_gain, carried, first_w, ring[1], ring[-1]],
+        [*pieces, norm_gain, carried, first_w],
         [shape((ND, SEQS, FIRST_PAY), bf16), shape((SEQS, COLS))],
         [pltpu.VMEM((NY, ROWS, COLS), f32)],
     )
     got = lax.all_to_all(payload, DP, 0, 0, tiled=True)
     out, u0 = call(
         mid_kernel,
-        [got, first_w],
+        [got, *ring_soon],
         [shape((SEQS, 2 * COLS)), shape((SEQS, BLOCK))],
         [BLOCKS, *GATED],
     )
@@ -374,7 +377,7 @@
     u0 = turn(u0, back=True)
     payload, x = call(
         next_kernel,
-        [out, *others, x, norm_gain, carried, *ring],
+        [out, *others, x, norm_gain, carried, *ring_soon],
         [shape((ND, SEQS, NEXT_PAY), bf16), shape((SEQS, COLS))],
         [BLOCKS],
     )
@@ -385,7 +388,7 @@
     u1 = turn(u1, back=True)
     own, s1, s2, s3 = call(
         last_kernel,
-        [got, u, *ring],
+        [got, u, *ring_late],
         [shape((ROWS, 2 * COLS))] * NY,
         [*GATED, pltpu.VMEM((NY, ROWS, 2 * COLS), f32)],
     )

time: 98.3 us -> 112 us (1.14)
  starting transfers between devices: 51.4 us -> 65.3 us
    ppermute x7 -> x14, starting transfers between devices: 15.2 us -> 28.9 us  [shift_z(): return lax.ppermute(value, 'z', [(i, (i + k) % NZ) for i in range(NZ)])]
    ppermute x7 -> x14, waiting for transfers between devices: 5.14 us -> 15.1 us  [shift_z(): return lax.ppermute(value, 'z', [(i, (i + k) % NZ) for i in range(NZ)])]
    ppermute x3, waiting for transfers between devices: 26.1 us -> 17.7 us  [turn(): return lax.ppermute(value, ALL, pairs)]
    all_to_all x2, starting transfers between devices: 11.5 us -> 10.2 us  [both_layers(): got = lax.all_to_all(payload, DP, 0, 0, tiled=True)]
    ppermute x9, waiting for transfers between devices: 5.59 us -> 4.33 us  [shift_y(): return lax.ppermute(value, 'y', [(i, (i + k) % NY) for i in range(NY)])]
  transfers between devices with their start and end apart: 22 -> 29, of which waited for: 10 -> 11; matrix products, arithmetic and copies ran while one was open for 0% -> 0% of each run, Pallas kernels for 3% -> 2%
where the time goes in v3:
time: 112 us
  starting transfers between devices  65.3 us (58%)
  waiting for transfers between devices  37.2 us (33%)
  Pallas kernels  7.95 us (7%)
    ppermute x14, starting transfers between devices, shift_z(): return lax.ppermute(value, 'z', [(i, (i + k) % NZ) for i in range(NZ)])  28.9 us
    ppermute x3, waiting for transfers between devices, turn(): return lax.ppermute(value, ALL, pairs)  17.7 us
    ppermute x9, starting transfers between devices, shift_y(): return lax.ppermute(value, 'y', [(i, (i + k) % NY) for i in range(NY)])  15.7 us
    ppermute x14, waiting for transfers between devices, shift_z(): return lax.ppermute(value, 'z', [(i, (i + k) % NZ) for i in range(NZ)])  15.1 us
    all_to_all x2, starting transfers between devices, both_layers(): got = lax.all_to_all(payload, DP, 0, 0, tiled=True)  10.2 us
    pallas_call x9, Pallas kernels, call(): pl.pallas_call(body, in_specs=[pl.BlockSpec(memory_space=s) for s in spac...  7.95 us
    all_to_all x1, starting transfers between devices, both_layers(): first_w = lax.all_to_all(packed, 'z', 0, 0, tiled=True)  7.8 us
    ppermute x9, waiting for transfers between devices, shift_y(): return lax.ppermute(value, 'y', [(i, (i + k) % NY) for i in range(NY)])  4.33 us
  transfers between devices with their start and end apart: 29, of which 11 were waited for; matrix products, arithmetic and copies ran while one was open for 0% of the time, Pallas kernels for 2%

profile of v3, /device:TPU:110, one launch (start us, length us, event | category | flops | bytes accessed | tf_op | source)
XLA Modules:
  0.0 112.0 jit_solution(2268052961042240626)
XLA Ops:
  2.3 7.8 %all-to-all-start = ((bf16[8,64,256]{2,1,0:T(8,128)(2,1)}), bf16[8,64,256]{2,1,0:T(8,128)(2,1)S(1)}, u32[]{:S(2)}, u32[]{:S(2)}) async-start(bf16[8,64,256]{2,1,0:T(8,128)(2,1)} %get-tuple-element.21), calls=%async_computation | async-start | bytes 524288 | tf_op jit(solution)/shard_map/all_to_all | solution.py:334
  12.1 2.7 %collective-permute-start.3 = (f32[128,64]{1,0:T(8,128)S(1)}, f32[128,64]{1,0:T(8,128)S(1)}, u32[]{:S(2)}, u32[]{:S(2)}) collective-permute-start(f32[128,64]{1,0:T(8,128)S(1)} %get-tuple-element.20), channel_id=1, source_target_pairs={{0,5},{32,7},{64,3},{96,1},{128,0},{160,2},{192,6},{224,4},{8,13},... | collective-permute-start | bytes 98312 | tf_op jit(solution)/shard_map/ppermute | solution.py:45
  17.2 2.4 %collective-permute-start.2 = (bf16[8,256]{1,0:T(8,128)(2,1)S(1)}, bf16[8,256]{1,0:T(8,128)(2,1)S(1)}, u32[]{:S(2)}, u32[]{:S(2)}) collective-permute-start(bf16[8,256]{1,0:T(8,128)(2,1)S(1)} %copy-done.11), channel_id=1, source_target_pairs={{0,24},{8,0},{16,8},{24,16},{1,25},{9,1},{17,9},{25,17},{2,26},{10... | collective-permute-start | bytes 12296 | tf_op jit(solution)/shard_map/ppermute | solution.py:49
  22.5 5.4 %all-to-all-start.1 = ((bf16[8,32,1024]{2,1,0:T(8,128)(2,1)}), bf16[8,32,1024]{2,1,0:T(8,128)(2,1)S(1)}, u32[]{:S(2)}, u32[]{:S(2)}) async-start(bf16[8,32,1024]{2,1,0:T(8,128)(2,1)} %get-tuple-element.22), calls=%async_computation.1 | async-start | bytes 1048576 | tf_op jit(solution)/shard_map/all_to_all | solution.py:369
  28.0 3.6 %collective-permute-start.4 = (bf16[64,768]{1,0:T(8,128)(2,1)S(1)}, bf16[64,768]{1,0:T(8,128)(2,1)S(1)}, u32[]{:S(2)}, u32[]{:S(2)}) collective-permute-start(bf16[64,768]{1,0:T(8,128)(2,1)S(1)} %copy-done), channel_id=1, source_target_pairs={{0,32},{32,64},{64,96},{96,128},{128,160},{160,192},{192,224},{224... | collective-permute-start | bytes 294920 | tf_op jit(solution)/shard_map/ppermute | solution.py:53
  31.6 2.3 %collective-permute-done.4.refs_1_ = bf16[64,768]{1,0:T(8,128)(2,1)S(1)} collective-permute-done((bf16[64,768]{1,0:T(8,128)(2,1)S(1)}, bf16[64,768]{1,0:T(8,128)(2,1)S(1)}, u32[]{:S(2)}, u32[]{:S(2)}) %collective-permute-start.4) | collective-permute-done | bytes 98336 | tf_op jit(solution)/shard_map/ppermute | solution.py:53
  33.9 3.7 %collective-permute-start.5 = (bf16[64,768]{1,0:T(8,128)(2,1)S(1)}, bf16[64,768]{1,0:T(8,128)(2,1)S(1)}, u32[]{:S(2)}, u32[]{:S(2)}) collective-permute-start(bf16[64,768]{1,0:T(8,128)(2,1)S(1)} %collective-permute-done.4.refs_1_), channel_id=1, source_target_pairs={{0,32},{32,64},{64,96},{96,128},{128,160},{160,192},{192,224},{224... | collective-permute-start | bytes 294920 | tf_op jit(solution)/shard_map/ppermute | solution.py:53
  37.6 2.2 %collective-permute-done.5.refs_2_ = bf16[64,768]{1,0:T(8,128)(2,1)S(1)} collective-permute-done((bf16[64,768]{1,0:T(8,128)(2,1)S(1)}, bf16[64,768]{1,0:T(8,128)(2,1)S(1)}, u32[]{:S(2)}, u32[]{:S(2)}) %collective-permute-start.5) | collective-permute-done | bytes 98336 | tf_op jit(solution)/shard_map/ppermute | solution.py:53
  39.8 3.6 %collective-permute-start.6 = (bf16[64,768]{1,0:T(8,128)(2,1)S(1)}, bf16[64,768]{1,0:T(8,128)(2,1)S(1)}, u32[]{:S(2)}, u32[]{:S(2)}) collective-permute-start(bf16[64,768]{1,0:T(8,128)(2,1)S(1)} %collective-permute-done.5.refs_2_), channel_id=1, source_target_pairs={{0,32},{32,64},{64,96},{96,128},{128,160},{160,192},{192,224},{224... | collective-permute-start | bytes 294920 | tf_op jit(solution)/shard_map/ppermute | solution.py:53
  43.5 2.2 %collective-permute-done.6.refs_3_ = bf16[64,768]{1,0:T(8,128)(2,1)S(1)} collective-permute-done((bf16[64,768]{1,0:T(8,128)(2,1)S(1)}, bf16[64,768]{1,0:T(8,128)(2,1)S(1)}, u32[]{:S(2)}, u32[]{:S(2)}) %collective-permute-start.6) | collective-permute-done | bytes 98336 | tf_op jit(solution)/shard_map/ppermute | solution.py:53
  45.7 3.6 %collective-permute-start.7 = (bf16[64,768]{1,0:T(8,128)(2,1)S(1)}, bf16[64,768]{1,0:T(8,128)(2,1)S(1)}, u32[]{:S(2)}, u32[]{:S(2)}) collective-permute-start(bf16[64,768]{1,0:T(8,128)(2,1)S(1)} %collective-permute-done.6.refs_3_), channel_id=1, source_target_pairs={{0,32},{32,64},{64,96},{96,128},{128,160},{160,192},{192,224},{224... | collective-permute-start | bytes 294920 | tf_op jit(solution)/shard_map/ppermute | solution.py:53
  49.3 2.2 %collective-permute-done.7.refs_4_ = bf16[64,768]{1,0:T(8,128)(2,1)S(1)} collective-permute-done((bf16[64,768]{1,0:T(8,128)(2,1)S(1)}, bf16[64,768]{1,0:T(8,128)(2,1)S(1)}, u32[]{:S(2)}, u32[]{:S(2)}) %collective-permute-start.7) | collective-permute-done | bytes 98336 | tf_op jit(solution)/shard_map/ppermute | solution.py:53
  54.7 2.4 %collective-permute-start.13 = (f32[32,512]{1,0:T(8,128)S(1)}, f32[32,512]{1,0:T(8,128)S(1)}, u32[]{:S(2)}, u32[]{:S(2)}) collective-permute-start(f32[32,512]{1,0:T(8,128)S(1)} %get-tuple-element.24.out), channel_id=1, source_target_pairs={{0,24},{8,0},{16,8},{24,16},{1,25},{9,1},{17,9},{25,17},{2,26},{10... | collective-permute-start | bytes 196616 | tf_op jit(solution)/shard_map/ppermute | solution.py:49
  57.1 2.5 %collective-permute-done.12.r2 = f32[32,512]{1,0:T(8,128)S(1)} collective-permute-done((f32[32,512]{1,0:T(8,128)S(1)}, f32[32,512]{1,0:T(8,128)S(1)}, u32[]{:S(2)}, u32[]{:S(2)}) %collective-permute-start.12) | collective-permute-done | bytes 65568 | tf_op jit(solution)/shard_map/ppermute | solution.py:49
  60.7 4.8 %all-to-all-start.2 = ((bf16[8,32,768]{2,1,0:T(8,128)(2,1)}), bf16[8,32,768]{2,1,0:T(8,128)(2,1)S(1)}, u32[]{:S(2)}, u32[]{:S(2)}) async-start(bf16[8,32,768]{2,1,0:T(8,128)(2,1)} %get-tuple-element.26), calls=%async_computation.2 | async-start | bytes 786432 | tf_op jit(solution)/shard_map/all_to_all | solution.py:384
  65.5 3.6 %collective-permute-start.15 = (bf16[64,640]{1,0:T(8,128)(2,1)S(1)}, bf16[64,640]{1,0:T(8,128)(2,1)S(1)}, u32[]{:S(2)}, u32[]{:S(2)}) collective-permute-start(bf16[64,640]{1,0:T(8,128)(2,1)S(1)} %get-tuple-element.29.refs_0_), channel_id=1, source_target_pairs={{0,32},{32,64},{64,96},{96,128},{128,160},{160,192},{192,224},{224... | collective-permute-start | bytes 245768 | tf_op jit(solution)/shard_map/ppermute | solution.py:53
  69.1 2.1 %collective-permute-done.15.refs_1_ = bf16[64,640]{1,0:T(8,128)(2,1)S(1)} collective-permute-done((bf16[64,640]{1,0:T(8,128)(2,1)S(1)}, bf16[64,640]{1,0:T(8,128)(2,1)S(1)}, u32[]{:S(2)}, u32[]{:S(2)}) %collective-permute-start.15) | collective-permute-done | bytes 81952 | tf_op jit(solution)/shard_map/ppermute | solution.py:53
  71.2 3.6 %collective-permute-start.16 = (bf16[64,640]{1,0:T(8,128)(2,1)S(1)}, bf16[64,640]{1,0:T(8,128)(2,1)S(1)}, u32[]{:S(2)}, u32[]{:S(2)}) collective-permute-start(bf16[64,640]{1,0:T(8,128)(2,1)S(1)} %collective-permute-done.15.refs_1_), channel_id=1, source_target_pairs={{0,32},{32,64},{64,96},{96,128},{128,160},{160,192},{192,224},{224... | collective-permute-start | bytes 245768 | tf_op jit(solution)/shard_map/ppermute | solution.py:53
  74.8 2.1 %collective-permute-done.16.refs_2_ = bf16[64,640]{1,0:T(8,128)(2,1)S(1)} collective-permute-done((bf16[64,640]{1,0:T(8,128)(2,1)S(1)}, bf16[64,640]{1,0:T(8,128)(2,1)S(1)}, u32[]{:S(2)}, u32[]{:S(2)}) %collective-permute-start.16) | collective-permute-done | bytes 81952 | tf_op jit(solution)/shard_map/ppermute | solution.py:53
  76.9 3.6 %collective-permute-start.17 = (bf16[64,640]{1,0:T(8,128)(2,1)S(1)}, bf16[64,640]{1,0:T(8,128)(2,1)S(1)}, u32[]{:S(2)}, u32[]{:S(2)}) collective-permute-start(bf16[64,640]{1,0:T(8,128)(2,1)S(1)} %collective-permute-done.16.refs_2_), channel_id=1, source_target_pairs={{0,32},{32,64},{64,96},{96,128},{128,160},{160,192},{192,224},{224... | collective-permute-start | bytes 245768 | tf_op jit(solution)/shard_map/ppermute | solution.py:53
  82.5 3.6 %collective-permute-start.18 = (bf16[64,640]{1,0:T(8,128)(2,1)S(1)}, bf16[64,640]{1,0:T(8,128)(2,1)S(1)}, u32[]{:S(2)}, u32[]{:S(2)}) collective-permute-start(bf16[64,640]{1,0:T(8,128)(2,1)S(1)} %collective-permute-done.17.refs_3_), channel_id=1, source_target_pairs={{0,32},{32,64},{64,96},{96,128},{128,160},{160,192},{192,224},{224... | collective-permute-start | bytes 245768 | tf_op jit(solution)/shard_map/ppermute | solution.py:53
  86.1 8.9 %collective-permute-done.14.earlier.u0 = f32[32,64]{1,0:T(8,128)S(1)} collective-permute-done((f32[32,64]{1,0:T(8,128)S(1)}, f32[32,64]{1,0:T(8,128)S(1)}, u32[]{:S(2)}, u32[]{:S(2)}) %collective-permute-start.14) | collective-permute-done | bytes 8224 | tf_op jit(solution)/shard_map/ppermute | solution.py:45
  96.9 2.6 %collective-permute-start.23 = (f32[8,512]{1,0:T(8,128)S(1)}, f32[8,512]{1,0:T(8,128)S(1)}, u32[]{:S(2)}, u32[]{:S(2)}) collective-permute-start(f32[8,512]{1,0:T(8,128)S(1)} %get-tuple-element.32), channel_id=1, source_target_pairs={{0,16},{8,24},{16,0},{24,8},{1,17},{9,25},{17,1},{25,9},{2,18},{10... | collective-permute-start | bytes 49160 | tf_op jit(solution)/shard_map/ppermute | solution.py:49
  101.5 8.9 %collective-permute-done.25.u1 = f32[32,64]{1,0:T(8,128)S(1)} collective-permute-done((f32[32,64]{1,0:T(8,128)S(1)}, f32[32,64]{1,0:T(8,128)S(1)}, u32[]{:S(2)}, u32[]{:S(2)}) %collective-permute-start.25) | collective-permute-done | bytes 8224 | tf_op jit(solution)/shard_map/ppermute | solution.py:45
  (71 shorter events, 20.8 us)
Async XLA Ops:
  2.3 19.1 %all-to-all-start = ((bf16[8,64,256]{2,1,0:T(8,128)(2,1)}), bf16[8,64,256]{2,1,0:T(8,128)(2,1)S(1)}, u32[]{:S(2)}, u32[]{:S(2)}) async-start(bf16[8,64,256]{2,1,0:T(8,128)(2,1)} %get-tuple-element.21), calls=%async_computation | async-start | bytes 524288 | tf_op jit(solution)/shard_map/all_to_all | solution.py:334
  12.1 9.4 %collective-permute-start.3 = (f32[128,64]{1,0:T(8,128)S(1)}, f32[128,64]{1,0:T(8,128)S(1)}, u32[]{:S(2)}, u32[]{:S(2)}) collective-permute-start(f32[128,64]{1,0:T(8,128)S(1)} %get-tuple-element.20), channel_id=1, source_target_pairs={{0,5},{32,7},{64,3},{96,1},{128,0},{160,2},{192,6},{224,4},{8,13},... | collective-permute-start | bytes 98312 | tf_op jit(solution)/shard_map/ppermute | solution.py:45
  22.5 28.9 %all-to-all-start.1 = ((bf16[8,32,1024]{2,1,0:T(8,128)(2,1)}), bf16[8,32,1024]{2,1,0:T(8,128)(2,1)S(1)}, u32[]{:S(2)}, u32[]{:S(2)}) async-start(bf16[8,32,1024]{2,1,0:T(8,128)(2,1)} %get-tuple-element.22), calls=%async_computation.1 | async-start | bytes 1048576 | tf_op jit(solution)/shard_map/all_to_all | solution.py:369
  28.0 5.9 %collective-permute-start.4 = (bf16[64,768]{1,0:T(8,128)(2,1)S(1)}, bf16[64,768]{1,0:T(8,128)(2,1)S(1)}, u32[]{:S(2)}, u32[]{:S(2)}) collective-permute-start(bf16[64,768]{1,0:T(8,128)(2,1)S(1)} %copy-done), channel_id=1, source_target_pairs={{0,32},{32,64},{64,96},{96,128},{128,160},{160,192},{192,224},{224... | collective-permute-start | bytes 294920 | tf_op jit(solution)/shard_map/ppermute | solution.py:53
  31.6 6.0 %collective-permute-start.8 = (bf16[64,768]{1,0:T(8,128)(2,1)S(1)}, bf16[64,768]{1,0:T(8,128)(2,1)S(1)}, u32[]{:S(2)}, u32[]{:S(2)}) collective-permute-start(bf16[64,768]{1,0:T(8,128)(2,1)S(1)} %copy-done), channel_id=1, source_target_pairs={{0,224},{32,0},{64,32},{96,64},{128,96},{160,128},{192,160},{224,1... | collective-permute-start | bytes 294920 | tf_op jit(solution)/shard_map/ppermute | solution.py:53
  33.9 5.9 %collective-permute-start.5 = (bf16[64,768]{1,0:T(8,128)(2,1)S(1)}, bf16[64,768]{1,0:T(8,128)(2,1)S(1)}, u32[]{:S(2)}, u32[]{:S(2)}) collective-permute-start(bf16[64,768]{1,0:T(8,128)(2,1)S(1)} %collective-permute-done.4.refs_1_), channel_id=1, source_target_pairs={{0,32},{32,64},{64,96},{96,128},{128,160},{160,192},{192,224},{224... | collective-permute-start | bytes 294920 | tf_op jit(solution)/shard_map/ppermute | solution.py:53
  37.6 5.8 %collective-permute-start.9 = (bf16[64,768]{1,0:T(8,128)(2,1)S(1)}, bf16[64,768]{1,0:T(8,128)(2,1)S(1)}, u32[]{:S(2)}, u32[]{:S(2)}) collective-permute-start(bf16[64,768]{1,0:T(8,128)(2,1)S(1)} %collective-permute-done.8.refs_7_), channel_id=1, source_target_pairs={{0,224},{32,0},{64,32},{96,64},{128,96},{160,128},{192,160},{224,1... | collective-permute-start | bytes 294920 | tf_op jit(solution)/shard_map/ppermute | solution.py:53
  39.8 5.8 %collective-permute-start.6 = (bf16[64,768]{1,0:T(8,128)(2,1)S(1)}, bf16[64,768]{1,0:T(8,128)(2,1)S(1)}, u32[]{:S(2)}, u32[]{:S(2)}) collective-permute-start(bf16[64,768]{1,0:T(8,128)(2,1)S(1)} %collective-permute-done.5.refs_2_), channel_id=1, source_target_pairs={{0,32},{32,64},{64,96},{96,128},{128,160},{160,192},{192,224},{224... | collective-permute-start | bytes 294920 | tf_op jit(solution)/shard_map/ppermute | solution.py:53
  43.4 5.8 %collective-permute-start.10 = (bf16[64,768]{1,0:T(8,128)(2,1)S(1)}, bf16[64,768]{1,0:T(8,128)(2,1)S(1)}, u32[]{:S(2)}, u32[]{:S(2)}) collective-permute-start(bf16[64,768]{1,0:T(8,128)(2,1)S(1)} %collective-permute-done.9.refs_6_), channel_id=1, source_target_pairs={{0,224},{32,0},{64,32},{96,64},{128,96},{160,128},{192,160},{224,1... | collective-permute-start | bytes 294920 | tf_op jit(solution)/shard_map/ppermute | solution.py:53
  45.7 5.8 %collective-permute-start.7 = (bf16[64,768]{1,0:T(8,128)(2,1)S(1)}, bf16[64,768]{1,0:T(8,128)(2,1)S(1)}, u32[]{:S(2)}, u32[]{:S(2)}) collective-permute-start(bf16[64,768]{1,0:T(8,128)(2,1)S(1)} %collective-permute-done.6.refs_3_), channel_id=1, source_target_pairs={{0,32},{32,64},{64,96},{96,128},{128,160},{160,192},{192,224},{224... | collective-permute-start | bytes 294920 | tf_op jit(solution)/shard_map/ppermute | solution.py:53
  53.7 5.9 %collective-permute-start.12 = (f32[32,512]{1,0:T(8,128)S(1)}, f32[32,512]{1,0:T(8,128)S(1)}, u32[]{:S(2)}, u32[]{:S(2)}) collective-permute-start(f32[32,512]{1,0:T(8,128)S(1)} %get-tuple-element.24.out), channel_id=1, source_target_pairs={{0,16},{8,24},{16,0},{24,8},{1,17},{9,25},{17,1},{25,9},{2,18},{10... | collective-permute-start | bytes 196616 | tf_op jit(solution)/shard_map/ppermute | solution.py:49
  60.7 34.2 %all-to-all-start.2 = ((bf16[8,32,768]{2,1,0:T(8,128)(2,1)}), bf16[8,32,768]{2,1,0:T(8,128)(2,1)S(1)}, u32[]{:S(2)}, u32[]{:S(2)}) async-start(bf16[8,32,768]{2,1,0:T(8,128)(2,1)} %get-tuple-element.26), calls=%async_computation.2 | async-start | bytes 786432 | tf_op jit(solution)/shard_map/all_to_all | solution.py:384
  65.5 5.7 %collective-permute-start.15 = (bf16[64,640]{1,0:T(8,128)(2,1)S(1)}, bf16[64,640]{1,0:T(8,128)(2,1)S(1)}, u32[]{:S(2)}, u32[]{:S(2)}) collective-permute-start(bf16[64,640]{1,0:T(8,128)(2,1)S(1)} %get-tuple-element.29.refs_0_), channel_id=1, source_target_pairs={{0,32},{32,64},{64,96},{96,128},{128,160},{160,192},{192,224},{224... | collective-permute-start | bytes 245768 | tf_op jit(solution)/shard_map/ppermute | solution.py:53
  69.1 5.7 %collective-permute-start.19 = (bf16[64,640]{1,0:T(8,128)(2,1)S(1)}, bf16[64,640]{1,0:T(8,128)(2,1)S(1)}, u32[]{:S(2)}, u32[]{:S(2)}) collective-permute-start(bf16[64,640]{1,0:T(8,128)(2,1)S(1)} %get-tuple-element.29.refs_0_), channel_id=1, source_target_pairs={{0,224},{32,0},{64,32},{96,64},{128,96},{160,128},{192,160},{224,1... | collective-permute-start | bytes 245768 | tf_op jit(solution)/shard_map/ppermute | solution.py:53
  71.2 5.7 %collective-permute-start.16 = (bf16[64,640]{1,0:T(8,128)(2,1)S(1)}, bf16[64,640]{1,0:T(8,128)(2,1)S(1)}, u32[]{:S(2)}, u32[]{:S(2)}) collective-permute-start(bf16[64,640]{1,0:T(8,128)(2,1)S(1)} %collective-permute-done.15.refs_1_), channel_id=1, source_target_pairs={{0,32},{32,64},{64,96},{96,128},{128,160},{160,192},{192,224},{224... | collective-permute-start | bytes 245768 | tf_op jit(solution)/shard_map/ppermute | solution.py:53
  74.8 5.7 %collective-permute-start.20 = (bf16[64,640]{1,0:T(8,128)(2,1)S(1)}, bf16[64,640]{1,0:T(8,128)(2,1)S(1)}, u32[]{:S(2)}, u32[]{:S(2)}) collective-permute-start(bf16[64,640]{1,0:T(8,128)(2,1)S(1)} %collective-permute-done.19.refs_7_), channel_id=1, source_target_pairs={{0,224},{32,0},{64,32},{96,64},{128,96},{160,128},{192,160},{224,1... | collective-permute-start | bytes 245768 | tf_op jit(solution)/shard_map/ppermute | solution.py:53
  76.9 5.7 %collective-permute-start.17 = (bf16[64,640]{1,0:T(8,128)(2,1)S(1)}, bf16[64,640]{1,0:T(8,128)(2,1)S(1)}, u32[]{:S(2)}, u32[]{:S(2)}) collective-permute-start(bf16[64,640]{1,0:T(8,128)(2,1)S(1)} %collective-permute-done.16.refs_2_), channel_id=1, source_target_pairs={{0,32},{32,64},{64,96},{96,128},{128,160},{160,192},{192,224},{224... | collective-permute-start | bytes 245768 | tf_op jit(solution)/shard_map/ppermute | solution.py:53
  80.4 14.7 %collective-permute-start.21 = (bf16[64,640]{1,0:T(8,128)(2,1)S(1)}, bf16[64,640]{1,0:T(8,128)(2,1)S(1)}, u32[]{:S(2)}, u32[]{:S(2)}) collective-permute-start(bf16[64,640]{1,0:T(8,128)(2,1)S(1)} %collective-permute-done.20.refs_6_), channel_id=1, source_target_pairs={{0,224},{32,0},{64,32},{96,64},{128,96},{160,128},{192,160},{224,1... | collective-permute-start | bytes 245768 | tf_op jit(solution)/shard_map/ppermute | solution.py:53
  82.5 12.6 %collective-permute-start.18 = (bf16[64,640]{1,0:T(8,128)(2,1)S(1)}, bf16[64,640]{1,0:T(8,128)(2,1)S(1)}, u32[]{:S(2)}, u32[]{:S(2)}) collective-permute-start(bf16[64,640]{1,0:T(8,128)(2,1)S(1)} %collective-permute-done.17.refs_3_), channel_id=1, source_target_pairs={{0,32},{32,64},{64,96},{96,128},{128,160},{160,192},{192,224},{224... | collective-permute-start | bytes 245768 | tf_op jit(solution)/shard_map/ppermute | solution.py:53
  86.1 8.9 %collective-permute-start.14 = (f32[32,64]{1,0:T(8,128)S(1)}, f32[32,64]{1,0:T(8,128)S(1)}, u32[]{:S(2)}, u32[]{:S(2)}) collective-permute-start(f32[32,64]{1,0:T(8,128)S(1)} %get-tuple-element.27), channel_id=1, source_target_pairs={{5,0},{7,32},{3,64},{1,96},{0,128},{2,160},{6,192},{4,224},{13,8},... | collective-permute-start | bytes 24584 | tf_op jit(solution)/shard_map/ppermute | solution.py:45
  95.7 15.7 %collective-permute-start.22 = (f32[8,512]{1,0:T(8,128)S(1)}, f32[8,512]{1,0:T(8,128)S(1)}, u32[]{:S(2)}, u32[]{:S(2)}) collective-permute-start(f32[8,512]{1,0:T(8,128)S(1)} %get-tuple-element.31), channel_id=1, source_target_pairs={{0,8},{8,16},{16,24},{24,0},{1,9},{9,17},{17,25},{25,1},{2,10},{10... | collective-permute-start | bytes 49160 | tf_op jit(solution)/shard_map/ppermute | solution.py:49
  96.9 14.5 %collective-permute-start.23 = (f32[8,512]{1,0:T(8,128)S(1)}, f32[8,512]{1,0:T(8,128)S(1)}, u32[]{:S(2)}, u32[]{:S(2)}) collective-permute-start(f32[8,512]{1,0:T(8,128)S(1)} %get-tuple-element.32), channel_id=1, source_target_pairs={{0,16},{8,24},{16,0},{24,8},{1,17},{9,25},{17,1},{25,9},{2,18},{10... | collective-permute-start | bytes 49160 | tf_op jit(solution)/shard_map/ppermute | solution.py:49
  99.6 11.8 %collective-permute-start.24 = (f32[8,512]{1,0:T(8,128)S(1)}, f32[8,512]{1,0:T(8,128)S(1)}, u32[]{:S(2)}, u32[]{:S(2)}) collective-permute-start(f32[8,512]{1,0:T(8,128)S(1)} %get-tuple-element.33), channel_id=1, source_target_pairs={{0,24},{8,0},{16,8},{24,16},{1,25},{9,1},{17,9},{25,17},{2,26},{10... | collective-permute-start | bytes 49160 | tf_op jit(solution)/shard_map/ppermute | solution.py:49
  101.5 8.9 %collective-permute-start.25 = (f32[32,64]{1,0:T(8,128)S(1)}, f32[32,64]{1,0:T(8,128)S(1)}, u32[]{:S(2)}, u32[]{:S(2)}) collective-permute-start(f32[32,64]{1,0:T(8,128)S(1)} %get-tuple-element.37), channel_id=1, source_target_pairs={{5,0},{7,32},{3,64},{1,96},{0,128},{2,160},{6,192},{4,224},{13,8},... | collective-permute-start | bytes 24584 | tf_op jit(solution)/shard_map/ppermute | solution.py:45
  (19 other events, 127.1 us)

commit v4 on v3

--- a/solution.py
+++ b/solution.py
@@ -247,7 +247,7 @@
     out[...] = gated(got, u_blocks, w, ordered, weights)
 
 
-def inputs_kernel(got, earlier, u_blocks, own_u):
+def inputs_kernel(got, u_blocks, own_u):
     split_blocks(inputs_of(got), u_blocks)
     own_u[...] = own_block(u_blocks)
 
@@ -332,7 +332,8 @@
         space=pl.ANY,
     )
     first_w = lax.all_to_all(packed, "z", 0, 0, tiled=True)
-    pieces = [stream] + [shift_y(stream, k) for k in range(1, NY)]
+    after, before = shift_y(stream, 1), shift_y(stream, -1)
+    pieces = [stream, after, shift_y(after, 1), before]
     base, drive, own, late = call(
         prep_kernel,
         [
@@ -383,7 +384,7 @@
     )
     got = lax.all_to_all(payload, DP, 0, 0, tiled=True)
     u, u1 = call(
-        inputs_kernel, [got, u0], [shape((NZ, SEQS, BLOCK)), shape((SEQS, BLOCK))]
+        inputs_kernel, [got], [shape((NZ, SEQS, BLOCK)), shape((SEQS, BLOCK))]
     )
     u1 = turn(u1, back=True)
     own, s1, s2, s3 = call(

time: 112 us -> 109 us (0.973)
  the two profiles are of different devices: /device:TPU:110 before, /device:TPU:12 now
where the time goes in v4:
time: 109 us
  starting transfers between devices  57.2 us (52%)
  waiting for transfers between devices  42.2 us (39%)
  Pallas kernels  7.96 us (7%)
    ppermute x14, waiting for transfers between devices, shift_z(): return lax.ppermute(value, 'z', [(i, (i + k) % NZ) for i in range(NZ)])  26.5 us
    ppermute x14, starting transfers between devices, shift_z(): return lax.ppermute(value, 'z', [(i, (i + k) % NZ) for i in range(NZ)])  19.4 us
    ppermute x9, starting transfers between devices, shift_y(): return lax.ppermute(value, 'y', [(i, (i + k) % NY) for i in range(NY)])  13.4 us
    all_to_all x2, starting transfers between devices, both_layers(): got = lax.all_to_all(payload, DP, 0, 0, tiled=True)  9.74 us
    all_to_all x1, starting transfers between devices, both_layers(): first_w = lax.all_to_all(packed, 'z', 0, 0, tiled=True)  8.61 us
    pallas_call x9, Pallas kernels, call(): pl.pallas_call(body, in_specs=[pl.BlockSpec(memory_space=s) for s in spac...  7.96 us
    ppermute x9, waiting for transfers between devices, shift_y(): return lax.ppermute(value, 'y', [(i, (i + k) % NY) for i in range(NY)])  7.88 us
    ppermute x3, waiting for transfers between devices, turn(): return lax.ppermute(value, ALL, pairs)  7.76 us
  transfers between devices with their start and end apart: 29, of which 15 were waited for; matrix products, arithmetic and copies ran while one was open for 0% of the time, Pallas kernels for 2%

profile of v4, /device:TPU:12, one launch (start us, length us, event | category | flops | bytes accessed | tf_op | source)
XLA Modules:
  0.0 108.8 jit_solution(7130951187288803141)
XLA Ops:
  2.3 8.6 %all-to-all-start = ((bf16[8,64,256]{2,1,0:T(8,128)(2,1)}), bf16[8,64,256]{2,1,0:T(8,128)(2,1)S(1)}, u32[]{:S(2)}, u32[]{:S(2)}) async-start(bf16[8,64,256]{2,1,0:T(8,128)(2,1)} %get-tuple-element.21), calls=%async_computation | async-start | bytes 524288 | tf_op jit(solution)/shard_map/all_to_all | solution.py:334
  12.9 6.0 %collective-permute-start.3 = (f32[128,64]{1,0:T(8,128)S(1)}, f32[128,64]{1,0:T(8,128)S(1)}, u32[]{:S(2)}, u32[]{:S(2)}) collective-permute-start(f32[128,64]{1,0:T(8,128)S(1)} %get-tuple-element.20), channel_id=1, source_target_pairs={{0,5},{32,7},{64,3},{96,1},{128,0},{160,2},{192,6},{224,4},{8,13},... | collective-permute-start | bytes 98312 | tf_op jit(solution)/shard_map/ppermute | solution.py:45
  24.1 2.0 %collective-permute-done.1.p2 = bf16[8,256]{1,0:T(8,128)(2,1)S(1)} collective-permute-done((bf16[8,256]{1,0:T(8,128)(2,1)S(1)}, bf16[8,256]{1,0:T(8,128)(2,1)S(1)}, u32[]{:S(2)}, u32[]{:S(2)}) %collective-permute-start.1) | collective-permute-done | bytes 4128 | tf_op jit(solution)/shard_map/ppermute | solution.py:49
  27.2 4.9 %all-to-all-start.1 = ((bf16[8,32,1024]{2,1,0:T(8,128)(2,1)}), bf16[8,32,1024]{2,1,0:T(8,128)(2,1)S(1)}, u32[]{:S(2)}, u32[]{:S(2)}) async-start(bf16[8,32,1024]{2,1,0:T(8,128)(2,1)} %get-tuple-element.22), calls=%async_computation.1 | async-start | bytes 1048576 | tf_op jit(solution)/shard_map/all_to_all | solution.py:370
  33.3 2.0 %collective-permute-start.8 = (bf16[64,768]{1,0:T(8,128)(2,1)S(1)}, bf16[64,768]{1,0:T(8,128)(2,1)S(1)}, u32[]{:S(2)}, u32[]{:S(2)}) collective-permute-start(bf16[64,768]{1,0:T(8,128)(2,1)S(1)} %copy-done), channel_id=1, source_target_pairs={{0,224},{32,0},{64,32},{96,64},{128,96},{160,128},{192,160},{224,1... | collective-permute-start | bytes 294920 | tf_op jit(solution)/shard_map/ppermute | solution.py:53
  35.4 2.8 %collective-permute-done.4.refs_1_ = bf16[64,768]{1,0:T(8,128)(2,1)S(1)} collective-permute-done((bf16[64,768]{1,0:T(8,128)(2,1)S(1)}, bf16[64,768]{1,0:T(8,128)(2,1)S(1)}, u32[]{:S(2)}, u32[]{:S(2)}) %collective-permute-start.4) | collective-permute-done | bytes 98336 | tf_op jit(solution)/shard_map/ppermute | solution.py:53
  38.2 3.2 %collective-permute-start.9 = (bf16[64,768]{1,0:T(8,128)(2,1)S(1)}, bf16[64,768]{1,0:T(8,128)(2,1)S(1)}, u32[]{:S(2)}, u32[]{:S(2)}) collective-permute-start(bf16[64,768]{1,0:T(8,128)(2,1)S(1)} %collective-permute-done.8.refs_7_), channel_id=1, source_target_pairs={{0,224},{32,0},{64,32},{96,64},{128,96},{160,128},{192,160},{224,1... | collective-permute-start | bytes 294920 | tf_op jit(solution)/shard_map/ppermute | solution.py:53
  41.4 2.6 %collective-permute-done.5.refs_2_ = bf16[64,768]{1,0:T(8,128)(2,1)S(1)} collective-permute-done((bf16[64,768]{1,0:T(8,128)(2,1)S(1)}, bf16[64,768]{1,0:T(8,128)(2,1)S(1)}, u32[]{:S(2)}, u32[]{:S(2)}) %collective-permute-start.5) | collective-permute-done | bytes 98336 | tf_op jit(solution)/shard_map/ppermute | solution.py:53
  44.0 3.2 %collective-permute-start.10 = (bf16[64,768]{1,0:T(8,128)(2,1)S(1)}, bf16[64,768]{1,0:T(8,128)(2,1)S(1)}, u32[]{:S(2)}, u32[]{:S(2)}) collective-permute-start(bf16[64,768]{1,0:T(8,128)(2,1)S(1)} %collective-permute-done.9.refs_6_), channel_id=1, source_target_pairs={{0,224},{32,0},{64,32},{96,64},{128,96},{160,128},{192,160},{224,1... | collective-permute-start | bytes 294920 | tf_op jit(solution)/shard_map/ppermute | solution.py:53
  47.2 2.6 %collective-permute-done.6.refs_3_ = bf16[64,768]{1,0:T(8,128)(2,1)S(1)} collective-permute-done((bf16[64,768]{1,0:T(8,128)(2,1)S(1)}, bf16[64,768]{1,0:T(8,128)(2,1)S(1)}, u32[]{:S(2)}, u32[]{:S(2)}) %collective-permute-start.6) | collective-permute-done | bytes 98336 | tf_op jit(solution)/shard_map/ppermute | solution.py:53
  49.8 5.8 %collective-permute-done.7.refs_4_ = bf16[64,768]{1,0:T(8,128)(2,1)S(1)} collective-permute-done((bf16[64,768]{1,0:T(8,128)(2,1)S(1)}, bf16[64,768]{1,0:T(8,128)(2,1)S(1)}, u32[]{:S(2)}, u32[]{:S(2)}) %collective-permute-start.7) | collective-permute-done | bytes 98336 | tf_op jit(solution)/shard_map/ppermute | solution.py:53
  57.9 3.4 %collective-permute-start.12 = (f32[32,512]{1,0:T(8,128)S(1)}, f32[32,512]{1,0:T(8,128)S(1)}, u32[]{:S(2)}, u32[]{:S(2)}) collective-permute-start(f32[32,512]{1,0:T(8,128)S(1)} %get-tuple-element.24.out), channel_id=1, source_target_pairs={{0,16},{8,24},{16,0},{24,8},{1,17},{9,25},{17,1},{25,9},{2,18},{10... | collective-permute-start | bytes 196616 | tf_op jit(solution)/shard_map/ppermute | solution.py:49
  61.4 2.2 %collective-permute-done.12.r2 = f32[32,512]{1,0:T(8,128)S(1)} collective-permute-done((f32[32,512]{1,0:T(8,128)S(1)}, f32[32,512]{1,0:T(8,128)S(1)}, u32[]{:S(2)}, u32[]{:S(2)}) %collective-permute-start.12) | collective-permute-done | bytes 65568 | tf_op jit(solution)/shard_map/ppermute | solution.py:49
  66.6 4.8 %all-to-all-start.2 = ((bf16[8,32,768]{2,1,0:T(8,128)(2,1)}), bf16[8,32,768]{2,1,0:T(8,128)(2,1)S(1)}, u32[]{:S(2)}, u32[]{:S(2)}) async-start(bf16[8,32,768]{2,1,0:T(8,128)(2,1)} %get-tuple-element.26), calls=%async_computation.2 | async-start | bytes 786432 | tf_op jit(solution)/shard_map/all_to_all | solution.py:385
  71.4 3.2 %collective-permute-start.18 = (bf16[64,640]{1,0:T(8,128)(2,1)S(1)}, bf16[64,640]{1,0:T(8,128)(2,1)S(1)}, u32[]{:S(2)}, u32[]{:S(2)}) collective-permute-start(bf16[64,640]{1,0:T(8,128)(2,1)S(1)} %get-tuple-element.28.refs_0_), channel_id=1, source_target_pairs={{0,224},{32,0},{64,32},{96,64},{128,96},{160,128},{192,160},{224,1... | collective-permute-start | bytes 245768 | tf_op jit(solution)/shard_map/ppermute | solution.py:53
  74.6 2.4 %collective-permute-done.14.refs_1_ = bf16[64,640]{1,0:T(8,128)(2,1)S(1)} collective-permute-done((bf16[64,640]{1,0:T(8,128)(2,1)S(1)}, bf16[64,640]{1,0:T(8,128)(2,1)S(1)}, u32[]{:S(2)}, u32[]{:S(2)}) %collective-permute-start.14) | collective-permute-done | bytes 81952 | tf_op jit(solution)/shard_map/ppermute | solution.py:53
  77.1 3.2 %collective-permute-start.19 = (bf16[64,640]{1,0:T(8,128)(2,1)S(1)}, bf16[64,640]{1,0:T(8,128)(2,1)S(1)}, u32[]{:S(2)}, u32[]{:S(2)}) collective-permute-start(bf16[64,640]{1,0:T(8,128)(2,1)S(1)} %collective-permute-done.18.refs_7_), channel_id=1, source_target_pairs={{0,224},{32,0},{64,32},{96,64},{128,96},{160,128},{192,160},{224,1... | collective-permute-start | bytes 245768 | tf_op jit(solution)/shard_map/ppermute | solution.py:53
  80.3 2.4 %collective-permute-done.15.refs_2_ = bf16[64,640]{1,0:T(8,128)(2,1)S(1)} collective-permute-done((bf16[64,640]{1,0:T(8,128)(2,1)S(1)}, bf16[64,640]{1,0:T(8,128)(2,1)S(1)}, u32[]{:S(2)}, u32[]{:S(2)}) %collective-permute-start.15) | collective-permute-done | bytes 81952 | tf_op jit(solution)/shard_map/ppermute | solution.py:53
  82.7 3.2 %collective-permute-start.20 = (bf16[64,640]{1,0:T(8,128)(2,1)S(1)}, bf16[64,640]{1,0:T(8,128)(2,1)S(1)}, u32[]{:S(2)}, u32[]{:S(2)}) collective-permute-start(bf16[64,640]{1,0:T(8,128)(2,1)S(1)} %collective-permute-done.19.refs_6_), channel_id=1, source_target_pairs={{0,224},{32,0},{64,32},{96,64},{128,96},{160,128},{192,160},{224,1... | collective-permute-start | bytes 245768 | tf_op jit(solution)/shard_map/ppermute | solution.py:53
  86.0 2.4 %collective-permute-done.16.refs_3_ = bf16[64,640]{1,0:T(8,128)(2,1)S(1)} collective-permute-done((bf16[64,640]{1,0:T(8,128)(2,1)S(1)}, bf16[64,640]{1,0:T(8,128)(2,1)S(1)}, u32[]{:S(2)}, u32[]{:S(2)}) %collective-permute-start.16) | collective-permute-done | bytes 81952 | tf_op jit(solution)/shard_map/ppermute | solution.py:53
  88.6 5.5 %collective-permute-done.17.refs_4_ = bf16[64,640]{1,0:T(8,128)(2,1)S(1)} collective-permute-done((bf16[64,640]{1,0:T(8,128)(2,1)S(1)}, bf16[64,640]{1,0:T(8,128)(2,1)S(1)}, u32[]{:S(2)}, u32[]{:S(2)}) %collective-permute-start.17) | collective-permute-done | bytes 81952 | tf_op jit(solution)/shard_map/ppermute | solution.py:53
  94.7 2.8 %collective-permute-start.22 = (f32[8,512]{1,0:T(8,128)S(1)}, f32[8,512]{1,0:T(8,128)S(1)}, u32[]{:S(2)}, u32[]{:S(2)}) collective-permute-start(f32[8,512]{1,0:T(8,128)S(1)} %get-tuple-element.31), channel_id=1, source_target_pairs={{0,16},{8,24},{16,0},{24,8},{1,17},{9,25},{17,1},{25,9},{2,18},{10... | collective-permute-start | bytes 49160 | tf_op jit(solution)/shard_map/ppermute | solution.py:49
  97.4 1.9 %collective-permute-start.23 = (f32[8,512]{1,0:T(8,128)S(1)}, f32[8,512]{1,0:T(8,128)S(1)}, u32[]{:S(2)}, u32[]{:S(2)}) collective-permute-start(f32[8,512]{1,0:T(8,128)S(1)} %get-tuple-element.32), channel_id=1, source_target_pairs={{0,24},{8,0},{16,8},{24,16},{1,25},{9,1},{17,9},{25,17},{2,26},{10... | collective-permute-start | bytes 49160 | tf_op jit(solution)/shard_map/ppermute | solution.py:49
  99.4 7.6 %collective-permute-done.24.u0 = f32[32,64]{1,0:T(8,128)S(1)} collective-permute-done((f32[32,64]{1,0:T(8,128)S(1)}, f32[32,64]{1,0:T(8,128)S(1)}, u32[]{:S(2)}, u32[]{:S(2)}) %collective-permute-start.24) | collective-permute-done | bytes 8224 | tf_op jit(solution)/shard_map/ppermute | solution.py:45
  (71 shorter events, 19.0 us)
Async XLA Ops:
  2.3 23.7 %all-to-all-start = ((bf16[8,64,256]{2,1,0:T(8,128)(2,1)}), bf16[8,64,256]{2,1,0:T(8,128)(2,1)S(1)}, u32[]{:S(2)}, u32[]{:S(2)}) async-start(bf16[8,64,256]{2,1,0:T(8,128)(2,1)} %get-tuple-element.21), calls=%async_computation | async-start | bytes 524288 | tf_op jit(solution)/shard_map/all_to_all | solution.py:334
  12.9 13.2 %collective-permute-start.3 = (f32[128,64]{1,0:T(8,128)S(1)}, f32[128,64]{1,0:T(8,128)S(1)}, u32[]{:S(2)}, u32[]{:S(2)}) collective-permute-start(f32[128,64]{1,0:T(8,128)S(1)} %get-tuple-element.20), channel_id=1, source_target_pairs={{0,5},{32,7},{64,3},{96,1},{128,0},{160,2},{192,6},{224,4},{8,13},... | collective-permute-start | bytes 98312 | tf_op jit(solution)/shard_map/ppermute | solution.py:45
  27.2 28.5 %all-to-all-start.1 = ((bf16[8,32,1024]{2,1,0:T(8,128)(2,1)}), bf16[8,32,1024]{2,1,0:T(8,128)(2,1)S(1)}, u32[]{:S(2)}, u32[]{:S(2)}) async-start(bf16[8,32,1024]{2,1,0:T(8,128)(2,1)} %get-tuple-element.22), calls=%async_computation.1 | async-start | bytes 1048576 | tf_op jit(solution)/shard_map/all_to_all | solution.py:370
  32.1 6.0 %collective-permute-start.4 = (bf16[64,768]{1,0:T(8,128)(2,1)S(1)}, bf16[64,768]{1,0:T(8,128)(2,1)S(1)}, u32[]{:S(2)}, u32[]{:S(2)}) collective-permute-start(bf16[64,768]{1,0:T(8,128)(2,1)S(1)} %copy-done), channel_id=1, source_target_pairs={{0,32},{32,64},{64,96},{96,128},{128,160},{160,192},{192,224},{224... | collective-permute-start | bytes 294920 | tf_op jit(solution)/shard_map/ppermute | solution.py:53
  38.2 5.8 %collective-permute-start.5 = (bf16[64,768]{1,0:T(8,128)(2,1)S(1)}, bf16[64,768]{1,0:T(8,128)(2,1)S(1)}, u32[]{:S(2)}, u32[]{:S(2)}) collective-permute-start(bf16[64,768]{1,0:T(8,128)(2,1)S(1)} %collective-permute-done.4.refs_1_), channel_id=1, source_target_pairs={{0,32},{32,64},{64,96},{96,128},{128,160},{160,192},{192,224},{224... | collective-permute-start | bytes 294920 | tf_op jit(solution)/shard_map/ppermute | solution.py:53
  38.2 5.8 %collective-permute-start.9 = (bf16[64,768]{1,0:T(8,128)(2,1)S(1)}, bf16[64,768]{1,0:T(8,128)(2,1)S(1)}, u32[]{:S(2)}, u32[]{:S(2)}) collective-permute-start(bf16[64,768]{1,0:T(8,128)(2,1)S(1)} %collective-permute-done.8.refs_7_), channel_id=1, source_target_pairs={{0,224},{32,0},{64,32},{96,64},{128,96},{160,128},{192,160},{224,1... | collective-permute-start | bytes 294920 | tf_op jit(solution)/shard_map/ppermute | solution.py:53
  44.0 5.8 %collective-permute-start.6 = (bf16[64,768]{1,0:T(8,128)(2,1)S(1)}, bf16[64,768]{1,0:T(8,128)(2,1)S(1)}, u32[]{:S(2)}, u32[]{:S(2)}) collective-permute-start(bf16[64,768]{1,0:T(8,128)(2,1)S(1)} %collective-permute-done.5.refs_2_), channel_id=1, source_target_pairs={{0,32},{32,64},{64,96},{96,128},{128,160},{160,192},{192,224},{224... | collective-permute-start | bytes 294920 | tf_op jit(solution)/shard_map/ppermute | solution.py:53
  44.0 5.8 %collective-permute-start.10 = (bf16[64,768]{1,0:T(8,128)(2,1)S(1)}, bf16[64,768]{1,0:T(8,128)(2,1)S(1)}, u32[]{:S(2)}, u32[]{:S(2)}) collective-permute-start(bf16[64,768]{1,0:T(8,128)(2,1)S(1)} %collective-permute-done.9.refs_6_), channel_id=1, source_target_pairs={{0,224},{32,0},{64,32},{96,64},{128,96},{160,128},{192,160},{224,1... | collective-permute-start | bytes 294920 | tf_op jit(solution)/shard_map/ppermute | solution.py:53
  49.8 5.8 %collective-permute-start.7 = (bf16[64,768]{1,0:T(8,128)(2,1)S(1)}, bf16[64,768]{1,0:T(8,128)(2,1)S(1)}, u32[]{:S(2)}, u32[]{:S(2)}) collective-permute-start(bf16[64,768]{1,0:T(8,128)(2,1)S(1)} %collective-permute-done.6.refs_3_), channel_id=1, source_target_pairs={{0,32},{32,64},{64,96},{96,128},{128,160},{160,192},{192,224},{224... | collective-permute-start | bytes 294920 | tf_op jit(solution)/shard_map/ppermute | solution.py:53
  56.3 5.1 %collective-permute-start.11 = (f32[32,512]{1,0:T(8,128)S(1)}, f32[32,512]{1,0:T(8,128)S(1)}, u32[]{:S(2)}, u32[]{:S(2)}) collective-permute-start(f32[32,512]{1,0:T(8,128)S(1)} %get-tuple-element.24.out), channel_id=1, source_target_pairs={{0,8},{8,16},{16,24},{24,0},{1,9},{9,17},{17,25},{25,1},{2,10},{10... | collective-permute-start | bytes 196616 | tf_op jit(solution)/shard_map/ppermute | solution.py:49
  57.9 5.8 %collective-permute-start.12 = (f32[32,512]{1,0:T(8,128)S(1)}, f32[32,512]{1,0:T(8,128)S(1)}, u32[]{:S(2)}, u32[]{:S(2)}) collective-permute-start(f32[32,512]{1,0:T(8,128)S(1)} %get-tuple-element.24.out), channel_id=1, source_target_pairs={{0,16},{8,24},{16,0},{24,8},{1,17},{9,25},{17,1},{25,9},{2,18},{10... | collective-permute-start | bytes 196616 | tf_op jit(solution)/shard_map/ppermute | solution.py:49
  66.6 21.8 %all-to-all-start.2 = ((bf16[8,32,768]{2,1,0:T(8,128)(2,1)}), bf16[8,32,768]{2,1,0:T(8,128)(2,1)S(1)}, u32[]{:S(2)}, u32[]{:S(2)}) async-start(bf16[8,32,768]{2,1,0:T(8,128)(2,1)} %get-tuple-element.26), calls=%async_computation.2 | async-start | bytes 786432 | tf_op jit(solution)/shard_map/all_to_all | solution.py:385
  71.4 5.7 %collective-permute-start.14 = (bf16[64,640]{1,0:T(8,128)(2,1)S(1)}, bf16[64,640]{1,0:T(8,128)(2,1)S(1)}, u32[]{:S(2)}, u32[]{:S(2)}) collective-permute-start(bf16[64,640]{1,0:T(8,128)(2,1)S(1)} %get-tuple-element.28.refs_0_), channel_id=1, source_target_pairs={{0,32},{32,64},{64,96},{96,128},{128,160},{160,192},{192,224},{224... | collective-permute-start | bytes 245768 | tf_op jit(solution)/shard_map/ppermute | solution.py:53
  71.4 5.7 %collective-permute-start.18 = (bf16[64,640]{1,0:T(8,128)(2,1)S(1)}, bf16[64,640]{1,0:T(8,128)(2,1)S(1)}, u32[]{:S(2)}, u32[]{:S(2)}) collective-permute-start(bf16[64,640]{1,0:T(8,128)(2,1)S(1)} %get-tuple-element.28.refs_0_), channel_id=1, source_target_pairs={{0,224},{32,0},{64,32},{96,64},{128,96},{160,128},{192,160},{224,1... | collective-permute-start | bytes 245768 | tf_op jit(solution)/shard_map/ppermute | solution.py:53
  77.1 5.7 %collective-permute-start.15 = (bf16[64,640]{1,0:T(8,128)(2,1)S(1)}, bf16[64,640]{1,0:T(8,128)(2,1)S(1)}, u32[]{:S(2)}, u32[]{:S(2)}) collective-permute-start(bf16[64,640]{1,0:T(8,128)(2,1)S(1)} %collective-permute-done.14.refs_1_), channel_id=1, source_target_pairs={{0,32},{32,64},{64,96},{96,128},{128,160},{160,192},{192,224},{224... | collective-permute-start | bytes 245768 | tf_op jit(solution)/shard_map/ppermute | solution.py:53
  77.1 5.7 %collective-permute-start.19 = (bf16[64,640]{1,0:T(8,128)(2,1)S(1)}, bf16[64,640]{1,0:T(8,128)(2,1)S(1)}, u32[]{:S(2)}, u32[]{:S(2)}) collective-permute-start(bf16[64,640]{1,0:T(8,128)(2,1)S(1)} %collective-permute-done.18.refs_7_), channel_id=1, source_target_pairs={{0,224},{32,0},{64,32},{96,64},{128,96},{160,128},{192,160},{224,1... | collective-permute-start | bytes 245768 | tf_op jit(solution)/shard_map/ppermute | solution.py:53
  82.7 5.7 %collective-permute-start.16 = (bf16[64,640]{1,0:T(8,128)(2,1)S(1)}, bf16[64,640]{1,0:T(8,128)(2,1)S(1)}, u32[]{:S(2)}, u32[]{:S(2)}) collective-permute-start(bf16[64,640]{1,0:T(8,128)(2,1)S(1)} %collective-permute-done.15.refs_2_), channel_id=1, source_target_pairs={{0,32},{32,64},{64,96},{96,128},{128,160},{160,192},{192,224},{224... | collective-permute-start | bytes 245768 | tf_op jit(solution)/shard_map/ppermute | solution.py:53
  82.7 5.8 %collective-permute-start.20 = (bf16[64,640]{1,0:T(8,128)(2,1)S(1)}, bf16[64,640]{1,0:T(8,128)(2,1)S(1)}, u32[]{:S(2)}, u32[]{:S(2)}) collective-permute-start(bf16[64,640]{1,0:T(8,128)(2,1)S(1)} %collective-permute-done.19.refs_6_), channel_id=1, source_target_pairs={{0,224},{32,0},{64,32},{96,64},{128,96},{160,128},{192,160},{224,1... | collective-permute-start | bytes 245768 | tf_op jit(solution)/shard_map/ppermute | solution.py:53
  88.4 5.7 %collective-permute-start.17 = (bf16[64,640]{1,0:T(8,128)(2,1)S(1)}, bf16[64,640]{1,0:T(8,128)(2,1)S(1)}, u32[]{:S(2)}, u32[]{:S(2)}) collective-permute-start(bf16[64,640]{1,0:T(8,128)(2,1)S(1)} %collective-permute-done.16.refs_3_), channel_id=1, source_target_pairs={{0,32},{32,64},{64,96},{96,128},{128,160},{160,192},{192,224},{224... | collective-permute-start | bytes 245768 | tf_op jit(solution)/shard_map/ppermute | solution.py:53
  94.6 13.6 %collective-permute-start.21 = (f32[8,512]{1,0:T(8,128)S(1)}, f32[8,512]{1,0:T(8,128)S(1)}, u32[]{:S(2)}, u32[]{:S(2)}) collective-permute-start(f32[8,512]{1,0:T(8,128)S(1)} %get-tuple-element.30), channel_id=1, source_target_pairs={{0,8},{8,16},{16,24},{24,0},{1,9},{9,17},{17,25},{25,1},{2,10},{10... | collective-permute-start | bytes 49160 | tf_op jit(solution)/shard_map/ppermute | solution.py:49
  94.7 13.5 %collective-permute-start.22 = (f32[8,512]{1,0:T(8,128)S(1)}, f32[8,512]{1,0:T(8,128)S(1)}, u32[]{:S(2)}, u32[]{:S(2)}) collective-permute-start(f32[8,512]{1,0:T(8,128)S(1)} %get-tuple-element.31), channel_id=1, source_target_pairs={{0,16},{8,24},{16,0},{24,8},{1,17},{9,25},{17,1},{25,9},{2,18},{10... | collective-permute-start | bytes 49160 | tf_op jit(solution)/shard_map/ppermute | solution.py:49
  97.4 10.8 %collective-permute-start.23 = (f32[8,512]{1,0:T(8,128)S(1)}, f32[8,512]{1,0:T(8,128)S(1)}, u32[]{:S(2)}, u32[]{:S(2)}) collective-permute-start(f32[8,512]{1,0:T(8,128)S(1)} %get-tuple-element.32), channel_id=1, source_target_pairs={{0,24},{8,0},{16,8},{24,16},{1,25},{9,1},{17,9},{25,17},{2,26},{10... | collective-permute-start | bytes 49160 | tf_op jit(solution)/shard_map/ppermute | solution.py:49
  99.4 7.6 %collective-permute-start.24 = (f32[32,64]{1,0:T(8,128)S(1)}, f32[32,64]{1,0:T(8,128)S(1)}, u32[]{:S(2)}, u32[]{:S(2)}) collective-permute-start(f32[32,64]{1,0:T(8,128)S(1)} %get-tuple-element.36), channel_id=1, source_target_pairs={{5,0},{7,32},{3,64},{1,96},{0,128},{2,160},{6,192},{4,224},{13,8},... | collective-permute-start | bytes 24584 | tf_op jit(solution)/shard_map/ppermute | solution.py:45
  99.4 7.8 %collective-permute-start.25 = (f32[32,64]{1,0:T(8,128)S(1)}, f32[32,64]{1,0:T(8,128)S(1)}, u32[]{:S(2)}, u32[]{:S(2)}) collective-permute-start(f32[32,64]{1,0:T(8,128)S(1)} %get-tuple-element.37), channel_id=1, source_target_pairs={{5,0},{7,32},{3,64},{1,96},{0,128},{2,160},{6,192},{4,224},{13,8},... | collective-permute-start | bytes 24584 | tf_op jit(solution)/shard_map/ppermute | solution.py:45
  (19 other events, 137.7 us)

commit v5 on v3

--- a/solution.py
+++ b/solution.py
@@ -17,6 +17,7 @@
 SEQS = NY * ROWS
 COLS = 256
 BLOCK = 64
+CHANS = 16
 WIDTH = NZ * BLOCK
 
 eps = 1e-06
@@ -68,10 +69,12 @@
     return high, low
 
 
-def pack_kernel(w_in, w_val, w_gate, out, soon, first, row, sems):
+def pack_kernel(w_in, w_val, w_gate, out, soon, late, first, row, tail, sems):
     parts = [(w_in.at[0], first), (w_val.at[0], row.at[:, pl.ds(0, COLS)])]
     parts += [(w_gate.at[0], row.at[:, pl.ds(COLS, COLS)])]
     parts += [(w_in.at[1], row.at[:, pl.ds(2 * COLS, COLS)])]
+    parts += [(w_val.at[1], tail.at[:, pl.ds(0, COLS)])]
+    parts += [(w_gate.at[1], tail.at[:, pl.ds(COLS, COLS)])]
     copies = [pltpu.make_async_copy(a, b, sems.at[i]) for i, (a, b) in enumerate(parts)]
     for copy in copies:
         copy.start()
@@ -80,6 +83,7 @@
     for i in range(NZ):
         out[i] = first[...]
     soon[...] = row[...]
+    late[...] = tail[...]
 
 
 def prep_kernel(
@@ -92,12 +96,10 @@
     r_im,
     d_skip,
     state,
-    w_val,
-    w_gate,
     base,
-    drive,
+    drive_high,
+    drive_low,
     carried,
-    late,
 ):
     groups, chans, half = b_re.shape[1:]
     size = groups * chans
@@ -131,29 +133,34 @@
             base[n, :, g, :] = new
             offsets.append(times_turned(new, reads[g], HIGHEST))
         dcat = jnp.concatenate(drives)
-        drive[n] = dcat
+        spread = []
+        for g in range(groups):
+            zero = jnp.zeros_like(drives[g])
+            spread.append(jnp.concatenate([drives[g] if h == g else zero for h in range(groups)], axis=1))
+        drive_high[n], drive_low[n] = two_halves(jnp.concatenate(spread))
         full = times_turned(dcat, jnp.concatenate(reads), HIGHEST)
         mix = jnp.where(row // chans == col // chans, full, 0.0)
         mix = mix + jnp.where(row == col, d_skip[n : n + 1, :], 0.0)
         carried[n * SEQS : (n + 1) * SEQS, :] = jnp.concatenate(offsets, axis=1)
-        if n == 0:
-            carried[LAYERS * SEQS :, :] = mix
-        else:
-            late[...] = jnp.concatenate([w_val[n], w_gate[n], *two_halves(mix)], axis=1)
-
-
-def write_payload(pay_ref, x, blocks, offset, mix=None):
+        compact = mix[:chans]
+        for g in range(1, groups):
+            compact = compact + mix[g * chans : (g + 1) * chans]
+        top = LAYERS * SEQS + n * chans
+        carried[top : top + chans, :] = compact
+
+
+def write_payload(pay_ref, x, blocks, carried, n):
     squares = jnp.sum(x * x, axis=1, keepdims=True)
     s_high, s_low = two_halves(squares)
-    lane = lax.broadcasted_iota(jnp.int32, (SEQS, 128), 1)
+    lane = lax.broadcasted_iota(jnp.int32, (SEQS, BLOCK), 1)
     s_part = jnp.where(lane == 0, s_high.astype(f32), jnp.where(lane == 1, s_low.astype(f32), 0.0))
-    parts = [blocks[j].astype(bf16) for j in range(NZ)]
-    parts += [*two_halves(offset), s_part.astype(bf16)]
-    if mix is not None:
-        half = BLOCK // 2
-        for m in two_halves(mix):
-            parts += [m[:half], m[half:]]
-    row = jnp.concatenate(parts, axis=1)
+    top = LAYERS * SEQS + n * CHANS
+    row = jnp.concatenate(
+        [blocks[j].astype(bf16) for j in range(NZ)]
+        + [*two_halves(carried[n * SEQS : (n + 1) * SEQS])]
+        + [jnp.concatenate(two_halves(carried[top : top + CHANS])), s_part.astype(bf16)],
+        axis=1,
+    )
     for i in range(ND):
         pay_ref[i] = row
 
@@ -172,7 +179,7 @@
     x_ref[...] = x
     normed = (x * gain[0:1]).astype(bf16)
     blocks = [times_turned(normed, w[j]) for j in range(NZ)]
-    write_payload(pay_ref, x, blocks, carried[:SEQS], carried[LAYERS * SEQS :])
+    write_payload(pay_ref, x, blocks, carried, 0)
 
 
 def next_kernel(out, r1, r2, r3, x_old, gain, carried, *refs):
@@ -186,20 +193,23 @@
     normed = (x * gain[1:2]).astype(bf16)
     for k in range(NZ):
         blocks[lax.rem(z + NZ - k, NZ)] = times_turned(normed, w[k][:, 2 * COLS : 3 * COLS])
-    write_payload(pay_ref, x, blocks, carried[SEQS : LAYERS * SEQS])
+    write_payload(pay_ref, x, blocks, carried, 1)
 
 
 def inputs_of(got):
     total = got[0, :, :WIDTH].astype(f32)
-    squares = got[0, :, WIDTH + 128 : WIDTH + 256].astype(f32)
+    squares = got[0, :, WIDTH + 192 :].astype(f32)
     for i in range(1, ND):
         total = total + got[i, :, :WIDTH].astype(f32)
-        squares = squares + got[i, :, WIDTH + 128 : WIDTH + 256].astype(f32)
+        squares = squares + got[i, :, WIDTH + 192 :].astype(f32)
     return total * lax.rsqrt(jnp.sum(squares, axis=1, keepdims=True) / D + eps)
 
 
 def gated(got, u_blocks, w, ordered, weights):
     z = lax.axis_index("z")
+    row = lax.broadcasted_iota(jnp.int32, (BLOCK, BLOCK), 0)
+    col = lax.broadcasted_iota(jnp.int32, (BLOCK, BLOCK), 1)
+    same = row // CHANS == col // CHANS
     for delta in range(NZ):
         block, slot, source = lax.rem(z + delta, NZ), (NZ - delta) % NZ, place(z, delta)
         sent = got[source]
@@ -207,13 +217,9 @@
         offset = offset + sent[:, WIDTH + BLOCK : WIDTH + 2 * BLOCK].astype(f32)
         cut = slice(slot * BLOCK, (slot + 1) * BLOCK)
         weights[cut, :] = w[slot][:, : 2 * COLS]
-        if got.shape[2] == NEXT_PAY:
-            m_high = w[slot][:, 2 * COLS : 2 * COLS + BLOCK]
-            m_low = w[slot][:, 2 * COLS + BLOCK :]
-        else:
-            m = sent[:, WIDTH + 256 :]
-            m_high = jnp.concatenate([m[:, :BLOCK], m[:, BLOCK : 2 * BLOCK]], axis=0)
-            m_low = jnp.concatenate([m[:, 2 * BLOCK : 3 * BLOCK], m[:, 3 * BLOCK :]], axis=0)
+        m = sent[:, WIDTH + 128 : WIDTH + 192].astype(f32)
+        m_high = jnp.where(same, jnp.concatenate([m[:CHANS]] * (BLOCK // CHANS)), 0.0).astype(bf16)
+        m_low = jnp.where(same, jnp.concatenate([m[CHANS:]] * (BLOCK // CHANS)), 0.0).astype(bf16)
         high, low = two_halves(u_blocks[block])
         pre = (
             offset
@@ -249,7 +255,8 @@
 
 def inputs_kernel(got, earlier, u_blocks, own_u):
     split_blocks(inputs_of(got), u_blocks)
-    own_u[...] = own_block(u_blocks)
+    own_u[:SEQS, :] = earlier[...]
+    own_u[SEQS:, :] = own_block(u_blocks)
 
 
 def last_kernel(got, u_blocks, *refs):
@@ -270,14 +277,17 @@
     out[...] = (mine + total[:, :COLS] * jax.nn.sigmoid(total[:, COLS:])).astype(bf16)
 
 
-def states_kernel(base, drive, u0, u1, out):
-    groups = base.shape[2]
-    chans = BLOCK // groups
-    for n, u in enumerate((u0, u1)):
+def states_kernel(base, drive_high, drive_low, u, out):
+    groups, doubled = base.shape[2:]
+    for n in range(LAYERS):
+        high, low = two_halves(u[n * SEQS : (n + 1) * SEQS, :])
+        push = (
+            jnp.dot(high, drive_low[n], preferred_element_type=f32)
+            + jnp.dot(low, drive_high[n], preferred_element_type=f32)
+            + jnp.dot(high, drive_high[n], preferred_element_type=f32)
+        )
         for g in range(groups):
-            cut = slice(g * chans, (g + 1) * chans)
-            push = jnp.dot(u[:, cut], drive[n, cut, :], precision=HIGHEST, preferred_element_type=f32)
-            out[n, :, g, :] = base[n, :, g, :] + push
+            out[n, :, g, :] = base[n, :, g, :] + push[:, g * doubled : (g + 1) * doubled]
 
 
 def call(body, args, outs, scratch=(), scalar=None, space=pltpu.VMEM):
@@ -297,8 +307,7 @@
     return jax.ShapeDtypeStruct(dims, dtype)
 
 
-FIRST_PAY = WIDTH + 512
-NEXT_PAY = WIDTH + 256
+PAY_OUTS = [shape((ND, SEQS, WIDTH + 256), bf16), shape((SEQS, COLS))]
 BLOCKS = pltpu.VMEM((NZ, SEQS, BLOCK), f32)
 GATED = [pltpu.VMEM((SEQS, WIDTH), bf16), pltpu.VMEM((WIDTH, 2 * COLS), bf16)]
 
@@ -320,20 +329,27 @@
     state,
 ):
     w_turned = jnp.swapaxes(w_input, 1, 2)
-    packed, soon = call(
+    packed, soon, late = call(
         pack_kernel,
         [w_turned, w_val, w_gate],
-        [shape((NZ, BLOCK, COLS), bf16), shape((BLOCK, 3 * COLS), bf16)],
+        [
+            shape((NZ, BLOCK, COLS), bf16),
+            shape((BLOCK, 3 * COLS), bf16),
+            shape((BLOCK, 2 * COLS), bf16),
+        ],
         [
             pltpu.VMEM((BLOCK, COLS), bf16),
             pltpu.VMEM((BLOCK, 3 * COLS), bf16),
-            pltpu.SemaphoreType.DMA((4,)),
+            pltpu.VMEM((BLOCK, 2 * COLS), bf16),
+            pltpu.SemaphoreType.DMA((6,)),
         ],
         space=pl.ANY,
     )
     first_w = lax.all_to_all(packed, "z", 0, 0, tiled=True)
-    pieces = [stream] + [shift_y(stream, k) for k in range(1, NY)]
-    base, drive, own, late = call(
+    after = shift_y(stream, 1)
+    before = shift_y(stream, -1)
+    pieces = [stream, after, shift_y(after, 1), before]
+    base, drive_high, drive_low, own = call(
         prep_kernel,
         [
             lam_re,
@@ -345,14 +361,12 @@
             readout_imaginary,
             d_skip,
             state,
-            w_val,
-            w_gate,
         ],
         [
             shape(state.shape),
-            shape((LAYERS, BLOCK, state.shape[-1])),
-            shape((LAYERS * SEQS + BLOCK, BLOCK)),
-            shape((BLOCK, 2 * COLS + 2 * BLOCK), bf16),
+            shape((LAYERS, BLOCK, 2 * COLS), bf16),
+            shape((LAYERS, BLOCK, 2 * COLS), bf16),
+            shape((LAYERS * (SEQS + CHANS), BLOCK)),
         ],
         scalar=2,
     )
@@ -363,7 +377,7 @@
     payload, x = call(
         first_kernel,
         [*pieces, norm_gain, carried, first_w],
-        [shape((ND, SEQS, FIRST_PAY), bf16), shape((SEQS, COLS))],
+        PAY_OUTS,
         [pltpu.VMEM((NY, ROWS, COLS), f32)],
     )
     got = lax.all_to_all(payload, DP, 0, 0, tiled=True)
@@ -374,18 +388,17 @@
         [BLOCKS, *GATED],
     )
     others = [shift_y(out, k) for k in range(1, NY)]
-    u0 = turn(u0, back=True)
     payload, x = call(
         next_kernel,
         [out, *others, x, norm_gain, carried, *ring_soon],
-        [shape((ND, SEQS, NEXT_PAY), bf16), shape((SEQS, COLS))],
+        PAY_OUTS,
         [BLOCKS],
     )
     got = lax.all_to_all(payload, DP, 0, 0, tiled=True)
-    u, u1 = call(
-        inputs_kernel, [got, u0], [shape((NZ, SEQS, BLOCK)), shape((SEQS, BLOCK))]
-    )
-    u1 = turn(u1, back=True)
+    u, both = call(
+        inputs_kernel, [got, u0], [shape((NZ, SEQS, BLOCK)), shape((LAYERS * SEQS, BLOCK))]
+    )
+    both = turn(both, back=True)
     own, s1, s2, s3 = call(
         last_kernel,
         [got, u, *ring_late],
@@ -394,7 +407,7 @@
     )
     others = [shift_y(sent, k) for k, sent in enumerate((s1, s2, s3), 1)]
     (stream,) = call(stream_kernel, [own, *others, x], [shape((ROWS, COLS), bf16)])
-    (states,) = call(states_kernel, [base, drive, u0, u1], [shape(state.shape)])
+    (states,) = call(states_kernel, [base, drive_high, drive_low, both], [shape(state.shape)])
     return (stream, states)
 
 

time: 112 us -> 98.6 us (0.88)
  the two profiles are of different devices: /device:TPU:110 before, /device:TPU:2 now
where the time goes in v5:
time: 98.6 us; the launch traced here: 98.1 us
  starting transfers between devices  54 us (55%)
  waiting for transfers between devices  34.7 us (35%)
  Pallas kernels  7.86 us (8%)
    ppermute x14, waiting for transfers between devices, shift_z(): return lax.ppermute(value, 'z', [(i, (i + k) % NZ) for i in range(NZ)])  23 us
    ppermute x14, starting transfers between devices, shift_z(): return lax.ppermute(value, 'z', [(i, (i + k) % NZ) for i in range(NZ)])  18.6 us
    ppermute x9, starting transfers between devices, shift_y(): return lax.ppermute(value, 'y', [(i, (i + k) % NY) for i in range(NY)])  12.4 us
    all_to_all x2, starting transfers between devices, both_layers(): got = lax.all_to_all(payload, DP, 0, 0, tiled=True)  11.9 us
    ppermute x9, waiting for transfers between devices, shift_y(): return lax.ppermute(value, 'y', [(i, (i + k) % NY) for i in range(NY)])  11.7 us
    all_to_all x1, starting transfers between devices, both_layers(): first_w = lax.all_to_all(packed, 'z', 0, 0, tiled=True)  8.61 us
    pallas_call x9, Pallas kernels, call(): pl.pallas_call(body, in_specs=[pl.BlockSpec(memory_space=s) for s in spac...  7.86 us
    ppermute x2, starting transfers between devices, turn(): return lax.ppermute(value, ALL, pairs)  2.47 us
  transfers between devices with their start and end apart: 28, of which 15 were waited for; matrix products, arithmetic and copies ran while one was open for 0% of the time, Pallas kernels for 4%

profile of v5, /device:TPU:2, one launch (start us, length us, event | category | flops | bytes accessed | tf_op | source)
XLA Modules:
  0.0 98.1 jit_solution(15134436212602721540)
XLA Ops:
  0.6 1.7 %shard_map.150 = (bf16[8,64,256]{2,1,0:T(8,128)(2,1)}, bf16[64,768]{1,0:T(8,128)(2,1)}, bf16[64,512]{1,0:T(8,128)(2,1)}) custom-call(bf16[2,64,256]{2,1,0:T(8,128)(2,1)} %bitcast.5, bf16[2,64,256]{2,1,0:T(8,128)(2,1)} %w_val.1, bf16[2,64,256]{2,1,0:T(8,128)(2,1)} %w_gate.1), custom_call_target="tpu_custom_call" | custom-call | flops 16777216 | bytes 1048576 | tf_op jit(solution)/shard_map/pallas_call | solution.py:295
  2.4 8.6 %all-to-all-start = ((bf16[8,64,256]{2,1,0:T(8,128)(2,1)}), bf16[8,64,256]{2,1,0:T(8,128)(2,1)S(1)}, u32[]{:S(2)}, u32[]{:S(2)}) async-start(bf16[8,64,256]{2,1,0:T(8,128)(2,1)} %get-tuple-element.22), calls=%async_computation | async-start | bytes 524288 | tf_op jit(solution)/shard_map/all_to_all | solution.py:348
  11.0 2.1 %collective-permute-start.4 = (bf16[64,768]{1,0:T(8,128)(2,1)S(1)}, bf16[64,768]{1,0:T(8,128)(2,1)S(1)}, u32[]{:S(2)}, u32[]{:S(2)}) collective-permute-start(bf16[64,768]{1,0:T(8,128)(2,1)S(1)} %copy-done), channel_id=1, source_target_pairs={{0,32},{32,64},{64,96},{96,128},{128,160},{160,192},{192,224},{224... | collective-permute-start | bytes 294920 | tf_op jit(solution)/shard_map/ppermute | solution.py:54
  15.0 2.4 %collective-permute-start.3 = (f32[96,64]{1,0:T(8,128)S(1)}, f32[96,64]{1,0:T(8,128)S(1)}, u32[]{:S(2)}, u32[]{:S(2)}) collective-permute-start(f32[96,64]{1,0:T(8,128)S(1)} %get-tuple-element.21), channel_id=1, source_target_pairs={{0,5},{32,7},{64,3},{96,1},{128,0},{160,2},{192,6},{224,4},{8,13},... | collective-permute-start | bytes 73736 | tf_op jit(solution)/shard_map/ppermute | solution.py:46
  18.9 1.7 %collective-permute-start.2 = (bf16[8,256]{1,0:T(8,128)(2,1)S(1)}, bf16[8,256]{1,0:T(8,128)(2,1)S(1)}, u32[]{:S(2)}, u32[]{:S(2)}) collective-permute-start(bf16[8,256]{1,0:T(8,128)(2,1)S(1)} %copy-done.10), channel_id=1, source_target_pairs={{0,24},{8,0},{16,8},{24,16},{1,25},{9,1},{17,9},{25,17},{2,26},{10... | collective-permute-start | bytes 12296 | tf_op jit(solution)/shard_map/ppermute | solution.py:50
  22.5 4.4 %collective-permute-done.1.p2 = bf16[8,256]{1,0:T(8,128)(2,1)S(1)} collective-permute-done((bf16[8,256]{1,0:T(8,128)(2,1)S(1)}, bf16[8,256]{1,0:T(8,128)(2,1)S(1)}, u32[]{:S(2)}, u32[]{:S(2)}) %collective-permute-start.1) | collective-permute-done | bytes 4128 | tf_op jit(solution)/shard_map/ppermute | solution.py:50
  28.0 7.0 %all-to-all-start.1 = ((bf16[8,32,768]{2,1,0:T(8,128)(2,1)}), bf16[8,32,768]{2,1,0:T(8,128)(2,1)S(1)}, u32[]{:S(2)}, u32[]{:S(2)}) async-start(bf16[8,32,768]{2,1,0:T(8,128)(2,1)} %get-tuple-element.23), calls=%async_computation.1 | async-start | bytes 786432 | tf_op jit(solution)/shard_map/all_to_all | solution.py:383
  35.3 1.7 %collective-permute-start.5 = (bf16[64,768]{1,0:T(8,128)(2,1)S(1)}, bf16[64,768]{1,0:T(8,128)(2,1)S(1)}, u32[]{:S(2)}, u32[]{:S(2)}) collective-permute-start(bf16[64,768]{1,0:T(8,128)(2,1)S(1)} %collective-permute-done.4.refs_1_), channel_id=1, source_target_pairs={{0,32},{32,64},{64,96},{96,128},{128,160},{160,192},{192,224},{224... | collective-permute-start | bytes 294920 | tf_op jit(solution)/shard_map/ppermute | solution.py:54
  37.0 2.8 %collective-permute-done.8.refs_7_ = bf16[64,768]{1,0:T(8,128)(2,1)S(1)} collective-permute-done((bf16[64,768]{1,0:T(8,128)(2,1)S(1)}, bf16[64,768]{1,0:T(8,128)(2,1)S(1)}, u32[]{:S(2)}, u32[]{:S(2)}) %collective-permute-start.8) | collective-permute-done | bytes 98336 | tf_op jit(solution)/shard_map/ppermute | solution.py:54
  41.9 2.6 %collective-permute-done.9.refs_6_ = bf16[64,768]{1,0:T(8,128)(2,1)S(1)} collective-permute-done((bf16[64,768]{1,0:T(8,128)(2,1)S(1)}, bf16[64,768]{1,0:T(8,128)(2,1)S(1)}, u32[]{:S(2)}, u32[]{:S(2)}) %collective-permute-start.9) | collective-permute-done | bytes 98336 | tf_op jit(solution)/shard_map/ppermute | solution.py:54
  44.4 2.7 %collective-permute-start.10 = (bf16[64,768]{1,0:T(8,128)(2,1)S(1)}, bf16[64,768]{1,0:T(8,128)(2,1)S(1)}, u32[]{:S(2)}, u32[]{:S(2)}) collective-permute-start(bf16[64,768]{1,0:T(8,128)(2,1)S(1)} %collective-permute-done.9.refs_6_), channel_id=1, source_target_pairs={{0,224},{32,0},{64,32},{96,64},{128,96},{160,128},{192,160},{224,1... | collective-permute-start | bytes 294920 | tf_op jit(solution)/shard_map/ppermute | solution.py:54
  47.2 2.2 %collective-permute-done.10.refs_5_ = bf16[64,768]{1,0:T(8,128)(2,1)S(1)} collective-permute-done((bf16[64,768]{1,0:T(8,128)(2,1)S(1)}, bf16[64,768]{1,0:T(8,128)(2,1)S(1)}, u32[]{:S(2)}, u32[]{:S(2)}) %collective-permute-start.10) | collective-permute-done | bytes 98336 | tf_op jit(solution)/shard_map/ppermute | solution.py:54
  49.4 3.6 %collective-permute-done.7.refs_4_ = bf16[64,768]{1,0:T(8,128)(2,1)S(1)} collective-permute-done((bf16[64,768]{1,0:T(8,128)(2,1)S(1)}, bf16[64,768]{1,0:T(8,128)(2,1)S(1)}, u32[]{:S(2)}, u32[]{:S(2)}) %collective-permute-start.7) | collective-permute-done | bytes 98336 | tf_op jit(solution)/shard_map/ppermute | solution.py:54
  54.0 2.9 %collective-permute-start.12 = (f32[32,512]{1,0:T(8,128)S(1)}, f32[32,512]{1,0:T(8,128)S(1)}, u32[]{:S(2)}, u32[]{:S(2)}) collective-permute-start(f32[32,512]{1,0:T(8,128)S(1)} %get-tuple-element.25.out), channel_id=1, source_target_pairs={{0,16},{8,24},{16,0},{24,8},{1,17},{9,25},{17,1},{25,9},{2,18},{10... | collective-permute-start | bytes 196616 | tf_op jit(solution)/shard_map/ppermute | solution.py:50
  62.3 4.9 %all-to-all-start.2 = ((bf16[8,32,768]{2,1,0:T(8,128)(2,1)}), bf16[8,32,768]{2,1,0:T(8,128)(2,1)S(1)}, u32[]{:S(2)}, u32[]{:S(2)}) async-start(bf16[8,32,768]{2,1,0:T(8,128)(2,1)} %get-tuple-element.27), calls=%async_computation.2 | async-start | bytes 786432 | tf_op jit(solution)/shard_map/all_to_all | solution.py:397
  67.2 3.2 %collective-permute-start.18 = (bf16[64,512]{1,0:T(8,128)(2,1)S(1)}, bf16[64,512]{1,0:T(8,128)(2,1)S(1)}, u32[]{:S(2)}, u32[]{:S(2)}) collective-permute-start(bf16[64,512]{1,0:T(8,128)(2,1)S(1)} %copy-done.6), channel_id=1, source_target_pairs={{0,224},{32,0},{64,32},{96,64},{128,96},{160,128},{192,160},{224,1... | collective-permute-start | bytes 196616 | tf_op jit(solution)/shard_map/ppermute | solution.py:54
  70.5 2.2 %collective-permute-done.14.refs_1_ = bf16[64,512]{1,0:T(8,128)(2,1)S(1)} collective-permute-done((bf16[64,512]{1,0:T(8,128)(2,1)S(1)}, bf16[64,512]{1,0:T(8,128)(2,1)S(1)}, u32[]{:S(2)}, u32[]{:S(2)}) %collective-permute-start.14) | collective-permute-done | bytes 65568 | tf_op jit(solution)/shard_map/ppermute | solution.py:54
  72.7 3.2 %collective-permute-start.19 = (bf16[64,512]{1,0:T(8,128)(2,1)S(1)}, bf16[64,512]{1,0:T(8,128)(2,1)S(1)}, u32[]{:S(2)}, u32[]{:S(2)}) collective-permute-start(bf16[64,512]{1,0:T(8,128)(2,1)S(1)} %collective-permute-done.18.refs_7_), channel_id=1, source_target_pairs={{0,224},{32,0},{64,32},{96,64},{128,96},{160,128},{192,160},{224,1... | collective-permute-start | bytes 196616 | tf_op jit(solution)/shard_map/ppermute | solution.py:54
  75.9 2.2 %collective-permute-done.15.refs_2_ = bf16[64,512]{1,0:T(8,128)(2,1)S(1)} collective-permute-done((bf16[64,512]{1,0:T(8,128)(2,1)S(1)}, bf16[64,512]{1,0:T(8,128)(2,1)S(1)}, u32[]{:S(2)}, u32[]{:S(2)}) %collective-permute-start.15) | collective-permute-done | bytes 65568 | tf_op jit(solution)/shard_map/ppermute | solution.py:54
  78.2 3.2 %collective-permute-start.20 = (bf16[64,512]{1,0:T(8,128)(2,1)S(1)}, bf16[64,512]{1,0:T(8,128)(2,1)S(1)}, u32[]{:S(2)}, u32[]{:S(2)}) collective-permute-start(bf16[64,512]{1,0:T(8,128)(2,1)S(1)} %collective-permute-done.19.refs_6_), channel_id=1, source_target_pairs={{0,224},{32,0},{64,32},{96,64},{128,96},{160,128},{192,160},{224,1... | collective-permute-start | bytes 196616 | tf_op jit(solution)/shard_map/ppermute | solution.py:54
  81.4 2.2 %collective-permute-done.16.refs_3_ = bf16[64,512]{1,0:T(8,128)(2,1)S(1)} collective-permute-done((bf16[64,512]{1,0:T(8,128)(2,1)S(1)}, bf16[64,512]{1,0:T(8,128)(2,1)S(1)}, u32[]{:S(2)}, u32[]{:S(2)}) %collective-permute-start.16) | collective-permute-done | bytes 65568 | tf_op jit(solution)/shard_map/ppermute | solution.py:54
  84.0 5.1 %collective-permute-done.17.refs_4_ = bf16[64,512]{1,0:T(8,128)(2,1)S(1)} collective-permute-done((bf16[64,512]{1,0:T(8,128)(2,1)S(1)}, bf16[64,512]{1,0:T(8,128)(2,1)S(1)}, u32[]{:S(2)}, u32[]{:S(2)}) %collective-permute-start.17) | collective-permute-done | bytes 65568 | tf_op jit(solution)/shard_map/ppermute | solution.py:54
  90.6 3.1 %collective-permute-start.22 = (f32[8,512]{1,0:T(8,128)S(1)}, f32[8,512]{1,0:T(8,128)S(1)}, u32[]{:S(2)}, u32[]{:S(2)}) collective-permute-start(f32[8,512]{1,0:T(8,128)S(1)} %get-tuple-element.33), channel_id=1, source_target_pairs={{0,16},{8,24},{16,0},{24,8},{1,17},{9,25},{17,1},{25,9},{2,18},{10... | collective-permute-start | bytes 49160 | tf_op jit(solution)/shard_map/ppermute | solution.py:50
  95.8 1.6 %collective-permute-done.23.r3 = f32[8,512]{1,0:T(8,128)S(1)} collective-permute-done((f32[8,512]{1,0:T(8,128)S(1)}, f32[8,512]{1,0:T(8,128)S(1)}, u32[]{:S(2)}, u32[]{:S(2)}) %collective-permute-start.23) | collective-permute-done | bytes 16416 | tf_op jit(solution)/shard_map/ppermute | solution.py:50
  (67 shorter events, 19.6 us)
Async XLA Ops:
  2.4 24.6 %all-to-all-start = ((bf16[8,64,256]{2,1,0:T(8,128)(2,1)}), bf16[8,64,256]{2,1,0:T(8,128)(2,1)S(1)}, u32[]{:S(2)}, u32[]{:S(2)}) async-start(bf16[8,64,256]{2,1,0:T(8,128)(2,1)} %get-tuple-element.22), calls=%async_computation | async-start | bytes 524288 | tf_op jit(solution)/shard_map/all_to_all | solution.py:348
  11.0 24.3 %collective-permute-start.4 = (bf16[64,768]{1,0:T(8,128)(2,1)S(1)}, bf16[64,768]{1,0:T(8,128)(2,1)S(1)}, u32[]{:S(2)}, u32[]{:S(2)}) collective-permute-start(bf16[64,768]{1,0:T(8,128)(2,1)S(1)} %copy-done), channel_id=1, source_target_pairs={{0,32},{32,64},{64,96},{96,128},{128,160},{160,192},{192,224},{224... | collective-permute-start | bytes 294920 | tf_op jit(solution)/shard_map/ppermute | solution.py:54
  15.0 12.0 %collective-permute-start.3 = (f32[96,64]{1,0:T(8,128)S(1)}, f32[96,64]{1,0:T(8,128)S(1)}, u32[]{:S(2)}, u32[]{:S(2)}) collective-permute-start(f32[96,64]{1,0:T(8,128)S(1)} %get-tuple-element.21), channel_id=1, source_target_pairs={{0,5},{32,7},{64,3},{96,1},{128,0},{160,2},{192,6},{224,4},{8,13},... | collective-permute-start | bytes 73736 | tf_op jit(solution)/shard_map/ppermute | solution.py:46
  17.4 4.8 %collective-permute-start = (bf16[8,256]{1,0:T(8,128)(2,1)S(1)}, bf16[8,256]{1,0:T(8,128)(2,1)S(1)}, u32[]{:S(2)}, u32[]{:S(2)}) collective-permute-start(bf16[8,256]{1,0:T(8,128)(2,1)S(1)} %copy-done.10), channel_id=1, source_target_pairs={{0,8},{8,16},{16,24},{24,0},{1,9},{9,17},{17,25},{25,1},{2,10},{10... | collective-permute-start | bytes 12296 | tf_op jit(solution)/shard_map/ppermute | solution.py:50
  22.2 4.8 %collective-permute-start.1 = (bf16[8,256]{1,0:T(8,128)(2,1)S(1)}, bf16[8,256]{1,0:T(8,128)(2,1)S(1)}, u32[]{:S(2)}, u32[]{:S(2)}) collective-permute-start(bf16[8,256]{1,0:T(8,128)(2,1)S(1)} %collective-permute-done.p1), channel_id=1, source_target_pairs={{0,8},{8,16},{16,24},{24,0},{1,9},{9,17},{17,25},{25,1},{2,10},{10... | collective-permute-start | bytes 12296 | tf_op jit(solution)/shard_map/ppermute | solution.py:50
  28.0 25.0 %all-to-all-start.1 = ((bf16[8,32,768]{2,1,0:T(8,128)(2,1)}), bf16[8,32,768]{2,1,0:T(8,128)(2,1)S(1)}, u32[]{:S(2)}, u32[]{:S(2)}) async-start(bf16[8,32,768]{2,1,0:T(8,128)(2,1)} %get-tuple-element.23), calls=%async_computation.1 | async-start | bytes 786432 | tf_op jit(solution)/shard_map/all_to_all | solution.py:383
  35.0 4.8 %collective-permute-start.8 = (bf16[64,768]{1,0:T(8,128)(2,1)S(1)}, bf16[64,768]{1,0:T(8,128)(2,1)S(1)}, u32[]{:S(2)}, u32[]{:S(2)}) collective-permute-start(bf16[64,768]{1,0:T(8,128)(2,1)S(1)} %copy-done), channel_id=1, source_target_pairs={{0,224},{32,0},{64,32},{96,64},{128,96},{160,128},{192,160},{224,1... | collective-permute-start | bytes 294920 | tf_op jit(solution)/shard_map/ppermute | solution.py:54
  35.3 6.0 %collective-permute-start.5 = (bf16[64,768]{1,0:T(8,128)(2,1)S(1)}, bf16[64,768]{1,0:T(8,128)(2,1)S(1)}, u32[]{:S(2)}, u32[]{:S(2)}) collective-permute-start(bf16[64,768]{1,0:T(8,128)(2,1)S(1)} %collective-permute-done.4.refs_1_), channel_id=1, source_target_pairs={{0,32},{32,64},{64,96},{96,128},{128,160},{160,192},{192,224},{224... | collective-permute-start | bytes 294920 | tf_op jit(solution)/shard_map/ppermute | solution.py:54
  41.3 5.8 %collective-permute-start.6 = (bf16[64,768]{1,0:T(8,128)(2,1)S(1)}, bf16[64,768]{1,0:T(8,128)(2,1)S(1)}, u32[]{:S(2)}, u32[]{:S(2)}) collective-permute-start(bf16[64,768]{1,0:T(8,128)(2,1)S(1)} %collective-permute-done.5.refs_2_), channel_id=1, source_target_pairs={{0,32},{32,64},{64,96},{96,128},{128,160},{160,192},{192,224},{224... | collective-permute-start | bytes 294920 | tf_op jit(solution)/shard_map/ppermute | solution.py:54
  44.4 4.9 %collective-permute-start.10 = (bf16[64,768]{1,0:T(8,128)(2,1)S(1)}, bf16[64,768]{1,0:T(8,128)(2,1)S(1)}, u32[]{:S(2)}, u32[]{:S(2)}) collective-permute-start(bf16[64,768]{1,0:T(8,128)(2,1)S(1)} %collective-permute-done.9.refs_6_), channel_id=1, source_target_pairs={{0,224},{32,0},{64,32},{96,64},{128,96},{160,128},{192,160},{224,1... | collective-permute-start | bytes 294920 | tf_op jit(solution)/shard_map/ppermute | solution.py:54
  47.2 5.8 %collective-permute-start.7 = (bf16[64,768]{1,0:T(8,128)(2,1)S(1)}, bf16[64,768]{1,0:T(8,128)(2,1)S(1)}, u32[]{:S(2)}, u32[]{:S(2)}) collective-permute-start(bf16[64,768]{1,0:T(8,128)(2,1)S(1)} %collective-permute-done.6.refs_3_), channel_id=1, source_target_pairs={{0,32},{32,64},{64,96},{96,128},{128,160},{160,192},{192,224},{224... | collective-permute-start | bytes 294920 | tf_op jit(solution)/shard_map/ppermute | solution.py:54
  53.7 5.5 %collective-permute-start.11 = (f32[32,512]{1,0:T(8,128)S(1)}, f32[32,512]{1,0:T(8,128)S(1)}, u32[]{:S(2)}, u32[]{:S(2)}) collective-permute-start(f32[32,512]{1,0:T(8,128)S(1)} %get-tuple-element.25.out), channel_id=1, source_target_pairs={{0,8},{8,16},{16,24},{24,0},{1,9},{9,17},{17,25},{25,1},{2,10},{10... | collective-permute-start | bytes 196616 | tf_op jit(solution)/shard_map/ppermute | solution.py:50
  54.0 5.8 %collective-permute-start.12 = (f32[32,512]{1,0:T(8,128)S(1)}, f32[32,512]{1,0:T(8,128)S(1)}, u32[]{:S(2)}, u32[]{:S(2)}) collective-permute-start(f32[32,512]{1,0:T(8,128)S(1)} %get-tuple-element.25.out), channel_id=1, source_target_pairs={{0,16},{8,24},{16,0},{24,8},{1,17},{9,25},{17,1},{25,9},{2,18},{10... | collective-permute-start | bytes 196616 | tf_op jit(solution)/shard_map/ppermute | solution.py:50
  62.3 21.4 %all-to-all-start.2 = ((bf16[8,32,768]{2,1,0:T(8,128)(2,1)}), bf16[8,32,768]{2,1,0:T(8,128)(2,1)S(1)}, u32[]{:S(2)}, u32[]{:S(2)}) async-start(bf16[8,32,768]{2,1,0:T(8,128)(2,1)} %get-tuple-element.27), calls=%async_computation.2 | async-start | bytes 786432 | tf_op jit(solution)/shard_map/all_to_all | solution.py:397
  67.2 5.5 %collective-permute-start.14 = (bf16[64,512]{1,0:T(8,128)(2,1)S(1)}, bf16[64,512]{1,0:T(8,128)(2,1)S(1)}, u32[]{:S(2)}, u32[]{:S(2)}) collective-permute-start(bf16[64,512]{1,0:T(8,128)(2,1)S(1)} %copy-done.6), channel_id=1, source_target_pairs={{0,32},{32,64},{64,96},{96,128},{128,160},{160,192},{192,224},{224... | collective-permute-start | bytes 196616 | tf_op jit(solution)/shard_map/ppermute | solution.py:54
  67.2 5.5 %collective-permute-start.18 = (bf16[64,512]{1,0:T(8,128)(2,1)S(1)}, bf16[64,512]{1,0:T(8,128)(2,1)S(1)}, u32[]{:S(2)}, u32[]{:S(2)}) collective-permute-start(bf16[64,512]{1,0:T(8,128)(2,1)S(1)} %copy-done.6), channel_id=1, source_target_pairs={{0,224},{32,0},{64,32},{96,64},{128,96},{160,128},{192,160},{224,1... | collective-permute-start | bytes 196616 | tf_op jit(solution)/shard_map/ppermute | solution.py:54
  72.7 5.5 %collective-permute-start.15 = (bf16[64,512]{1,0:T(8,128)(2,1)S(1)}, bf16[64,512]{1,0:T(8,128)(2,1)S(1)}, u32[]{:S(2)}, u32[]{:S(2)}) collective-permute-start(bf16[64,512]{1,0:T(8,128)(2,1)S(1)} %collective-permute-done.14.refs_1_), channel_id=1, source_target_pairs={{0,32},{32,64},{64,96},{96,128},{128,160},{160,192},{192,224},{224... | collective-permute-start | bytes 196616 | tf_op jit(solution)/shard_map/ppermute | solution.py:54
  72.7 5.5 %collective-permute-start.19 = (bf16[64,512]{1,0:T(8,128)(2,1)S(1)}, bf16[64,512]{1,0:T(8,128)(2,1)S(1)}, u32[]{:S(2)}, u32[]{:S(2)}) collective-permute-start(bf16[64,512]{1,0:T(8,128)(2,1)S(1)} %collective-permute-done.18.refs_7_), channel_id=1, source_target_pairs={{0,224},{32,0},{64,32},{96,64},{128,96},{160,128},{192,160},{224,1... | collective-permute-start | bytes 196616 | tf_op jit(solution)/shard_map/ppermute | solution.py:54
  78.2 5.5 %collective-permute-start.16 = (bf16[64,512]{1,0:T(8,128)(2,1)S(1)}, bf16[64,512]{1,0:T(8,128)(2,1)S(1)}, u32[]{:S(2)}, u32[]{:S(2)}) collective-permute-start(bf16[64,512]{1,0:T(8,128)(2,1)S(1)} %collective-permute-done.15.refs_2_), channel_id=1, source_target_pairs={{0,32},{32,64},{64,96},{96,128},{128,160},{160,192},{192,224},{224... | collective-permute-start | bytes 196616 | tf_op jit(solution)/shard_map/ppermute | solution.py:54
  78.2 5.8 %collective-permute-start.20 = (bf16[64,512]{1,0:T(8,128)(2,1)S(1)}, bf16[64,512]{1,0:T(8,128)(2,1)S(1)}, u32[]{:S(2)}, u32[]{:S(2)}) collective-permute-start(bf16[64,512]{1,0:T(8,128)(2,1)S(1)} %collective-permute-done.19.refs_6_), channel_id=1, source_target_pairs={{0,224},{32,0},{64,32},{96,64},{128,96},{160,128},{192,160},{224,1... | collective-permute-start | bytes 196616 | tf_op jit(solution)/shard_map/ppermute | solution.py:54
  83.6 5.5 %collective-permute-start.17 = (bf16[64,512]{1,0:T(8,128)(2,1)S(1)}, bf16[64,512]{1,0:T(8,128)(2,1)S(1)}, u32[]{:S(2)}, u32[]{:S(2)}) collective-permute-start(bf16[64,512]{1,0:T(8,128)(2,1)S(1)} %collective-permute-done.16.refs_3_), channel_id=1, source_target_pairs={{0,32},{32,64},{64,96},{96,128},{128,160},{160,192},{192,224},{224... | collective-permute-start | bytes 196616 | tf_op jit(solution)/shard_map/ppermute | solution.py:54
  83.9 9.9 %collective-permute-start.24 = (f32[64,64]{1,0:T(8,128)S(1)}, f32[64,64]{1,0:T(8,128)S(1)}, u32[]{:S(2)}, u32[]{:S(2)}) collective-permute-start(f32[64,64]{1,0:T(8,128)S(1)} %get-tuple-element.39), channel_id=1, source_target_pairs={{5,0},{7,32},{3,64},{1,96},{0,128},{2,160},{6,192},{4,224},{13,8},... | collective-permute-start | bytes 49160 | tf_op jit(solution)/shard_map/ppermute | solution.py:46
  89.6 5.1 %collective-permute-start.21 = (f32[8,512]{1,0:T(8,128)S(1)}, f32[8,512]{1,0:T(8,128)S(1)}, u32[]{:S(2)}, u32[]{:S(2)}) collective-permute-start(f32[8,512]{1,0:T(8,128)S(1)} %get-tuple-element.32), channel_id=1, source_target_pairs={{0,8},{8,16},{16,24},{24,0},{1,9},{9,17},{17,25},{25,1},{2,10},{10... | collective-permute-start | bytes 49160 | tf_op jit(solution)/shard_map/ppermute | solution.py:50
  90.6 5.2 %collective-permute-start.22 = (f32[8,512]{1,0:T(8,128)S(1)}, f32[8,512]{1,0:T(8,128)S(1)}, u32[]{:S(2)}, u32[]{:S(2)}) collective-permute-start(f32[8,512]{1,0:T(8,128)S(1)} %get-tuple-element.33), channel_id=1, source_target_pairs={{0,16},{8,24},{16,0},{24,8},{1,17},{9,25},{17,1},{25,9},{2,18},{10... | collective-permute-start | bytes 49160 | tf_op jit(solution)/shard_map/ppermute | solution.py:50
  (17 other events, 125.0 us)
